TPU v7x, 32 devices: a whole 2x2x4 slice. The times are simulated.
32 devices in a mesh: grp: 2 (over y), sp: 4 (over z), fs: 2 (over x), tp: 2 (over core).
Axes of the slice: x: 2, y: 2, z: 4, core: 2. Of those that a mesh axis runs over, the one named last changes fastest.
Arguments:
- tokens: bfloat16 [8, 256, 2048], P(('grp', 'fs'), 'sp'), parts along dimension 0, may hold values from -6 to 6
- pre_gain: float32 [2048], replicated, may hold values from 0.1 to 1.9
- query_weight: bfloat16 [2048, 1024], P(('sp', 'fs'), 'tp'), may hold values from -0.125 to 0.125
- key_weight: bfloat16 [2048, 1024], P(('sp', 'fs'), 'tp'), may hold values from -0.125 to 0.125
- value_weight: bfloat16 [2048, 1024], P(('sp', 'fs'), 'tp'), may hold values from -0.125 to 0.125
- beta_weight: bfloat16 [2048, 8], replicated, may hold values from -0.125 to 0.125
- decay_weight: bfloat16 [2048, 8], replicated, may hold values from -0.125 to 0.125
- decay_rate: float32 [8], replicated, may hold values from 0 to 1
- delta_gain: float32 [128], replicated, may hold values from 0.1 to 1.9
- query_down: bfloat16 [2048, 512], P(('sp', 'fs')), may hold values from -0.125 to 0.125
- latent_down: bfloat16 [2048, 256], P(('sp', 'fs')), may hold values from -0.125 to 0.125
- rope_weight: bfloat16 [2048, 32], replicated, may hold values from -0.125 to 0.125
- query_gain: float32 [512], replicated, may hold values from 0.1 to 1.9
- latent_gain: float32 [256], replicated, may hold values from 0.1 to 1.9
- query_up: bfloat16 [512, 1536], P(None, 'tp'), may hold values from -4 to 4
- latent_up: bfloat16 [256, 2048], P(None, 'tp'), may hold values from -4 to 4
- delta_out: bfloat16 [1024, 2048], P('tp', ('sp', 'fs')), may hold values from -8 to 8
- latent_out: bfloat16 [1024, 2048], P('tp', ('sp', 'fs')), may hold values from -8 to 8
- post_gain: float32 [2048], P('tp'), may hold values from 0.1 to 1.9
Outputs:
- mixed_out: bfloat16 [8, 256, 2048], P(('grp', 'fs'), 'sp', 'tp'), parts along dimension 0
There are 2 independent parts, one for each index of `grp`. A program takes and returns all parts, laid end to end along the dimension named above; an argument that names none is the same for every part. Nothing has to cross between parts.
All inputs are finite; a program needn't handle non-finite values.
Results may differ from a plain program's by a relative error of at most 0.018.
The roundings to bfloat16 on the way count: a program that leaves them out, or rounds other values in their place, can miss the bound.
Values may be sent and summed in bfloat16 or wider, within the bound.
No kernel may reach another device: no remote copies, remote signals or barrier semaphores. Data moves between devices by JAX's collectives and lax.ppermute only.
A program may use at most 128 MiB of HBM per device.

v0:
```python
import math

import jax
import jax.numpy as jnp
import numpy as np
from jax import lax
from jax.experimental import pallas as pl
from jax.experimental.pallas import tpu as pltpu
from jax.sharding import PartitionSpec as P


D = 2048
HEAD = 128
NOPE = 64
ROPE = 32
VDIM = 64
BLOCK = 64


NORM_EPS = 1e-06
ROPE_THETA = 10000.0
HIGHEST = lax.Precision.HIGHEST


def prefix(array, axis, join, neutral):
    place = lax.axis_index(axis)
    gathered = jax.tree.map(
        lambda a, kind: lax.all_gather(a.astype(kind), axis), array, (jnp.bfloat16, jnp.bfloat16)
    )
    state = jax.tree.map(lambda a, e: jnp.zeros_like(a) + jnp.asarray(e, a.dtype), array, neutral)

    def one(step, state):
        return join(
            state,
            jax.tree.map(
                lambda a, own: lax.dynamic_index_in_dim(a, step, 0, False).astype(own.dtype),
                gathered,
                array,
            ),
        )

    return lax.fori_loop(0, place, one, state)


def stored(values):
    return lax.optimization_barrier(values.astype(jnp.bfloat16))


def rms_scale(values):
    return lax.rsqrt(jnp.mean(values * values, axis=-1, keepdims=True) + NORM_EPS)


def unit_rows(values):
    return values * lax.rsqrt(jnp.sum(values * values, axis=-1, keepdims=True) + NORM_EPS)


def rope_tables(positions, rope_width):
    frequency = ROPE_THETA ** (-jnp.arange(0, rope_width, 2, dtype=jnp.float32) / rope_width)
    angles = positions.astype(jnp.float32)[:, None] * frequency[None, :]
    return (jnp.cos(angles), jnp.sin(angles))


def rotate(values, cosine_table, sine_table):
    lower_half, upper_half = jnp.split(values, 2, axis=-1)
    return jnp.concatenate(
        [
            lower_half * cosine_table - upper_half * sine_table,
            upper_half * cosine_table + lower_half * sine_table,
        ],
        axis=-1,
    )


def delta_terms(query_vectors, key_vectors, value_vectors, beta_gate, log_decay):
    length, head_count, _ = query_vectors.shape
    nblocks = length // BLOCK

    def split_blocks(tensor):
        return jnp.moveaxis(tensor.reshape((nblocks, BLOCK, head_count) + tensor.shape[2:]), 2, 0)

    query_vectors = split_blocks(query_vectors)
    key_vectors = split_blocks(key_vectors)
    value_vectors = split_blocks(value_vectors)
    beta_gate = split_blocks(beta_gate)
    gate_sum = jnp.cumsum(split_blocks(log_decay), axis=-1)
    position = jnp.arange(BLOCK)
    strict = position[:, None] > position[None, :]
    causal = position[:, None] >= position[None, :]
    gate_gap = gate_sum[..., :, None] - gate_sum[..., None, :]
    strict_decay = jnp.where(strict, jnp.exp(jnp.where(strict, gate_gap, 0.0)), 0.0)
    causal_decay = jnp.where(causal, jnp.exp(jnp.where(causal, gate_gap, 0.0)), 0.0)
    keys_scaled = key_vectors * beta_gate[..., None]
    lower_mat = (
        jnp.einsum("hnid,hnjd->hnij", keys_scaled, key_vectors, precision=HIGHEST) * strict_decay
    )
    identity = jnp.eye(BLOCK, dtype=jnp.float32)
    inverse = jax.scipy.linalg.solve_triangular(
        identity + lower_mat, jnp.broadcast_to(identity, lower_mat.shape), lower=True
    )
    new_values = jnp.einsum(
        "hnij,hnjd->hnid", inverse, value_vectors * beta_gate[..., None], precision=HIGHEST
    )
    key_weights = jnp.einsum(
        "hnij,hnjd->hnid", inverse, keys_scaled * jnp.exp(gate_sum)[..., None], precision=HIGHEST
    )
    scores = (
        jnp.einsum("hnid,hnjd->hnij", query_vectors, key_vectors, precision=HIGHEST) * causal_decay
    )
    last_gate = gate_sum[..., -1]
    query_decay = query_vectors * jnp.exp(gate_sum)[..., None]
    key_decay = key_vectors * jnp.exp(last_gate[..., None] - gate_sum)[..., None]
    return (query_decay, key_decay, new_values, key_weights, scores, last_gate)


def compose(earlier, following):
    return (
        jnp.einsum("hij,hjk->hik", following[0], earlier[0], precision=HIGHEST),
        jnp.einsum("hij,hjk->hik", following[0], earlier[1], precision=HIGHEST) + following[1],
    )


def keep_same(current):
    return current


def local(
    tokens,
    pre_gain,
    query_weight,
    key_weight,
    value_weight,
    beta_weight,
    decay_weight,
    decay_rate,
    delta_gain,
    query_down,
    latent_down,
    rope_weight,
    query_gain,
    latent_gain,
    query_up,
    latent_up,
    delta_out,
    latent_out,
    post_gain,
):
    f32 = jnp.float32
    seq_count, token_count = (tokens.shape[0], tokens.shape[1])
    row_total = seq_count * token_count
    sequence = tokens.reshape(row_total, tokens.shape[2]).astype(f32)
    query_start = lax.axis_index("sp") * token_count
    positions = query_start + jnp.arange(token_count)
    normed = (sequence * rms_scale(sequence) * pre_gain).astype(jnp.bfloat16)
    head_group = lax.axis_index("tp")
    q_width = query_down.shape[1] // lax.axis_size("tp")
    kv_width = latent_down.shape[1] // lax.axis_size("tp")
    q_own = lax.dynamic_slice_in_dim(query_down, head_group * q_width, q_width, 1)
    kv_own = lax.dynamic_slice_in_dim(latent_down, head_group * kv_width, kv_width, 1)
    portion = (
        lax.all_gather(query_weight, ("sp", "fs"), axis=0, tiled=True),
        lax.all_gather(key_weight, ("sp", "fs"), axis=0, tiled=True),
        lax.all_gather(value_weight, ("sp", "fs"), axis=0, tiled=True),
        lax.all_gather(q_own, ("sp", "fs"), axis=0, tiled=True),
        lax.all_gather(kv_own, ("sp", "fs"), axis=0, tiled=True),
    )
    row_count = portion[0].shape[0]
    projected = tuple((jnp.dot(normed, weight, preferred_element_type=f32) for weight in portion))
    raw_query, raw_key, raw_value, q_half, kv_half = tuple((stored(member) for member in projected))
    q_latent, kv_latent = (
        lax.all_gather(q_half, "tp", axis=1, tiled=True),
        lax.all_gather(kv_half, "tp", axis=1, tiled=True),
    )
    head_count = query_weight.shape[1] // HEAD
    lane_count = seq_count * head_count
    beta_full = jax.nn.sigmoid(jnp.dot(normed, beta_weight, preferred_element_type=f32))
    beta_gate = lax.dynamic_slice_in_dim(beta_full, head_group * head_count, head_count, 1)
    decay_full = jnp.dot(normed, decay_weight, preferred_element_type=f32)
    decay_pre = lax.dynamic_slice_in_dim(decay_full, head_group * head_count, head_count, 1)
    decay_local = lax.dynamic_slice_in_dim(decay_rate, head_group * head_count, head_count, 0)
    log_decay = -decay_local[None, :] * jax.nn.softplus(decay_pre)

    def by_position(values):
        shaped = values.reshape((seq_count, token_count) + values.shape[1:])
        shaped = jnp.moveaxis(shaped, 0, 1)
        return shaped.reshape((token_count, seq_count * values.shape[1]) + values.shape[2:])

    query_vectors = by_position(
        unit_rows(jax.nn.silu(raw_query.astype(f32)).reshape(row_total, head_count, HEAD))
        * HEAD ** (-0.5)
    )
    key_vectors = by_position(
        unit_rows(jax.nn.silu(raw_key.astype(f32)).reshape(row_total, head_count, HEAD))
    )
    value_vectors = by_position(
        jax.nn.silu(raw_value.astype(f32)).reshape(row_total, head_count, HEAD)
    )
    block_terms = delta_terms(
        query_vectors, key_vectors, value_vectors, by_position(beta_gate), by_position(log_decay)
    )
    inputs = tuple((jnp.moveaxis(tensor, 1, 0) for tensor in block_terms))

    def advance(totals, block_in):
        carried, transfer = totals
        query_decay, key_decay, new_values, key_weights, scores, last_gate = block_in
        corrected = new_values - jnp.einsum("hcd,hde->hce", key_weights, carried, precision=HIGHEST)
        output = jnp.einsum("hcd,hde->hce", query_decay, carried, precision=HIGHEST) + jnp.einsum(
            "hij,hje->hie", scores, corrected, precision=HIGHEST
        )
        reader_rows = query_decay - jnp.einsum(
            "hij,hjd->hid", scores, key_weights, precision=HIGHEST
        )
        reader = jnp.einsum("hcd,hde->hce", reader_rows, transfer, precision=HIGHEST)
        factor = jnp.exp(last_gate)[:, None, None]
        carried = carried * factor + jnp.einsum(
            "hcd,hce->hde", key_decay, corrected, precision=HIGHEST
        )
        moved = jnp.einsum("hcd,hde->hce", key_weights, transfer, precision=HIGHEST)
        transfer = transfer * factor - jnp.einsum(
            "hcd,hce->hde", key_decay, moved, precision=HIGHEST
        )
        return ((carried, transfer), (output, reader))

    eye_stack = jnp.broadcast_to(jnp.eye(HEAD, dtype=f32), (lane_count, HEAD, HEAD))
    zero_state = jnp.zeros((lane_count, HEAD, HEAD), f32)
    (state_end, transfer_end), (outputs, readers) = lax.scan(
        advance, (zero_state, eye_stack), inputs
    )
    _, incoming = prefix((transfer_end, state_end), "sp", compose, (eye_stack, zero_state))
    outputs = outputs + jnp.einsum("nhcd,hde->nhce", readers, incoming, precision=HIGHEST)
    delta_raw = jnp.transpose(outputs, (0, 2, 1, 3)).reshape(
        token_count, seq_count, head_count, HEAD
    )
    delta_raw = jnp.moveaxis(delta_raw, 1, 0).reshape(row_total, head_count, HEAD)
    delta_heads = (
        (delta_raw * rms_scale(delta_raw) * delta_gain)
        .astype(jnp.bfloat16)
        .reshape(row_total, head_count * HEAD)
    )
    q_lat32 = q_latent.astype(f32)
    kv_lat32 = kv_latent.astype(f32)
    q_normed = (q_lat32 * rms_scale(q_lat32) * query_gain).astype(jnp.bfloat16)
    kv_normed = (kv_lat32 * rms_scale(kv_lat32) * latent_gain).astype(jnp.bfloat16)
    rope_raw = stored(jnp.dot(normed, rope_weight, preferred_element_type=f32))
    cosine_table, sine_table = rope_tables(positions, rope_raw.shape[1])
    rope_keys = rotate(
        rope_raw.astype(f32).reshape(seq_count, token_count, rope_raw.shape[1]),
        cosine_table,
        sine_table,
    ).astype(jnp.bfloat16)
    latent_count = query_up.shape[1] // (NOPE + ROPE)
    query_all = stored(jnp.dot(q_normed, query_up, preferred_element_type=f32)).reshape(
        seq_count, token_count, latent_count, NOPE + ROPE
    )
    query_plain = query_all[..., :NOPE]
    query_turned = rotate(
        query_all[..., NOPE:].astype(f32), cosine_table[:, None, :], sine_table[:, None, :]
    ).astype(jnp.bfloat16)
    score_scale = (NOPE + ROPE) ** (-0.5)
    query_block = positions // BLOCK
    kv_seq = kv_normed.reshape(seq_count, token_count, kv_normed.shape[1])

    def attend_block(totals, key_plain, value_rows, rope_rows, key_start):
        row_max, row_sum, weighted = totals
        key_block = (key_start + jnp.arange(key_plain.shape[1])) // BLOCK
        allowed = key_block[None, :] <= query_block[:, None]
        logits = (
            jnp.einsum("sqhd,skhd->shqk", query_plain, key_plain, preferred_element_type=f32)
            + jnp.einsum("sqhd,skd->shqk", query_turned, rope_rows, preferred_element_type=f32)
        ) * score_scale
        logits = jnp.where(allowed[None, None], logits, -jnp.inf)
        new_max = jnp.maximum(row_max, jnp.max(logits, axis=-1))
        shift = jnp.where(jnp.isfinite(new_max), new_max, 0.0)
        weights = jnp.where(allowed[None, None], jnp.exp(logits - shift[..., None]), 0.0)
        rescale = jnp.exp(row_max - shift)
        row_sum = row_sum * rescale + jnp.sum(weights, axis=-1)
        weighted = weighted * rescale[..., None] + jnp.einsum(
            "shqk,skhd->shqd", weights.astype(jnp.bfloat16), value_rows, preferred_element_type=f32
        )
        return (new_max, row_sum, weighted)

    start_stats = (
        jnp.full((seq_count, latent_count, token_count), -jnp.inf, f32),
        jnp.zeros((seq_count, latent_count, token_count), f32),
        jnp.zeros((seq_count, latent_count, token_count, VDIM), f32),
    )

    def expand_latent(portion, row_start, span_rows):
        latent_rows = lax.dynamic_slice_in_dim(portion[0], row_start, span_rows, 1)
        expanded = jnp.dot(
            latent_rows.reshape(seq_count * span_rows, latent_rows.shape[2]),
            latent_up,
            preferred_element_type=f32,
        ).astype(jnp.bfloat16)
        expanded = expanded.reshape(seq_count, span_rows, latent_count, NOPE + VDIM)
        return (
            expanded[..., :NOPE],
            expanded[..., NOPE:],
            lax.dynamic_slice_in_dim(portion[1], row_start, span_rows, 1),
        )

    portion = (
        lax.all_gather(kv_seq, "sp", axis=1, tiled=True),
        lax.all_gather(rope_keys, "sp", axis=1, tiled=True),
    )
    row_count = portion[0].shape[1]
    span_rows = math.gcd(row_count, token_count * max(1, 512 // token_count))

    def visit_rows(current):

        def visit_block(block_index, stats):
            row_start = block_index * span_rows
            key_plain, value_rows, rope_rows = expand_latent(portion, row_start, span_rows)
            return attend_block(stats, key_plain, value_rows, rope_rows, row_start)

        return lax.fori_loop(0, row_count // span_rows, visit_block, current)

    _, row_sum, weighted = lax.cond(
        jnp.int32(0) < query_start + token_count, visit_rows, keep_same, start_stats
    )
    latent_heads = (
        jnp.transpose(weighted / row_sum[..., None], (0, 2, 1, 3))
        .reshape(row_total, latent_count * VDIM)
        .astype(jnp.bfloat16)
    )
    heads_joined = jnp.concatenate([delta_heads, latent_heads], axis=1)
    out_rows = jnp.concatenate([delta_out, latent_out], axis=0)
    partial_value = jnp.dot(
        heads_joined,
        lax.all_gather(out_rows, ("sp", "fs"), axis=1, tiled=True),
        preferred_element_type=f32,
    )
    mixed_half = lax.psum_scatter(
        partial_value.astype(jnp.bfloat16), "tp", scatter_dimension=1, tiled=True
    ).astype(jnp.float32)
    squares = lax.psum(jnp.sum(mixed_half * mixed_half, axis=1), "tp")
    row_scale = lax.rsqrt(squares / D + NORM_EPS)
    result = mixed_half * row_scale[:, None] * post_gain
    return result.astype(jnp.bfloat16).reshape(seq_count, token_count, result.shape[1])


def pick(array, index):
    return lax.dynamic_index_in_dim(array, index, 0, False)


def dot32(left, right):
    return jnp.dot(left, right, preferred_element_type=jnp.float32)


def dot_t(left, right):
    return lax.dot_general(
        left, right, (((1,), (1,)), ((), ())), preferred_element_type=jnp.float32
    )


def two_parts(values):
    high = values.astype(jnp.bfloat16)
    return high, (values - high.astype(jnp.float32)).astype(jnp.bfloat16)


def fine_dot(left, right, product=dot32):
    left_high, left_low = two_parts(left)
    right_high, right_low = two_parts(right)
    return product(left_high, right_high) + (
        product(left_high, right_low) + product(left_low, right_high)
    )


def kernel_call(body, out_shapes, args, scratch=(), inside=(True, True), outside=0):
    space = pl.BlockSpec(memory_space=pltpu.VMEM)
    operand_space, result_space = (pltpu.VMEM if here else pltpu.HBM for here in inside)
    return pl.pallas_call(
        body,
        out_shape=jax.tree.map(lambda leaf: result_space(leaf.shape, leaf.dtype), out_shapes),
        in_specs=[space] * len(args),
        out_specs=jax.tree.map(lambda _: space, out_shapes),
        scratch_shapes=scratch,
        compiler_params=pltpu.CompilerParams(vmem_limit_bytes=16 * 1024 * 1024),
    )(
        *(
            pltpu.with_memory_space_constraint(arg, pltpu.HBM if i < outside else operand_space)
            for i, arg in enumerate(args)
        )
    )


def started(pairs, sems):
    copies = [pltpu.make_async_copy(*pair, sems.at[i]) for i, pair in enumerate(pairs)]
    for copy in copies:
        copy.start()
    return copies


def outgoing_weights(mixers, lats, sp_size):
    count = len(mixers)
    half = mixers[0].shape[0] // 2
    per_mixer = mixers[0].shape[1] // sp_size
    per_lat = [w.shape[1] // sp_size // 2 for w in lats]
    first_lat = count * per_mixer
    padded = first_lat + 128

    def body(*refs):
        out_ref, own_ref, *held_refs, sems = refs[count + 2 :]
        rows = pl.ds(pl.multiple_of(lax.axis_index("grp") * half, half), half)
        held = started([(ref.at[rows], to) for ref, to in zip(refs, held_refs)], sems)
        first = lax.axis_index("tp") == 0
        for copy in held:
            copy.wait()
        for s in range(sp_size):
            for k in range(count):
                out_ref[s, :, k * per_mixer : (k + 1) * per_mixer] = held_refs[k][
                    :, s * per_mixer : (s + 1) * per_mixer
                ]
            pieces = []
            for ref, per in zip(held_refs[count:], per_lat):
                pair = ref[:, 2 * s * per : 2 * (s + 1) * per]
                pieces.append(jnp.where(first, pair[:, :per], pair[:, per:]))
            pieces.append(jnp.zeros((half, 128 - sum(per_lat)), jnp.bfloat16))
            out_ref[s, :, first_lat:] = jnp.concatenate(pieces, axis=1)
        own_ref[...] = out_ref[lax.axis_index("sp")]

    space = pl.BlockSpec(memory_space=pltpu.VMEM)
    return pl.pallas_call(
        body,
        out_shape=(
            pltpu.HBM((sp_size, half, padded), jnp.bfloat16),
            pltpu.HBM((half, padded), jnp.bfloat16),
        ),
        in_specs=[pl.BlockSpec(memory_space=pl.ANY)] * (count + 2),
        out_specs=(space, space),
        scratch_shapes=(
            *(pltpu.VMEM((half, w.shape[1]), jnp.bfloat16) for w in (*mixers, *lats)),
            pltpu.SemaphoreType.DMA((count + 2,)),
        ),
        name="outgoing_weights",
        compiler_params=pltpu.CompilerParams(vmem_limit_bytes=16 * 1024 * 1024),
    )(*(pltpu.with_memory_space_constraint(w, pltpu.HBM) for w in (*mixers, *lats)))


def outgoing_tokens(tokens, gain, sp_size):
    rows, width = tokens.shape
    block = width // (sp_size * 4)

    def body(token_ref, gain_ref, mine_ref, their_ref):
        values = token_ref[...].astype(jnp.float32)
        normed = (values * rms_scale(values) * gain_ref[...]).astype(jnp.bfloat16)
        first = lax.axis_index("tp") == 0
        for f in range(2):
            for s in range(sp_size):
                begin = (s * 2 + f) * 2 * block
                low = normed[:, begin : begin + block]
                high = normed[:, begin + block : begin + 2 * block]
                at = (f * sp_size + s) * block
                mine_ref[:, at : at + block] = jnp.where(first, low, high)
                their_ref[:, at : at + block] = jnp.where(first, high, low)

    shape = jax.ShapeDtypeStruct((rows, width // 2), jnp.bfloat16)
    return kernel_call(body, (shape, shape), (tokens, gain))


def prepare(narrow, query_up, latent_up, sp_size):
    width = narrow[0].shape[1]
    block = width // (sp_size * 4)
    rank, query_width = query_up.shape
    per_query = query_width // sp_size
    heads = per_query // (NOPE + ROPE)
    per_latent = latent_up.shape[1] // sp_size

    def body(rope_ref, beta_ref, decay_ref, query_ref, latent_ref, narrow_ref, q_ref, kv_ref):
        place = lax.axis_index("sp")
        rows = jnp.concatenate([rope_ref[...], beta_ref[...], decay_ref[...]], axis=0)
        for s in range(sp_size):
            for f in range(2):
                for g in range(2):
                    begin = ((s * 2 + f) * 2 + g) * block
                    at = ((g * 2 + f) * sp_size + s) * block
                    narrow_ref[:, at : at + block] = rows[:, begin : begin + block]
        own = query_ref[:, :per_query]
        for s in range(1, sp_size):
            own = jnp.where(place == s, query_ref[:, s * per_query : (s + 1) * per_query], own)
        pairs = [
            (own[:, h * (NOPE + ROPE) :][:, :NOPE], own[:, h * (NOPE + ROPE) :][:, NOPE : NOPE + ROPE])
            for h in range(heads)
        ]
        parts = [plain for plain, _ in pairs] + [turn for _, turn in pairs]
        for _, turn in pairs:
            parts += [turn[:, ROPE // 2 :], turn[:, : ROPE // 2]]
        q_ref[...] = jnp.concatenate(parts, axis=1)
        kv_ref[...] = latent_ref[:, pl.ds(pl.multiple_of(place * per_latent, 128), per_latent)]

    bf16 = jnp.bfloat16
    return kernel_call(
        body,
        (
            jax.ShapeDtypeStruct((sum(n.shape[0] for n in narrow), width), bf16),
            jax.ShapeDtypeStruct((rank, heads * (NOPE + 2 * ROPE)), bf16),
            jax.ShapeDtypeStruct((latent_up.shape[0], per_latent), bf16),
        ),
        (*narrow, query_up, latent_up),
        inside=(False, True),
    )


def project(mine, theirs, block, peers, extra, sizes):
    seq_count, token_count, fine, q_cols, kv_cols = sizes
    sp_size = len(mine)
    chunk, part = mine[0].shape
    span = sp_size * token_count
    rows = seq_count * span
    piece, columns = peers[0].shape
    extra_width = extra.shape[0]
    q_stack, kv_stack = 128 // q_cols, 128 // kv_cols
    packed = rows // q_stack + rows // kv_stack
    copies = 1 + 3 * (sp_size + 1) + 2 * sp_size

    def body(*refs):
        mine_refs, refs = refs[:sp_size], refs[sp_size:]
        their_refs, refs = refs[:sp_size], refs[sp_size:]
        block_ref, refs = refs[0], refs[1:]
        peer_refs, refs = refs[:9], refs[9:]
        extra_ref, fine_ref, pack_ref, ext_ref, lat_ref, weight_ref, token_ref, sems = refs
        place, fs_at = lax.axis_index("sp"), lax.axis_index("fs")
        tp_at, grp_at = lax.axis_index("tp"), lax.axis_index("grp")
        step = piece // 2

        def rows_at(same_grp, same_fs, source, first, number):
            grp_from = grp_at if same_grp else 1 - grp_at
            block_from = (grp_from * 2 + (fs_at if same_fs else 1 - fs_at)) * sp_size + source
            return weight_ref.at[pl.ds(pl.multiple_of(block_from * piece + first, step), number)]

        moves = [(block_ref, rows_at(True, True, 0, 0, sp_size * piece))]
        half_rows = (sp_size - 1) * step
        for k, flips in enumerate(((True, False), (False, True), (False, False))):
            own_ref, low_ref, high_ref = peer_refs[3 * k : 3 * k + 3]
            moves.append((own_ref, rows_at(*flips, place, 0, piece)))
            for o in range(1, sp_size):
                source = lax.rem(place + o, sp_size)
                begin, end = (o - 1) * piece, o * piece
                cut = min(max(begin, half_rows), end)
                if cut > begin:
                    from_ref = low_ref.at[begin:cut]
                    moves.append((from_ref, rows_at(*flips, source, 0, cut - begin)))
                if end > cut:
                    from_ref = high_ref.at[cut - half_rows : end - half_rows]
                    moves.append((from_ref, rows_at(*flips, source, cut - begin, end - cut)))
        for o in range(sp_size):
            of = pl.ds(o * chunk, chunk)
            at = pl.ds(pl.multiple_of(tp_at * part, part), part)
            moves.append((mine_refs[o], token_ref.at[of, at]))
            at = pl.ds(pl.multiple_of((1 - tp_at) * part, part), part)
            moves.append((their_refs[o], token_ref.at[of, at]))
        assert len(moves) <= copies
        moves = started(moves, sems)
        for copy in moves[: -2 * sp_size]:
            copy.wait()
        for o in range(sp_size):
            for copy in moves[len(moves) - 2 * (sp_size - o) :][:2]:
                copy.wait()
            lhs = token_ref[o * chunk : (o + 1) * chunk, :]
            value = dot32(lhs, weight_ref[...]).astype(jnp.bfloat16)
            outer = dot_t(lhs, extra_ref[...])
            source = lax.bitwise_xor(place, o)
            for n in range(seq_count):
                of = slice(n * token_count, (n + 1) * token_count)
                at = pl.ds(pl.multiple_of(source * token_count, token_count), token_count)
                fine_ref[n, at, :] = value[of, :fine]
                ext_ref[n, at, :] = outer[of]
                at = pl.ds(
                    pl.multiple_of(n * span + source * token_count, token_count), token_count
                )
                lat_ref[at, :] = value[of, fine : fine + 128]
        for start, first, width, count in (
            (0, 0, q_cols, q_stack),
            (rows // q_stack, q_cols, kv_cols, kv_stack),
        ):
            group = rows // count
            joined = jnp.concatenate(
                [
                    lat_ref[k * group : (k + 1) * group, first : first + width]
                    for k in range(count)
                ],
                axis=1,
            )
            for j in range(sp_size):
                pack_ref[j, start : start + group, :] = joined

    space = pl.BlockSpec(memory_space=pltpu.VMEM)
    moved = tuple(
        pltpu.with_memory_space_constraint(array, pltpu.HBM)
        for array in (*mine, *theirs, block, *peers)
    )
    return pl.pallas_call(
        body,
        out_shape=(
            pltpu.VMEM((seq_count, span, fine), jnp.bfloat16),
            pltpu.VMEM((sp_size, packed, 128), jnp.bfloat16),
            pltpu.VMEM((seq_count, span, extra_width), jnp.float32),
        ),
        in_specs=[pl.BlockSpec(memory_space=pl.ANY)] * len(moved) + [space],
        out_specs=(space,) * 3,
        scratch_shapes=(
            pltpu.VMEM((rows, 128), jnp.bfloat16),
            pltpu.VMEM((2 * part, columns), jnp.bfloat16),
            pltpu.VMEM((rows, 2 * part), jnp.bfloat16),
            pltpu.SemaphoreType.DMA((copies,)),
        ),
        name="project",
        compiler_params=pltpu.CompilerParams(vmem_limit_bytes=16 * 1024 * 1024),
    )(*moved, pltpu.with_memory_space_constraint(extra, pltpu.VMEM))


def send_by_pair(out_refs, pieces, sp_size):
    place = lax.axis_index("sp")
    for step, out_ref in enumerate(out_refs):
        second = lax.rem(place + step, sp_size) >= sp_size // 2
        for n, (low, high) in enumerate(pieces):
            rows = low.shape[0]
            out_ref[n * rows : (n + 1) * rows, :] = jnp.where(second, high, low)


def lower_inverses(lowers, base):
    size = lowers[0].shape[0]
    row = lax.broadcasted_iota(jnp.int32, (size, size), 0)
    col = lax.broadcasted_iota(jnp.int32, (size, size), 1)
    unit = jnp.where(row == col, 1.0, 0.0)
    powers = [jnp.where(row // base == col // base, low, 0.0) for low in lowers]
    inverses = [unit - p for p in powers]
    reach = 2
    while reach < base:
        powers = [fine_dot(p, p) for p in powers]
        inverses = [i + fine_dot(i, p) for i, p in zip(inverses, powers)]
        reach *= 2
    block = base
    while block < size:
        joint = (row // (2 * block) == col // (2 * block)) & (row // block != col // block)
        moved = [fine_dot(i, jnp.where(joint, low, 0.0)) for i, low in zip(inverses, lowers)]
        inverses = [i - fine_dot(m, i) for i, m in zip(inverses, moved)]
        block *= 2
    return inverses


def delta_mix(fine, ext, gains, gain_at, gates, gate_at, heads, sp_size):
    seq_count, span, _ = fine.shape
    tile = math.gcd(span, 128)
    tiles = span // tile

    def terms(raw_query, raw_key, raw_value, beta_pre, decay_pre, rate):
        query = unit_rows(jax.nn.silu(raw_query)) * HEAD ** (-0.5)
        key = unit_rows(jax.nn.silu(raw_key))
        value = jax.nn.silu(raw_value)
        beta = jax.nn.sigmoid(beta_pre)
        log_decay = -rate * jax.nn.softplus(decay_pre)
        row = lax.broadcasted_iota(jnp.int32, (span, span), 0)
        col = lax.broadcasted_iota(jnp.int32, (span, span), 1)
        as_row = jnp.sum(jnp.where(row == col, log_decay, 0.0), axis=0, keepdims=True)
        gate = jnp.sum(jnp.where(row >= col, as_row, 0.0), axis=1, keepdims=True)
        gate_row = jnp.sum(jnp.where(row == col, gate, 0.0), axis=0, keepdims=True)
        decay = jnp.where(row >= col, jnp.exp(jnp.where(row >= col, gate - gate_row, 0.0)), 0.0)
        lower = fine_dot(key * beta, key, dot_t) * jnp.where(row > col, decay, 0.0)
        scores = fine_dot(query, key, dot_t) * decay
        return lower, scores, value * beta

    def body(fine_ref, ext_ref, gain_ref, *out_refs):
        gain_row = gain_ref[:, gain_at : gain_at + HEAD]
        rate_row = gain_ref[:, gain_at + HEAD : gain_at + 2 * HEAD]
        first_head = (lax.axis_index("tp") * sp_size + lax.axis_index("sp")) * heads
        lane = lax.broadcasted_iota(jnp.int32, (span, ext.shape[2]), 1)
        rate_lane = lax.broadcasted_iota(jnp.int32, (1, HEAD), 1)
        chains = []
        for n in range(seq_count):
            for h in range(heads):
                raw = [
                    fine_ref[n, :, (k * heads + h) * HEAD : (k * heads + h + 1) * HEAD].astype(
                        jnp.float32
                    )
                    for k in range(3)
                ]
                head = first_head + h
                outer = ext_ref[n]
                beta_pre, decay_pre = (
                    jnp.sum(
                        jnp.where(lane == gate_at + k * gates + head, outer, 0.0),
                        axis=1,
                        keepdims=True,
                    )
                    for k in range(2)
                )
                rate = jnp.sum(
                    jnp.where(rate_lane == head, rate_row, 0.0), axis=1, keepdims=True
                )
                chains.append(terms(*raw, beta_pre, decay_pre, rate))
        cuts = [slice(j * tile, (j + 1) * tile) for j in range(tiles)]
        inverses = lower_inverses([c[0][cut, cut] for c in chains for cut in cuts], 8)
        solved = [[] for _ in chains]
        for j, cut in enumerate(cuts):
            for i, (lower, _, wanted) in enumerate(chains):
                rest = wanted[cut]
                if j:
                    rest = rest - fine_dot(
                        lower[cut, : j * tile], jnp.concatenate(solved[i], axis=0)
                    )
                solved[i].append(fine_dot(inverses[i * tiles + j], rest))
        pieces = []
        for i, (_, scores, _) in enumerate(chains):
            out = fine_dot(scores, jnp.concatenate(solved[i], axis=0))
            out = (out * rms_scale(out) * gain_row).astype(jnp.bfloat16)
            pieces.append((out[: span // 2], out[span // 2 :]))
        for h in range(heads):
            columns = slice(h * HEAD, (h + 1) * HEAD)
            views = [ref.at[:, columns] for ref in out_refs] if heads > 1 else out_refs
            send_by_pair(views, pieces[h::heads], sp_size)

    shape = jax.ShapeDtypeStruct((seq_count * span // 2, heads * HEAD), jnp.bfloat16)
    return kernel_call(body, (shape,) * sp_size, (fine, ext, gains), inside=(True, False))


def latent_mix(mine, theirs, ext, tables, gains, ups, q_cols, kv_cols, heads):
    sp_size = mine.shape[0]
    seq_count, span, _ = ext.shape
    rows = seq_count * span
    q_rank, kv_rank = ups[0].shape[0], ups[1].shape[0]
    scale = (NOPE + ROPE) ** (-0.5)

    def unpack(value, n, base, width):
        group = rows * width // 128
        pieces = []
        for k in range(128 // width):
            if n * span < (k + 1) * group and k * group < (n + 1) * span:
                low = max(n * span - k * group, 0)
                high = min((n + 1) * span - k * group, group)
                pieces.append(
                    value[base + low : base + high, k * width : (k + 1) * width]
                )
        return jnp.concatenate(pieces, axis=0) if len(pieces) > 1 else pieces[0]

    def body(mine_ref, their_ref, ext_ref, cos_ref, sin_ref, *refs):
        gain_ref, qup_ref, kup_ref, *out_refs = refs
        q_gain = gain_ref[:, :q_rank]
        kv_gain = gain_ref[:, q_rank : q_rank + kv_rank]
        first = lax.axis_index("tp") == 0
        row = lax.broadcasted_iota(jnp.int32, (span, span), 0) // BLOCK
        col = lax.broadcasted_iota(jnp.int32, (span, span), 1) // BLOCK
        allowed = col <= row
        cosine, sine = cos_ref[...], sin_ref[...]
        pairs = []
        for s in range(sp_size):
            own, other = mine_ref[s], their_ref[s]
            pairs += [jnp.where(first, own, other), jnp.where(first, other, own)]
        joins = []
        for n in range(seq_count):
            q_parts = [unpack(p, n, 0, q_cols) for p in pairs]
            kv_parts = [unpack(p, n, rows * q_cols // 128, kv_cols) for p in pairs]
            q_lat = jnp.concatenate(q_parts, axis=1).astype(jnp.float32)
            kv_lat = jnp.concatenate(kv_parts, axis=1).astype(jnp.float32)
            q_norm = (q_lat * rms_scale(q_lat) * q_gain).astype(jnp.bfloat16)
            kv_norm = (kv_lat * rms_scale(kv_lat) * kv_gain).astype(jnp.bfloat16)
            q_all = dot32(q_norm, qup_ref[...]).astype(jnp.bfloat16)
            kv_all = dot32(kv_norm, kup_ref[...]).astype(jnp.bfloat16)
            plain_width, turn_width = heads * NOPE, heads * ROPE
            plain = q_all[:, :plain_width]
            turn = q_all[:, plain_width : plain_width + turn_width].astype(jnp.float32)
            swapped = q_all[:, plain_width + turn_width :].astype(jnp.float32)
            turned = (turn * cosine + swapped * sine).astype(jnp.bfloat16)
            raw = ext_ref[n, :, :ROPE].astype(jnp.bfloat16).astype(jnp.float32)
            back = jnp.concatenate([raw[:, ROPE // 2 :], raw[:, : ROPE // 2]], axis=1)
            key_turn = (raw * cosine[:, :ROPE] + back * sine[:, :ROPE]).astype(jnp.bfloat16)
            results = []
            for h in range(heads):
                key_plain = kv_all[:, h * (NOPE + VDIM) : h * (NOPE + VDIM) + NOPE]
                values = kv_all[:, h * (NOPE + VDIM) + NOPE : (h + 1) * (NOPE + VDIM)]
                logits = (
                    dot_t(plain[:, h * NOPE : (h + 1) * NOPE], key_plain)
                    + dot_t(turned[:, h * ROPE : (h + 1) * ROPE], key_turn)
                ) * scale
                logits = jnp.where(allowed, logits, -jnp.inf)
                peak = jnp.max(logits, axis=-1, keepdims=True)
                weights = jnp.exp(logits - peak)
                total = jnp.sum(weights, axis=-1, keepdims=True)
                results.append(dot32(weights.astype(jnp.bfloat16), values) / total)
            joined = jnp.concatenate(results, axis=1).astype(jnp.bfloat16)
            joins.append((joined[: span // 2], joined[span // 2 :]))
        send_by_pair(out_refs, joins, sp_size)

    shape = jax.ShapeDtypeStruct((rows // 2, heads * VDIM), jnp.bfloat16)
    return kernel_call(
        body, (shape,) * sp_size, (mine, theirs, ext, *tables, gains, *ups), outside=2
    )


def output_partial(delta_all, latent_all, near, near_fs, far, sizes):
    seq_count, token_count = sizes
    sp_size = len(delta_all)
    rows, d_width = delta_all[0].shape
    l_width = latent_all[0].shape[1]
    total, columns = near.shape
    half = total // 2
    per_half = sp_size // 2

    def body(*refs):
        d_refs, refs = refs[:sp_size], refs[sp_size:]
        l_refs, refs = refs[:sp_size], refs[sp_size:]
        near_ref, near_fs_ref, *far_refs, keep_ref, pass_ref, lhs_ref = refs
        place, fs_at = lax.axis_index("sp"), lax.axis_index("fs")
        grp_at = lax.axis_index("grp")
        for o in range(sp_size):
            source = lax.rem(place + o, sp_size)
            base = (source // per_half) * half
            within = lax.rem(source, per_half)
            at = pl.multiple_of(base + within * d_width, 128)
            lhs_ref[:, pl.ds(at, d_width)] = d_refs[o][...]
            at = pl.multiple_of(base + per_half * d_width + within * l_width, 128)
            lhs_ref[:, pl.ds(at, l_width)] = l_refs[o][...]
        lhs = lhs_ref[...]
        own = lhs_ref[:, pl.ds(pl.multiple_of(grp_at * half, half), half)]
        other = lhs_ref[:, pl.ds(pl.multiple_of((1 - grp_at) * half, half), half)]
        close = (
            dot32(lhs, near_ref[...]).astype(jnp.bfloat16),
            dot32(lhs, near_fs_ref[...]).astype(jnp.bfloat16),
        )
        away = tuple(
            (dot32(own, far_refs[k][...]) + dot32(other, far_refs[k + 1][...])).astype(jnp.bfloat16)
            for k in (0, 2)
        )
        straight = place // per_half == lax.axis_index("tp")
        for k in range(2):
            begin = (1 - fs_at) if k else fs_at
            at = pl.ds(pl.multiple_of(begin * columns, columns), columns)
            keep = jnp.where(straight, close[k], away[k])
            onward = jnp.where(straight, away[k], close[k])
            pair_rows = 2 * token_count
            for n in range(seq_count):
                for p in range(2):
                    of = slice(n * pair_rows + p * token_count, n * pair_rows + (p + 1) * token_count)
                    to = slice(n * token_count, (n + 1) * token_count)
                    keep_ref[p, to, at] = keep[of]
                    pass_ref[p, to, at] = onward[of]

    shape = jax.ShapeDtypeStruct((2, rows // 2, 2 * columns), jnp.bfloat16)
    return kernel_call(
        body,
        (shape, shape),
        (*delta_all, *latent_all, near, near_fs, *far),
        scratch=(pltpu.VMEM((rows, total), jnp.bfloat16),),
    )


def whole_tables(length, repeats):
    frequency = ROPE_THETA ** (-np.arange(0, ROPE, 2, dtype=np.float32) / np.float32(ROPE))
    angles = np.arange(length, dtype=np.float32)[:, None] * frequency[None, :].astype(np.float32)
    cosine, sine = np.cos(angles), np.sin(angles)
    return tuple(
        jnp.asarray(np.tile(np.concatenate(pair, axis=1), (1, repeats)), jnp.float32)
        for pair in ((cosine, cosine), (-sine, sine))
    )


def whole_sequences(
    tokens,
    pre_gain,
    query_weight,
    key_weight,
    value_weight,
    beta_weight,
    decay_weight,
    decay_rate,
    delta_gain,
    query_down,
    latent_down,
    rope_weight,
    query_gain,
    latent_gain,
    query_up,
    latent_up,
    delta_out,
    latent_out,
    post_gain,
):
    f32, bf16 = jnp.float32, jnp.bfloat16
    sp_size, tp_size = lax.axis_size("sp"), lax.axis_size("tp")
    place, grp_at = lax.axis_index("sp"), lax.axis_index("grp")
    seq_count, token_count, width = tokens.shape
    rows = seq_count * token_count
    heads = query_weight.shape[1] // HEAD // sp_size
    shares = sp_size * tp_size
    q_cols, kv_cols = query_down.shape[1] // shares, latent_down.shape[1] // shares

    def exchange(values, axis):
        return lax.all_to_all(values, axis, 0, 0, tiled=True)

    def swap(values, axis):
        return lax.ppermute(values, axis, [(0, 1), (1, 0)])

    def along(values, step):
        return lax.ppermute(values, "sp", [(i, (i + step) % sp_size) for i in range(sp_size)])

    def from_sp(sends):
        return [sends[0]] + [along(sends[step], step) for step in range(sp_size - 1, 0, -1)]

    outgoing, own_piece = outgoing_weights(
        (query_weight, key_weight, value_weight), (query_down, latent_down), sp_size
    )
    block = exchange(outgoing, "sp")
    token_rows, outgoing = lax.optimization_barrier((tokens.reshape(rows, width), outgoing))

    own_half, other_half = outgoing_tokens(token_rows, pre_gain[None, :], sp_size)

    def beside(values):
        return lax.ppermute(values, "sp", [(i, i ^ 1) for i in range(sp_size)])

    far_half = along(own_half, sp_size // 2)
    mine = [own_half, beside(own_half), far_half, beside(far_half)]
    theirs = [other_half] + [swap(piece, "tp") for piece in mine[1:]]

    quarter = delta_out.shape[0] // 2
    near = jnp.concatenate(
        [w[k * quarter : (k + 1) * quarter] for k in range(2) for w in (delta_out, latent_out)]
    )
    near_fs = swap(near, "fs")

    own_grp, own_fs = swap(own_piece, "grp"), swap(own_piece, "fs")
    own_corner = swap(own_grp, "fs")
    rest = lax.dynamic_slice_in_dim(jnp.concatenate([block, block]), place + 1, sp_size - 1, 0)
    rest = rest.reshape(-1, rest.shape[2])
    block = block.reshape(-1, block.shape[2])
    middle = rest.shape[0] // 2
    low, high = rest[:middle], rest[middle:]
    low_grp, high_fs = swap(low, "grp"), swap(high, "fs")
    high_grp, low_fs = swap(high, "grp"), swap(low, "fs")
    corner = swap(low_grp, "fs"), swap(high_fs, "grp")
    peers = (own_fs, low_fs, high_fs, own_grp, low_grp, high_grp, own_corner, *corner)

    far_own = lax.dynamic_slice_in_dim(near, grp_at * 2 * quarter, 2 * quarter, 0)
    far_own = along(far_own, sp_size // 2)
    far_other = swap(far_own, "grp")
    far = (far_own, far_other, swap(far_own, "fs"))
    far = (*far, swap(far_other, "fs"))

    gate_at = rope_weight.shape[1]
    latent_heads = query_up.shape[1] // (NOPE + ROPE) // sp_size
    extra, q_up, kv_up = prepare(
        (rope_weight.T, beta_weight.T, decay_weight.T), query_up, latent_up, sp_size
    )
    tables = whole_tables(sp_size * token_count, latent_heads)
    rates = jnp.pad(decay_rate, (0, HEAD - decay_rate.shape[0]))
    latent_gains = jnp.concatenate([query_gain, latent_gain])[None, :]
    gains = jnp.concatenate([delta_gain, rates, post_gain])[None, :]
    mine[1], gains, latent_gains = lax.optimization_barrier((mine[1], gains, latent_gains))

    fine, lat, ext = project(
        mine,
        theirs,
        block,
        peers,
        extra,
        (seq_count, token_count, 3 * heads * HEAD, q_cols, kv_cols),
    )
    lat_mine = exchange(lat, "sp")
    delta_sends = delta_mix(
        fine, ext, gains, 0, decay_rate.shape[0], gate_at, heads, sp_size
    )
    lat_mine, _ = lax.optimization_barrier((lat_mine, delta_sends))
    lat_theirs = swap(lat_mine, "tp")
    delta_all = from_sp(delta_sends)
    latent_sends = latent_mix(
        lat_mine,
        lat_theirs,
        ext,
        tables,
        latent_gains,
        (q_up, kv_up),
        q_cols,
        kv_cols,
        latent_heads,
    )
    latent_all = from_sp(latent_sends)

    keep, onward = output_partial(
        delta_all, latent_all, near, near_fs, far, (seq_count, token_count)
    )
    mixed = (keep.astype(f32) + swap(onward, "tp").astype(f32)).astype(bf16)
    side = lax.rem(place, 2)

    def across(values):
        return lax.ppermute(pick(values, 1 - side), "sp", [(i, i ^ 1) for i in range(sp_size)])

    there = across(mixed)
    squares = jnp.sum(mixed.astype(f32) * mixed.astype(f32), axis=2)
    squares = squares + swap(squares, "tp")
    squares = (pick(squares, side) + across(squares))[:, None]
    here, there = pick(mixed, side).astype(f32), there.astype(f32)
    final = jnp.concatenate(
        [jnp.where(side == 0, here, there), jnp.where(side == 0, there, here)], axis=1
    )
    result = final * lax.rsqrt(squares / D + NORM_EPS) * gains[:, 2 * HEAD :]
    return result.astype(bf16).reshape(seq_count, token_count, final.shape[1])


def fits_whole(mesh):
    shape = mesh.shape
    return all(shape[name] == 2 for name in ("grp", "fs", "tp")) and shape["sp"] == 4


def solution(mesh):
    def chosen(*args):
        head_count = args[2].shape[1] // HEAD
        latent_count = args[14].shape[1] // (NOPE + ROPE)
        sp_size = mesh.shape["sp"]
        whole = fits_whole(mesh) and head_count % sp_size == 0 and latent_count % sp_size == 0
        return (whole_sequences if whole else local)(*args)

    return jax.shard_map(
        chosen,
        mesh=mesh,
        in_specs=(
            P(("grp", "fs"), "sp", None),
            P(),
            P(("sp", "fs"), "tp"),
            P(("sp", "fs"), "tp"),
            P(("sp", "fs"), "tp"),
            P(),
            P(),
            P(),
            P(),
            P(("sp", "fs"), None),
            P(("sp", "fs"), None),
            P(),
            P(),
            P(),
            P(None, "tp"),
            P(None, "tp"),
            P("tp", ("sp", "fs")),
            P("tp", ("sp", "fs")),
            P("tp"),
        ),
        out_specs=P(("grp", "fs"), "sp", "tp"),
        check_vma=False,
    )
```

profile of v0, /device:TPU:0, one launch (start us, length us, event | category | flops | bytes accessed | tf_op | source)
XLA Modules:
  0.0 126.8 jit_solution(8268148142493090672)
XLA Ops:
  0.0 2.3 %outgoing_weights.1 = (bf16[4,128,512]{2,1,0:T(8,128)(2,1)}, bf16[128,512]{1,0:T(8,128)(2,1)}) custom-call(bf16[256,512]{1,0:T(8,128)(2,1)} %refs_0_.1, bf16[256,512]{1,0:T(8,128)(2,1)} %refs_1_.1, bf16[256,512]{1,0:T(8,128)(2,1)} %refs_2_.1, bf16[256,512]{1,0:T(8,128)(2,1)} %refs_3_.1, bf16[256,256]{1,0:T(8,128)(2,1)} %refs_4_.1), custom_call_target="tpu_custom_call" | custom-call | tf_op jit(solution)/shard_map/outgoing_weights/pallas_call | solution.py:422
  2.3 6.5 %all-to-all-start = ((bf16[4,128,512]{2,1,0:T(8,128)(2,1)}), bf16[4,128,512]{2,1,0:T(8,128)(2,1)S(1)}, u32[]{:S(2)}, u32[]{:S(2)}) async-start(bf16[4,128,512]{2,1,0:T(8,128)(2,1)} %get-tuple-element.30), calls=%async_computation | async-start | bytes 1048576 | tf_op jit(solution)/shard_map/all_to_all | solution.py:887
  9.2 3.0 %collective-permute-start.1 = (bf16[128,1024]{1,0:T(8,128)(2,1)S(1)}, bf16[128,1024]{1,0:T(8,128)(2,1)S(1)}, u32[]{:S(2)}, u32[]{:S(2)}) collective-permute-start(bf16[128,1024]{1,0:T(8,128)(2,1)S(1)} %get-tuple-element.32.refs_0_), channel_id=1, source_target_pairs={{0,8},{4,12},{8,0},{12,4},{1,9},{5,13},{9,1},{13,5},{2,10},{6,14},... | collective-permute-start | bytes 786440 | tf_op jit(solution)/shard_map/ppermute | solution.py:893
  12.2 1.5 %collective-permute-start = (bf16[128,1024]{1,0:T(8,128)(2,1)S(1)}, bf16[128,1024]{1,0:T(8,128)(2,1)S(1)}, u32[]{:S(2)}, u32[]{:S(2)}) collective-permute-start(bf16[128,1024]{1,0:T(8,128)(2,1)S(1)} %get-tuple-element.32.refs_0_), channel_id=1, source_target_pairs={{0,4},{4,0},{8,12},{12,8},{1,5},{5,1},{9,13},{13,9},{2,6},{6,2},{1... | collective-permute-start | bytes 786440 | tf_op jit(solution)/shard_map/ppermute | solution.py:907
  13.6 1.5 %collective-permute-start.9 = (bf16[128,512]{1,0:T(8,128)(2,1)S(1)}, bf16[128,512]{1,0:T(8,128)(2,1)S(1)}, u32[]{:S(2)}, u32[]{:S(2)}) collective-permute-start(bf16[128,512]{1,0:T(8,128)(2,1)S(1)} %copy-done.32), channel_id=1, source_target_pairs={{0,16},{16,0},{1,17},{17,1},{2,18},{18,2},{3,19},{19,3},{4,20},{20... | collective-permute-start | bytes 393224 | tf_op jit(solution)/shard_map/ppermute | solution.py:890
  15.1 1.5 %collective-permute-start.6 = (bf16[128,512]{1,0:T(8,128)(2,1)S(1)}, bf16[128,512]{1,0:T(8,128)(2,1)S(1)}, u32[]{:S(2)}, u32[]{:S(2)}) collective-permute-start(bf16[128,512]{1,0:T(8,128)(2,1)S(1)} %copy-done.32), channel_id=1, source_target_pairs={{0,2},{2,0},{1,3},{3,1},{4,6},{6,4},{5,7},{7,5},{8,10},{10,8},{9,1... | collective-permute-start | bytes 393224 | tf_op jit(solution)/shard_map/ppermute | solution.py:890
  16.6 2.0 %collective-permute-done.9.refs_12_ = bf16[128,512]{1,0:T(8,128)(2,1)S(1)} collective-permute-done((bf16[128,512]{1,0:T(8,128)(2,1)S(1)}, bf16[128,512]{1,0:T(8,128)(2,1)S(1)}, u32[]{:S(2)}, u32[]{:S(2)}) %collective-permute-start.9) | collective-permute-done | bytes 131104 | tf_op jit(solution)/shard_map/ppermute | solution.py:890
  18.6 1.5 %collective-permute-start.12 = (bf16[128,512]{1,0:T(8,128)(2,1)S(1)}, bf16[128,512]{1,0:T(8,128)(2,1)S(1)}, u32[]{:S(2)}, u32[]{:S(2)}) collective-permute-start(bf16[128,512]{1,0:T(8,128)(2,1)S(1)} %collective-permute-done.9.refs_12_), channel_id=1, source_target_pairs={{0,2},{2,0},{1,3},{3,1},{4,6},{6,4},{5,7},{7,5},{8,10},{10,8},{9,1... | collective-permute-start | bytes 393224 | tf_op jit(solution)/shard_map/ppermute | solution.py:890
  20.1 14.4 %collective-permute-done.1.refs_2_ = bf16[128,1024]{1,0:T(8,128)(2,1)S(1)} collective-permute-done((bf16[128,1024]{1,0:T(8,128)(2,1)S(1)}, bf16[128,1024]{1,0:T(8,128)(2,1)S(1)}, u32[]{:S(2)}, u32[]{:S(2)}) %collective-permute-start.1) | collective-permute-done | bytes 262176 | tf_op jit(solution)/shard_map/ppermute | solution.py:893
  34.6 0.5 collective-permute-start.3
  35.2 0.8 fusion.9
  36.1 1.6 %collective-permute-start.10 = (bf16[192,512]{1,0:T(8,128)(2,1)}, bf16[192,512]{1,0:T(8,128)(2,1)S(1)}, u32[]{:S(2)}, u32[]{:S(2)}) collective-permute-start(bf16[192,512]{1,0:T(8,128)(2,1)} %get-tuple-element.60), channel_id=1, source_target_pairs={{0,16},{16,0},{1,17},{17,1},{2,18},{18,2},{3,19},{19,3},{4,20},{20... | collective-permute-start | bytes 589832 | tf_op jit(solution)/shard_map/ppermute | solution.py:890
  37.7 1.6 %collective-permute-start.8 = (bf16[192,512]{1,0:T(8,128)(2,1)}, bf16[192,512]{1,0:T(8,128)(2,1)}, u32[]{:S(2)}, u32[]{:S(2)}) collective-permute-start(bf16[192,512]{1,0:T(8,128)(2,1)} %get-tuple-element.59), channel_id=1, source_target_pairs={{0,2},{2,0},{1,3},{3,1},{4,6},{6,4},{5,7},{7,5},{8,10},{10,8},{9,1... | collective-permute-start | bytes 589832 | tf_op jit(solution)/shard_map/ppermute | solution.py:890
  39.2 2.6 %collective-permute-done.2.refs_3_ = bf16[128,1024]{1,0:T(8,128)(2,1)S(1)} collective-permute-done((bf16[128,1024]{1,0:T(8,128)(2,1)S(1)}, bf16[128,1024]{1,0:T(8,128)(2,1)S(1)}, u32[]{:S(2)}, u32[]{:S(2)}) %collective-permute-start.2) | collective-permute-done | bytes 262176 | tf_op jit(solution)/shard_map/ppermute | solution.py:907
  42.0 2.0 %shard_map.200 = (bf16[48,2048]{1,0:T(8,128)(2,1)S(1)}, bf16[512,256]{1,0:T(8,128)(2,1)S(1)}, bf16[256,256]{1,0:T(8,128)(2,1)S(1)}) custom-call(bf16[32,2048]{1,0:T(8,128)(2,1)} %bitcast.33, bf16[8,2048]{1,0:T(8,128)(2,1)} %bitcast.34, bf16[8,2048]{1,0:T(8,128)(2,1)} %bitcast.35, bf16[512,768]{1,0:T(8,128)(2,1)} %query_ref.1, bf16[256,1024]{1,0:T(8,128)(2,1)} %latent_ref.1), custom_call_target="tpu_custom_call" | custom-call | tf_op jit(solution)/shard_map/pallas_call | solution.py:371
  44.0 1.6 %collective-permute-start.11 = (bf16[192,512]{1,0:T(8,128)(2,1)}, bf16[192,512]{1,0:T(8,128)(2,1)S(1)}, u32[]{:S(2)}, u32[]{:S(2)}) collective-permute-start(bf16[192,512]{1,0:T(8,128)(2,1)} %get-tuple-element.59), channel_id=1, source_target_pairs={{0,16},{16,0},{1,17},{17,1},{2,18},{18,2},{3,19},{19,3},{4,20},{20... | collective-permute-start | bytes 589832 | tf_op jit(solution)/shard_map/ppermute | solution.py:890
  45.6 1.5 %collective-permute-start.7 = (bf16[192,512]{1,0:T(8,128)(2,1)}, bf16[192,512]{1,0:T(8,128)(2,1)S(1)}, u32[]{:S(2)}, u32[]{:S(2)}) collective-permute-start(bf16[192,512]{1,0:T(8,128)(2,1)} %get-tuple-element.60), channel_id=1, source_target_pairs={{0,2},{2,0},{1,3},{3,1},{4,6},{6,4},{5,7},{7,5},{8,10},{10,8},{9,1... | collective-permute-start | bytes 589832 | tf_op jit(solution)/shard_map/ppermute | solution.py:890
  47.1 0.5 collective-permute-start.13
  47.6 0.5 collective-permute-start.14
  48.2 3.8 %collective-permute-done.11.refs_14_ = bf16[192,512]{1,0:T(8,128)(2,1)S(1)} collective-permute-done((bf16[192,512]{1,0:T(8,128)(2,1)}, bf16[192,512]{1,0:T(8,128)(2,1)S(1)}, u32[]{:S(2)}, u32[]{:S(2)}) %collective-permute-start.11) | collective-permute-done | bytes 196640 | tf_op jit(solution)/shard_map/ppermute | solution.py:890
  52.0 1.5 %collective-permute-done.7.refs_10_ = bf16[192,512]{1,0:T(8,128)(2,1)S(1)} collective-permute-done((bf16[192,512]{1,0:T(8,128)(2,1)}, bf16[192,512]{1,0:T(8,128)(2,1)S(1)}, u32[]{:S(2)}, u32[]{:S(2)}) %collective-permute-start.7) | collective-permute-done | bytes 196640 | tf_op jit(solution)/shard_map/ppermute | solution.py:890
  53.6 3.5 %collective-permute-done.13.refs_16_ = bf16[192,512]{1,0:T(8,128)(2,1)S(1)} collective-permute-done((bf16[192,512]{1,0:T(8,128)(2,1)S(1)}, bf16[192,512]{1,0:T(8,128)(2,1)S(1)}, u32[]{:S(2)}, u32[]{:S(2)}) %collective-permute-start.13) | collective-permute-done | bytes 196640 | tf_op jit(solution)/shard_map/ppermute | solution.py:890
  57.0 0.7 copy-done.22
  57.8 5.3 %project.1 = (bf16[2,256,384]{2,1,0:T(8,128)(2,1)S(1)}, bf16[4,384,128]{2,1,0:T(8,128)(2,1)}, f32[2,256,48]{2,1,0:T(8,128)S(1)}) custom-call(bf16[128,1024]{1,0:T(8,128)(2,1)} %copy-done.1, bf16[128,1024]{1,0:T(8,128)(2,1)} %copy-done.12, bf16[128,1024]{1,0:T(8,128)(2,1)} %copy-done.11, bf16[128,1024]{1,0:T(8,128)(2,1)} %copy-done.13, ...), custom_call_target="tpu_custom_call" | custom-call | tf_op jit(solution)/shard_map/project/pallas_call | solution.py:591
  63.1 3.5 %all-to-all-start.1 = ((bf16[4,384,128]{2,1,0:T(8,128)(2,1)}), bf16[4,384,128]{2,1,0:T(8,128)(2,1)S(1)}, u32[]{:S(2)}, u32[]{:S(2)}) async-start(bf16[4,384,128]{2,1,0:T(8,128)(2,1)} %get-tuple-element.44), calls=%async_computation.1 | async-start | bytes 786432 | tf_op jit(solution)/shard_map/all_to_all | solution.py:887
  66.7 2.9 %collective-permute-start.23 = (bf16[512,256]{1,0:T(8,128)(2,1)S(1)}, bf16[512,256]{1,0:T(8,128)(2,1)S(1)}, u32[]{:S(2)}, u32[]{:S(2)}) collective-permute-start(bf16[512,256]{1,0:T(8,128)(2,1)S(1)} %constant_dynamic-slice_fusion.2), channel_id=1, source_target_pairs={{0,8},{4,12},{8,0},{12,4},{1,9},{5,13},{9,1},{13,5},{2,10},{6,14},... | collective-permute-start | bytes 786440 | tf_op jit(solution)/shard_map/ppermute | solution.py:893
  69.6 1.5 %collective-permute-start.22 = (bf16[1024,256]{1,0:T(8,128)(2,1)S(1)}, bf16[1024,256]{1,0:T(8,128)(2,1)S(1)}, u32[]{:S(2)}, u32[]{:S(2)}) collective-permute-start(bf16[1024,256]{1,0:T(8,128)(2,1)S(1)} %pad_maximum_fusion.refs_8_), channel_id=1, source_target_pairs={{0,2},{2,0},{1,3},{3,1},{4,6},{6,4},{5,7},{7,5},{8,10},{10,8},{9,1... | collective-permute-start | bytes 1572872 | tf_op jit(solution)/shard_map/ppermute | solution.py:890
  71.1 18.2 %collective-permute-done.23.refs_10_ = bf16[512,256]{1,0:T(8,128)(2,1)S(1)} collective-permute-done((bf16[512,256]{1,0:T(8,128)(2,1)S(1)}, bf16[512,256]{1,0:T(8,128)(2,1)S(1)}, u32[]{:S(2)}, u32[]{:S(2)}) %collective-permute-start.23) | collective-permute-done | bytes 262176 | tf_op jit(solution)/shard_map/ppermute | solution.py:893
  89.3 0.5 collective-permute-start.24
  89.8 4.3 %shard_map.201 = (bf16[256,128]{1,0:T(8,128)(2,1)}, bf16[256,128]{1,0:T(8,128)(2,1)}, bf16[256,128]{1,0:T(8,128)(2,1)}, bf16[256,128]{1,0:T(8,128)(2,1)}) custom-call(bf16[2,256,384]{2,1,0:T(8,128)(2,1)S(1)} %get-tuple-element.37.fine_ref, f32[2,256,48]{2,1,0:T(8,128)S(1)} %get-tuple-element.38.ext_ref, f32[1,1280]{1,0:T(1,128)S(1)} %broadcast_in_dim.11.gain_ref), custom_call_target="tpu_custom_call" | custom-call | tf_op jit(solution)/shard_map/pallas_call | solution.py:371
  94.2 1.6 %collective-permute-start.25 = (bf16[512,256]{1,0:T(8,128)(2,1)S(1)}, bf16[512,256]{1,0:T(8,128)(2,1)S(1)}, u32[]{:S(2)}, u32[]{:S(2)}) collective-permute-start(bf16[512,256]{1,0:T(8,128)(2,1)S(1)} %collective-permute-done.23.refs_10_), channel_id=1, source_target_pairs={{0,2},{2,0},{1,3},{3,1},{4,6},{6,4},{5,7},{7,5},{8,10},{10,8},{9,1... | collective-permute-start | bytes 786440 | tf_op jit(solution)/shard_map/ppermute | solution.py:890
  95.8 0.9 collective-permute-done.24.refs_11_
  96.6 1.5 %collective-permute-start.26 = (bf16[512,256]{1,0:T(8,128)(2,1)S(1)}, bf16[512,256]{1,0:T(8,128)(2,1)S(1)}, u32[]{:S(2)}, u32[]{:S(2)}) collective-permute-start(bf16[512,256]{1,0:T(8,128)(2,1)S(1)} %collective-permute-done.24.refs_11_), channel_id=1, source_target_pairs={{0,2},{2,0},{1,3},{3,1},{4,6},{6,4},{5,7},{7,5},{8,10},{10,8},{9,1... | collective-permute-start | bytes 786440 | tf_op jit(solution)/shard_map/ppermute | solution.py:890
  98.1 1.4 %collective-permute-start.15 = (bf16[256,128]{1,0:T(8,128)(2,1)}, bf16[256,128]{1,0:T(8,128)(2,1)S(1)}, u32[]{:S(2)}, u32[]{:S(2)}) collective-permute-start(bf16[256,128]{1,0:T(8,128)(2,1)} %get-tuple-element.41), channel_id=1, source_target_pairs={{0,12},{4,0},{8,4},{12,8},{1,13},{5,1},{9,5},{13,9},{2,14},{6,2},{... | collective-permute-start | bytes 196616 | tf_op jit(solution)/shard_map/ppermute | solution.py:893
  99.5 0.7 copy-done.10
  100.3 4.3 %shard_map.202 = (bf16[256,128]{1,0:T(8,128)(2,1)S(1)}, bf16[256,128]{1,0:T(8,128)(2,1)S(1)}, bf16[256,128]{1,0:T(8,128)(2,1)S(1)}, bf16[256,128]{1,0:T(8,128)(2,1)S(1)}) custom-call(bf16[4,384,128]{2,1,0:T(8,128)(2,1)} %copy-done.9, bf16[4,384,128]{2,1,0:T(8,128)(2,1)} %copy-done.10, f32[2,256,48]{2,1,0:T(8,128)S(1)} %get-tuple-element.38.ext_ref, ...), custom_call_target="tpu_custom_call" | custom-call | tf_op jit(solution)/shard_map/pallas_call | solution.py:371
  104.6 0.7 collective-permute-start.17
  105.3 3.2 %collective-permute-start.19 = (bf16[256,128]{1,0:T(8,128)(2,1)S(1)}, bf16[256,128]{1,0:T(8,128)(2,1)S(1)}, u32[]{:S(2)}, u32[]{:S(2)}) collective-permute-start(bf16[256,128]{1,0:T(8,128)(2,1)S(1)} %get-tuple-element.50), channel_id=1, source_target_pairs={{0,12},{4,0},{8,4},{12,8},{1,13},{5,1},{9,5},{13,9},{2,14},{6,2},{... | collective-permute-start | bytes 196616 | tf_op jit(solution)/shard_map/ppermute | solution.py:893
  108.9 1.7 %collective-permute-start.21 = (bf16[256,128]{1,0:T(8,128)(2,1)S(1)}, bf16[256,128]{1,0:T(8,128)(2,1)S(1)}, u32[]{:S(2)}, u32[]{:S(2)}) collective-permute-start(bf16[256,128]{1,0:T(8,128)(2,1)S(1)} %get-tuple-element.52), channel_id=1, source_target_pairs={{0,4},{4,8},{8,12},{12,0},{1,5},{5,9},{9,13},{13,1},{2,6},{6,10},{... | collective-permute-start | bytes 196616 | tf_op jit(solution)/shard_map/ppermute | solution.py:893
  111.0 4.6 %collective-permute-done.20.refs_6_ = bf16[256,128]{1,0:T(8,128)(2,1)S(1)} collective-permute-done((bf16[256,128]{1,0:T(8,128)(2,1)S(1)}, bf16[256,128]{1,0:T(8,128)(2,1)S(1)}, u32[]{:S(2)}, u32[]{:S(2)}) %collective-permute-start.20) | collective-permute-done | bytes 65568 | tf_op jit(solution)/shard_map/ppermute | solution.py:893
  115.6 0.9 shard_map.203
  116.6 1.5 %collective-permute-done.27 = bf16[2,128,512]{2,1,0:T(8,128)(2,1)S(1)} collective-permute-done((bf16[2,128,512]{2,1,0:T(8,128)(2,1)S(1)}, bf16[2,128,512]{2,1,0:T(8,128)(2,1)S(1)}, u32[]{:S(2)}, u32[]{:S(2)}) %collective-permute-start.27) | collective-permute-done | bytes 262176 | tf_op jit(solution)/shard_map/ppermute | solution.py:890
  118.5 1.0 collective-permute-done.29
  119.6 2.1 %collective-permute-start.28 = (bf16[128,512]{1,0:T(8,128)(2,1)S(1)}, bf16[128,512]{1,0:T(8,128)(2,1)S(1)}, u32[]{:S(2)}, u32[]{:S(2)}) collective-permute-start(bf16[128,512]{1,0:T(8,128)(2,1)S(1)} %dynamic-slice_bitcast_fusion), channel_id=1, source_target_pairs={{0,4},{4,0},{8,12},{12,8},{1,5},{5,1},{9,13},{13,9},{2,6},{6,2},{1... | collective-permute-start | bytes 393224 | tf_op jit(solution)/shard_map/ppermute | solution.py:983
  121.7 1.5 %collective-permute-done.30 = f32[128]{0:T(128)S(1)} collective-permute-done((f32[128]{0:T(128)S(1)}, f32[128]{0:T(128)S(1)}, u32[]{:S(2)}, u32[]{:S(2)}) %collective-permute-start.30) | collective-permute-done | bytes 544 | tf_op jit(solution)/shard_map/ppermute | solution.py:983
  123.2 2.0 %collective-permute-done.28 = bf16[128,512]{1,0:T(8,128)(2,1)S(1)} collective-permute-done((bf16[128,512]{1,0:T(8,128)(2,1)S(1)}, bf16[128,512]{1,0:T(8,128)(2,1)S(1)}, u32[]{:S(2)}, u32[]{:S(2)}) %collective-permute-start.28) | collective-permute-done | bytes 131104 | tf_op jit(solution)/shard_map/ppermute | solution.py:983
  125.3 0.7 slice-done
  126.0 0.8 fusion.1
  (112 shorter events, 2.5 us)
Async XLA Ops:
  2.3 6.5 %copy-start = (bf16[2,64,2048]{2,1,0:T(8,128)(2,1)S(1)}, bf16[2,64,2048]{2,1,0:T(8,128)(2,1)}, u32[]{:S(2)}) copy-start(bf16[2,64,2048]{2,1,0:T(8,128)(2,1)} %param.21) | copy-start | bytes 1572868
  2.3 6.5 %copy-start.7 = (f32[2048]{0:T(1024)S(1)}, f32[2048]{0:T(1024)}, u32[]{:S(2)}) copy-start(f32[2048]{0:T(1024)} %param.22) | copy-start | bytes 24580
  2.3 32.7 %all-to-all-start = ((bf16[4,128,512]{2,1,0:T(8,128)(2,1)}), bf16[4,128,512]{2,1,0:T(8,128)(2,1)S(1)}, u32[]{:S(2)}, u32[]{:S(2)}) async-start(bf16[4,128,512]{2,1,0:T(8,128)(2,1)} %get-tuple-element.30), calls=%async_computation | async-start | bytes 1048576 | tf_op jit(solution)/shard_map/all_to_all | solution.py:887
  9.2 26.0 %copy-start.1 = (bf16[128,1024]{1,0:T(8,128)(2,1)}, bf16[128,1024]{1,0:T(8,128)(2,1)S(1)}, u32[]{:S(2)}) copy-start(bf16[128,1024]{1,0:T(8,128)(2,1)S(1)} %get-tuple-element.32.refs_0_) | copy-start | bytes 786436
  9.2 26.0 %copy-start.2 = (bf16[128,1024]{1,0:T(8,128)(2,1)}, bf16[128,1024]{1,0:T(8,128)(2,1)S(1)}, u32[]{:S(2)}) copy-start(bf16[128,1024]{1,0:T(8,128)(2,1)S(1)} %get-tuple-element.34.refs_4_) | copy-start | bytes 786436
  9.2 25.3 %collective-permute-start.1 = (bf16[128,1024]{1,0:T(8,128)(2,1)S(1)}, bf16[128,1024]{1,0:T(8,128)(2,1)S(1)}, u32[]{:S(2)}, u32[]{:S(2)}) collective-permute-start(bf16[128,1024]{1,0:T(8,128)(2,1)S(1)} %get-tuple-element.32.refs_0_), channel_id=1, source_target_pairs={{0,8},{4,12},{8,0},{12,4},{1,9},{5,13},{9,1},{13,5},{2,10},{6,14},... | collective-permute-start | bytes 786440 | tf_op jit(solution)/shard_map/ppermute | solution.py:893
  12.2 22.4 %collective-permute-start = (bf16[128,1024]{1,0:T(8,128)(2,1)S(1)}, bf16[128,1024]{1,0:T(8,128)(2,1)S(1)}, u32[]{:S(2)}, u32[]{:S(2)}) collective-permute-start(bf16[128,1024]{1,0:T(8,128)(2,1)S(1)} %get-tuple-element.32.refs_0_), channel_id=1, source_target_pairs={{0,4},{4,0},{8,12},{12,8},{1,5},{5,1},{9,13},{13,9},{2,6},{6,2},{1... | collective-permute-start | bytes 786440 | tf_op jit(solution)/shard_map/ppermute | solution.py:907
  13.6 5.0 %collective-permute-start.9 = (bf16[128,512]{1,0:T(8,128)(2,1)S(1)}, bf16[128,512]{1,0:T(8,128)(2,1)S(1)}, u32[]{:S(2)}, u32[]{:S(2)}) collective-permute-start(bf16[128,512]{1,0:T(8,128)(2,1)S(1)} %copy-done.32), channel_id=1, source_target_pairs={{0,16},{16,0},{1,17},{17,1},{2,18},{18,2},{3,19},{19,3},{4,20},{20... | collective-permute-start | bytes 393224 | tf_op jit(solution)/shard_map/ppermute | solution.py:890
  15.1 20.9 %collective-permute-start.6 = (bf16[128,512]{1,0:T(8,128)(2,1)S(1)}, bf16[128,512]{1,0:T(8,128)(2,1)S(1)}, u32[]{:S(2)}, u32[]{:S(2)}) collective-permute-start(bf16[128,512]{1,0:T(8,128)(2,1)S(1)} %copy-done.32), channel_id=1, source_target_pairs={{0,2},{2,0},{1,3},{3,1},{4,6},{6,4},{5,7},{7,5},{8,10},{10,8},{9,1... | collective-permute-start | bytes 393224 | tf_op jit(solution)/shard_map/ppermute | solution.py:890
  18.6 16.6 %copy-start.24 = (bf16[128,512]{1,0:T(8,128)(2,1)}, bf16[128,512]{1,0:T(8,128)(2,1)S(1)}, u32[]{:S(2)}) copy-start(bf16[128,512]{1,0:T(8,128)(2,1)S(1)} %collective-permute-done.9.refs_12_) | copy-start | bytes 393220
  18.6 19.1 %collective-permute-start.12 = (bf16[128,512]{1,0:T(8,128)(2,1)S(1)}, bf16[128,512]{1,0:T(8,128)(2,1)S(1)}, u32[]{:S(2)}, u32[]{:S(2)}) collective-permute-start(bf16[128,512]{1,0:T(8,128)(2,1)S(1)} %collective-permute-done.9.refs_12_), channel_id=1, source_target_pairs={{0,2},{2,0},{1,3},{3,1},{4,6},{6,4},{5,7},{7,5},{8,10},{10,8},{9,1... | collective-permute-start | bytes 393224 | tf_op jit(solution)/shard_map/ppermute | solution.py:890
  34.5 7.3 %collective-permute-start.2 = (bf16[128,1024]{1,0:T(8,128)(2,1)S(1)}, bf16[128,1024]{1,0:T(8,128)(2,1)S(1)}, u32[]{:S(2)}, u32[]{:S(2)}) collective-permute-start(bf16[128,1024]{1,0:T(8,128)(2,1)S(1)} %collective-permute-done.1.refs_2_), channel_id=1, source_target_pairs={{0,4},{4,0},{8,12},{12,8},{1,5},{5,1},{9,13},{13,9},{2,6},{6,2},{1... | collective-permute-start | bytes 786440 | tf_op jit(solution)/shard_map/ppermute | solution.py:907
  34.5 9.4 %collective-permute-start.4 = (bf16[128,1024]{1,0:T(8,128)(2,1)S(1)}, bf16[128,1024]{1,0:T(8,128)(2,1)S(1)}, u32[]{:S(2)}, u32[]{:S(2)}) collective-permute-start(bf16[128,1024]{1,0:T(8,128)(2,1)S(1)} %collective-permute-done.1.refs_2_), channel_id=1, source_target_pairs={{0,1},{1,0},{2,3},{3,2},{4,5},{5,4},{6,7},{7,6},{8,9},{9,8},{10,11... | collective-permute-start | bytes 786440 | tf_op jit(solution)/shard_map/ppermute | solution.py:890
  34.6 11.0 %collective-permute-start.3 = (bf16[128,1024]{1,0:T(8,128)(2,1)S(1)}, bf16[128,1024]{1,0:T(8,128)(2,1)S(1)}, u32[]{:S(2)}, u32[]{:S(2)}) collective-permute-start(bf16[128,1024]{1,0:T(8,128)(2,1)S(1)} %collective-permute-done.refs_1_), channel_id=1, source_target_pairs={{0,1},{1,0},{2,3},{3,2},{4,5},{5,4},{6,7},{7,6},{8,9},{9,8},{10,11... | collective-permute-start | bytes 786440 | tf_op jit(solution)/shard_map/ppermute | solution.py:890
  36.0 5.9 %copy-start.25 = (bf16[128,512]{1,0:T(8,128)(2,1)}, bf16[128,512]{1,0:T(8,128)(2,1)S(1)}, u32[]{:S(2)}) copy-start(bf16[128,512]{1,0:T(8,128)(2,1)S(1)} %collective-permute-done.6.refs_9_) | copy-start | bytes 393220
  36.1 11.0 %collective-permute-start.10 = (bf16[192,512]{1,0:T(8,128)(2,1)}, bf16[192,512]{1,0:T(8,128)(2,1)S(1)}, u32[]{:S(2)}, u32[]{:S(2)}) collective-permute-start(bf16[192,512]{1,0:T(8,128)(2,1)} %get-tuple-element.60), channel_id=1, source_target_pairs={{0,16},{16,0},{1,17},{17,1},{2,18},{18,2},{3,19},{19,3},{4,20},{20... | collective-permute-start | bytes 589832 | tf_op jit(solution)/shard_map/ppermute | solution.py:890
  37.7 9.9 %collective-permute-start.8 = (bf16[192,512]{1,0:T(8,128)(2,1)}, bf16[192,512]{1,0:T(8,128)(2,1)}, u32[]{:S(2)}, u32[]{:S(2)}) collective-permute-start(bf16[192,512]{1,0:T(8,128)(2,1)} %get-tuple-element.59), channel_id=1, source_target_pairs={{0,2},{2,0},{1,3},{3,1},{4,6},{6,4},{5,7},{7,5},{8,10},{10,8},{9,1... | collective-permute-start | bytes 589832 | tf_op jit(solution)/shard_map/ppermute | solution.py:890
  41.9 6.3 %collective-permute-start.5 = (bf16[128,1024]{1,0:T(8,128)(2,1)S(1)}, bf16[128,1024]{1,0:T(8,128)(2,1)S(1)}, u32[]{:S(2)}, u32[]{:S(2)}) collective-permute-start(bf16[128,1024]{1,0:T(8,128)(2,1)S(1)} %collective-permute-done.2.refs_3_), channel_id=1, source_target_pairs={{0,1},{1,0},{2,3},{3,2},{4,5},{5,4},{6,7},{7,6},{8,9},{9,8},{10,11... | collective-permute-start | bytes 786440 | tf_op jit(solution)/shard_map/ppermute | solution.py:890
  41.9 76.6 %copy-start.6 = (f32[1,1280]{1,0:T(1,128)}, f32[1,1280]{1,0:T(1,128)S(1)}, u32[]{:S(2)}) copy-start(f32[1,1280]{1,0:T(1,128)S(1)} %broadcast_in_dim.11.gain_ref) | copy-start | bytes 15364
  41.9 6.2 %copy-start.17 = (bf16[512,256]{1,0:T(8,128)(2,1)S(1)}, bf16[512,256]{1,0:T(8,128)(2,1)}, u32[]{:S(2)}) copy-start(bf16[512,256]{1,0:T(8,128)(2,1)} %param.37) | copy-start | bytes 786436
  42.0 6.2 %copy-start.18 = (bf16[512,256]{1,0:T(8,128)(2,1)S(1)}, bf16[512,256]{1,0:T(8,128)(2,1)}, u32[]{:S(2)}) copy-start(bf16[512,256]{1,0:T(8,128)(2,1)} %param.38) | copy-start | bytes 786436
  44.0 8.0 %collective-permute-start.11 = (bf16[192,512]{1,0:T(8,128)(2,1)}, bf16[192,512]{1,0:T(8,128)(2,1)S(1)}, u32[]{:S(2)}, u32[]{:S(2)}) collective-permute-start(bf16[192,512]{1,0:T(8,128)(2,1)} %get-tuple-element.59), channel_id=1, source_target_pairs={{0,16},{16,0},{1,17},{17,1},{2,18},{18,2},{3,19},{19,3},{4,20},{20... | collective-permute-start | bytes 589832 | tf_op jit(solution)/shard_map/ppermute | solution.py:890
  45.6 8.0 %collective-permute-start.7 = (bf16[192,512]{1,0:T(8,128)(2,1)}, bf16[192,512]{1,0:T(8,128)(2,1)S(1)}, u32[]{:S(2)}, u32[]{:S(2)}) collective-permute-start(bf16[192,512]{1,0:T(8,128)(2,1)} %get-tuple-element.60), channel_id=1, source_target_pairs={{0,2},{2,0},{1,3},{3,1},{4,6},{6,4},{5,7},{7,5},{8,10},{10,8},{9,1... | collective-permute-start | bytes 589832 | tf_op jit(solution)/shard_map/ppermute | solution.py:890
  47.1 9.9 %collective-permute-start.13 = (bf16[192,512]{1,0:T(8,128)(2,1)S(1)}, bf16[192,512]{1,0:T(8,128)(2,1)S(1)}, u32[]{:S(2)}, u32[]{:S(2)}) collective-permute-start(bf16[192,512]{1,0:T(8,128)(2,1)S(1)} %collective-permute-done.10.refs_13_), channel_id=1, source_target_pairs={{0,2},{2,0},{1,3},{3,1},{4,6},{6,4},{5,7},{7,5},{8,10},{10,8},{9,1... | collective-permute-start | bytes 589832 | tf_op jit(solution)/shard_map/ppermute | solution.py:890
  47.6 9.4 %collective-permute-start.14 = (bf16[192,512]{1,0:T(8,128)(2,1)}, bf16[192,512]{1,0:T(8,128)(2,1)S(1)}, u32[]{:S(2)}, u32[]{:S(2)}) collective-permute-start(bf16[192,512]{1,0:T(8,128)(2,1)} %collective-permute-done.8.refs_11_), channel_id=1, source_target_pairs={{0,16},{16,0},{1,17},{17,1},{2,18},{18,2},{3,19},{19,3},{4,20},{20... | collective-permute-start | bytes 589832 | tf_op jit(solution)/shard_map/ppermute | solution.py:890
  48.2 8.8 %copy-start.16 = (bf16[128,1024]{1,0:T(8,128)(2,1)}, bf16[128,1024]{1,0:T(8,128)(2,1)S(1)}, u32[]{:S(2)}) copy-start(bf16[128,1024]{1,0:T(8,128)(2,1)S(1)} %collective-permute-done.5.refs_7_) | copy-start | bytes 786436
  52.0 5.0 %copy-start.20 = (bf16[192,512]{1,0:T(8,128)(2,1)}, bf16[192,512]{1,0:T(8,128)(2,1)S(1)}, u32[]{:S(2)}) copy-start(bf16[192,512]{1,0:T(8,128)(2,1)S(1)} %collective-permute-done.11.refs_14_) | copy-start | bytes 589828
  63.1 31.0 %all-to-all-start.1 = ((bf16[4,384,128]{2,1,0:T(8,128)(2,1)}), bf16[4,384,128]{2,1,0:T(8,128)(2,1)S(1)}, u32[]{:S(2)}, u32[]{:S(2)}) async-start(bf16[4,384,128]{2,1,0:T(8,128)(2,1)} %get-tuple-element.44), calls=%async_computation.1 | async-start | bytes 786432 | tf_op jit(solution)/shard_map/all_to_all | solution.py:887
  66.7 22.6 %collective-permute-start.23 = (bf16[512,256]{1,0:T(8,128)(2,1)S(1)}, bf16[512,256]{1,0:T(8,128)(2,1)S(1)}, u32[]{:S(2)}, u32[]{:S(2)}) collective-permute-start(bf16[512,256]{1,0:T(8,128)(2,1)S(1)} %constant_dynamic-slice_fusion.2), channel_id=1, source_target_pairs={{0,8},{4,12},{8,0},{12,4},{1,9},{5,13},{9,1},{13,5},{2,10},{6,14},... | collective-permute-start | bytes 786440 | tf_op jit(solution)/shard_map/ppermute | solution.py:893
  69.6 35.6 %collective-permute-start.22 = (bf16[1024,256]{1,0:T(8,128)(2,1)S(1)}, bf16[1024,256]{1,0:T(8,128)(2,1)S(1)}, u32[]{:S(2)}, u32[]{:S(2)}) collective-permute-start(bf16[1024,256]{1,0:T(8,128)(2,1)S(1)} %pad_maximum_fusion.refs_8_), channel_id=1, source_target_pairs={{0,2},{2,0},{1,3},{3,1},{4,6},{6,4},{5,7},{7,5},{8,10},{10,8},{9,1... | collective-permute-start | bytes 1572872 | tf_op jit(solution)/shard_map/ppermute | solution.py:890
  89.3 7.3 %collective-permute-start.24 = (bf16[512,256]{1,0:T(8,128)(2,1)S(1)}, bf16[512,256]{1,0:T(8,128)(2,1)S(1)}, u32[]{:S(2)}, u32[]{:S(2)}) collective-permute-start(bf16[512,256]{1,0:T(8,128)(2,1)S(1)} %collective-permute-done.23.refs_10_), channel_id=1, source_target_pairs={{0,16},{16,0},{1,17},{17,1},{2,18},{18,2},{3,19},{19,3},{4,20},{20... | collective-permute-start | bytes 786440 | tf_op jit(solution)/shard_map/ppermute | solution.py:890
  89.8 10.5 %copy-start.3 = (f32[256,64]{1,0:T(8,128)S(1)}, f32[256,64]{1,0:T(8,128)}, u32[]{:S(2)}) copy-start(f32[256,64]{1,0:T(8,128)} %constant.53.clone.cos_ref) | copy-start | bytes 196612
  89.8 10.5 %copy-start.4 = (f32[256,64]{1,0:T(8,128)S(1)}, f32[256,64]{1,0:T(8,128)}, u32[]{:S(2)}) copy-start(f32[256,64]{1,0:T(8,128)} %constant.54.clone.sin_ref) | copy-start | bytes 196612
  94.1 5.4 %copy-start.9 = (bf16[4,384,128]{2,1,0:T(8,128)(2,1)}, bf16[4,384,128]{2,1,0:T(8,128)(2,1)S(1)}, u32[]{:S(2)}) copy-start(bf16[4,384,128]{2,1,0:T(8,128)(2,1)S(1)} %all-to-all-done.1.mine_ref) | copy-start | bytes 1179652
  94.1 5.4 %collective-permute-start.18 = (bf16[4,384,128]{2,1,0:T(8,128)(2,1)S(1)}, bf16[4,384,128]{2,1,0:T(8,128)(2,1)S(1)}, u32[]{:S(2)}, u32[]{:S(2)}) collective-permute-start(bf16[4,384,128]{2,1,0:T(8,128)(2,1)S(1)} %all-to-all-done.1.mine_ref), channel_id=1, source_target_pairs={{0,1},{1,0},{2,3},{3,2},{4,5},{5,4},{6,7},{7,6},{8,9},{9,8},{10,11... | collective-permute-start | bytes 1179656 | tf_op jit(solution)/shard_map/ppermute | solution.py:890
  94.2 10.4 %collective-permute-start.25 = (bf16[512,256]{1,0:T(8,128)(2,1)S(1)}, bf16[512,256]{1,0:T(8,128)(2,1)S(1)}, u32[]{:S(2)}, u32[]{:S(2)}) collective-permute-start(bf16[512,256]{1,0:T(8,128)(2,1)S(1)} %collective-permute-done.23.refs_10_), channel_id=1, source_target_pairs={{0,2},{2,0},{1,3},{3,1},{4,6},{6,4},{5,7},{7,5},{8,10},{10,8},{9,1... | collective-permute-start | bytes 786440 | tf_op jit(solution)/shard_map/ppermute | solution.py:890
  96.6 11.9 %collective-permute-start.26 = (bf16[512,256]{1,0:T(8,128)(2,1)S(1)}, bf16[512,256]{1,0:T(8,128)(2,1)S(1)}, u32[]{:S(2)}, u32[]{:S(2)}) collective-permute-start(bf16[512,256]{1,0:T(8,128)(2,1)S(1)} %collective-permute-done.24.refs_11_), channel_id=1, source_target_pairs={{0,2},{2,0},{1,3},{3,1},{4,6},{6,4},{5,7},{7,5},{8,10},{10,8},{9,1... | collective-permute-start | bytes 786440 | tf_op jit(solution)/shard_map/ppermute | solution.py:890
  98.1 10.8 %collective-permute-start.15 = (bf16[256,128]{1,0:T(8,128)(2,1)}, bf16[256,128]{1,0:T(8,128)(2,1)S(1)}, u32[]{:S(2)}, u32[]{:S(2)}) collective-permute-start(bf16[256,128]{1,0:T(8,128)(2,1)} %get-tuple-element.41), channel_id=1, source_target_pairs={{0,12},{4,0},{8,4},{12,8},{1,13},{5,1},{9,5},{13,9},{2,14},{6,2},{... | collective-permute-start | bytes 196616 | tf_op jit(solution)/shard_map/ppermute | solution.py:893
  99.5 11.1 %collective-permute-start.16 = (bf16[256,128]{1,0:T(8,128)(2,1)}, bf16[256,128]{1,0:T(8,128)(2,1)S(1)}, u32[]{:S(2)}, u32[]{:S(2)}) collective-permute-start(bf16[256,128]{1,0:T(8,128)(2,1)} %get-tuple-element.42), channel_id=1, source_target_pairs={{0,8},{4,12},{8,0},{12,4},{1,9},{5,13},{9,1},{13,5},{2,10},{6,14},... | collective-permute-start | bytes 196616 | tf_op jit(solution)/shard_map/ppermute | solution.py:893
  100.3 15.4 %copy-start.5 = (bf16[256,128]{1,0:T(8,128)(2,1)S(1)}, bf16[256,128]{1,0:T(8,128)(2,1)}, u32[]{:S(2)}) copy-start(bf16[256,128]{1,0:T(8,128)(2,1)} %get-tuple-element.40.refs_0_) | copy-start | bytes 196612
  104.6 6.5 %collective-permute-start.17 = (bf16[256,128]{1,0:T(8,128)(2,1)S(1)}, bf16[256,128]{1,0:T(8,128)(2,1)S(1)}, u32[]{:S(2)}, u32[]{:S(2)}) collective-permute-start(bf16[256,128]{1,0:T(8,128)(2,1)S(1)} %copy-done.33), channel_id=1, source_target_pairs={{0,4},{4,8},{8,12},{12,0},{1,5},{5,9},{9,13},{13,1},{2,6},{6,10},{... | collective-permute-start | bytes 196616 | tf_op jit(solution)/shard_map/ppermute | solution.py:893
  105.3 5.8 %collective-permute-start.19 = (bf16[256,128]{1,0:T(8,128)(2,1)S(1)}, bf16[256,128]{1,0:T(8,128)(2,1)S(1)}, u32[]{:S(2)}, u32[]{:S(2)}) collective-permute-start(bf16[256,128]{1,0:T(8,128)(2,1)S(1)} %get-tuple-element.50), channel_id=1, source_target_pairs={{0,12},{4,0},{8,4},{12,8},{1,13},{5,1},{9,5},{13,9},{2,14},{6,2},{... | collective-permute-start | bytes 196616 | tf_op jit(solution)/shard_map/ppermute | solution.py:893
  108.5 7.1 %collective-permute-start.20 = (bf16[256,128]{1,0:T(8,128)(2,1)S(1)}, bf16[256,128]{1,0:T(8,128)(2,1)S(1)}, u32[]{:S(2)}, u32[]{:S(2)}) collective-permute-start(bf16[256,128]{1,0:T(8,128)(2,1)S(1)} %get-tuple-element.51), channel_id=1, source_target_pairs={{0,8},{4,12},{8,0},{12,4},{1,9},{5,13},{9,1},{13,5},{2,10},{6,14},... | collective-permute-start | bytes 196616 | tf_op jit(solution)/shard_map/ppermute | solution.py:893
  108.9 6.8 %collective-permute-start.21 = (bf16[256,128]{1,0:T(8,128)(2,1)S(1)}, bf16[256,128]{1,0:T(8,128)(2,1)S(1)}, u32[]{:S(2)}, u32[]{:S(2)}) collective-permute-start(bf16[256,128]{1,0:T(8,128)(2,1)S(1)} %get-tuple-element.52), channel_id=1, source_target_pairs={{0,4},{4,8},{8,12},{12,0},{1,5},{5,9},{9,13},{13,1},{2,6},{6,10},{... | collective-permute-start | bytes 196616 | tf_op jit(solution)/shard_map/ppermute | solution.py:893
  116.5 1.6 %collective-permute-start.27 = (bf16[2,128,512]{2,1,0:T(8,128)(2,1)S(1)}, bf16[2,128,512]{2,1,0:T(8,128)(2,1)S(1)}, u32[]{:S(2)}, u32[]{:S(2)}) collective-permute-start(bf16[2,128,512]{2,1,0:T(8,128)(2,1)S(1)} %get-tuple-element.54), channel_id=1, source_target_pairs={{0,1},{1,0},{2,3},{3,2},{4,5},{5,4},{6,7},{7,6},{8,9},{9,8},{10,11... | collective-permute-start | bytes 786440 | tf_op jit(solution)/shard_map/ppermute | solution.py:890
  118.3 1.2 collective-permute-start.29
  119.5 3.6 %collective-permute-start.30 = (f32[128]{0:T(128)S(1)}, f32[128]{0:T(128)S(1)}, u32[]{:S(2)}, u32[]{:S(2)}) collective-permute-start(f32[128]{0:T(128)S(1)} %fusion.8), channel_id=1, source_target_pairs={{0,4},{4,0},{8,12},{12,8},{1,5},{5,1},{9,13},{13,9},{2,6},{6,2},{1... | collective-permute-start | bytes 1544 | tf_op jit(solution)/shard_map/ppermute | solution.py:983
  119.6 5.6 %collective-permute-start.28 = (bf16[128,512]{1,0:T(8,128)(2,1)S(1)}, bf16[128,512]{1,0:T(8,128)(2,1)S(1)}, u32[]{:S(2)}, u32[]{:S(2)}) collective-permute-start(bf16[128,512]{1,0:T(8,128)(2,1)S(1)} %dynamic-slice_bitcast_fusion), channel_id=1, source_target_pairs={{0,4},{4,0},{8,12},{12,8},{1,5},{5,1},{9,13},{13,9},{2,6},{6,2},{1... | collective-permute-start | bytes 393224 | tf_op jit(solution)/shard_map/ppermute | solution.py:983
  (20 other events, 51.7 us)
where the time goes:
time: 127 us
  waiting for transfers between devices  58 us (46%)
  starting transfers between devices  44.4 us (35%)
  Pallas kernels  19.4 us (15%)
  local copies, waits for them, and re-layouts  3.26 us (3%)
    ppermute x8, waiting for transfers between devices, along(): lax.ppermute(values, 'sp', [(i, (i + step) % sp_size) for i in range(sp_s...  37.7 us
    ppermute x19, starting transfers between devices, swap(): return lax.ppermute(values, axis, [(0, 1), (1, 0)])  17.6 us
    ppermute x19, waiting for transfers between devices, swap(): return lax.ppermute(values, axis, [(0, 1), (1, 0)])  14.2 us
    ppermute x8, starting transfers between devices, along(): lax.ppermute(values, 'sp', [(i, (i + step) % sp_size) for i in range(sp_s...  13.2 us
    pallas_call x5, Pallas kernels, kernel_call(): pl.pallas_call(body, out_shape=jax.tree.map(lambda leaf: result_space(lea...  11.8 us
    all_to_all x2, starting transfers between devices, exchange(): return lax.all_to_all(values, axis, 0, 0, tiled=True)  9.96 us
    pallas_call x1, Pallas kernels, project(): pl.pallas_call(body, out_shape=(pltpu.VMEM((seq_count, span, fine), jnp.b...  5.33 us
    ppermute x2, waiting for transfers between devices, across(): lax.ppermute(pick(values, 1 - side), 'sp', [(i, i ^ 1) for i in range(sp_...  3.47 us
  transfers between devices with their start and end apart: 33, of which 15 were waited for; matrix products, arithmetic and copies ran while one was open for 1% of the time, Pallas kernels for 9%

commit v1 on v0

--- a/solution.py
+++ b/solution.py
@@ -782,11 +782,11 @@
 
     shape = jax.ShapeDtypeStruct((rows // 2, heads * VDIM), jnp.bfloat16)
     return kernel_call(
-        body, (shape,) * sp_size, (mine, theirs, ext, *tables, gains, *ups), outside=2
-    )
-
-
-def output_partial(delta_all, latent_all, near, near_fs, far, sizes):
+        body, (shape,) * sp_size, (mine, theirs, ext, *tables, gains, *ups), outside=1
+    )
+
+
+def output_partial(delta_all, latent_all, near, near_fs, far, gain, sizes):
     seq_count, token_count = sizes
     sp_size = len(delta_all)
     rows, d_width = delta_all[0].shape
@@ -798,7 +798,8 @@
     def body(*refs):
         d_refs, refs = refs[:sp_size], refs[sp_size:]
         l_refs, refs = refs[:sp_size], refs[sp_size:]
-        near_ref, near_fs_ref, *far_refs, keep_ref, pass_ref, lhs_ref = refs
+        near_ref, near_fs_ref, *far_refs, gain_ref, keep_ref, pass_ref, kept_ref, lhs_ref = refs
+        kept_ref[...] = gain_ref[...]
         place, fs_at = lax.axis_index("sp"), lax.axis_index("fs")
         grp_at = lax.axis_index("grp")
         for o in range(sp_size):
@@ -837,8 +838,8 @@
     shape = jax.ShapeDtypeStruct((2, rows // 2, 2 * columns), jnp.bfloat16)
     return kernel_call(
         body,
-        (shape, shape),
-        (*delta_all, *latent_all, near, near_fs, *far),
+        (shape, shape, jax.ShapeDtypeStruct(gain.shape, gain.dtype)),
+        (*delta_all, *latent_all, near, near_fs, *far, gain),
         scratch=(pltpu.VMEM((rows, total), jnp.bfloat16),),
     )
 
@@ -942,7 +943,7 @@
     tables = whole_tables(sp_size * token_count, latent_heads)
     rates = jnp.pad(decay_rate, (0, HEAD - decay_rate.shape[0]))
     latent_gains = jnp.concatenate([query_gain, latent_gain])[None, :]
-    gains = jnp.concatenate([delta_gain, rates, post_gain])[None, :]
+    gains = jnp.concatenate([delta_gain, rates])[None, :]
     mine[1], gains, latent_gains = lax.optimization_barrier((mine[1], gains, latent_gains))
 
     fine, lat, ext = project(
@@ -973,8 +974,8 @@
     )
     latent_all = from_sp(latent_sends)
 
-    keep, onward = output_partial(
-        delta_all, latent_all, near, near_fs, far, (seq_count, token_count)
+    keep, onward, post_row = output_partial(
+        delta_all, latent_all, near, near_fs, far, post_gain[None, :], (seq_count, token_count)
     )
     mixed = (keep.astype(f32) + swap(onward, "tp").astype(f32)).astype(bf16)
     side = lax.rem(place, 2)
@@ -990,7 +991,7 @@
     final = jnp.concatenate(
         [jnp.where(side == 0, here, there), jnp.where(side == 0, there, here)], axis=1
     )
-    result = final * lax.rsqrt(squares / D + NORM_EPS) * gains[:, 2 * HEAD :]
+    result = final * lax.rsqrt(squares / D + NORM_EPS) * post_row
     return result.astype(bf16).reshape(seq_count, token_count, final.shape[1])
 
 

time: 127 us -> 126 us (level)
  transfers between devices with their start and end apart: 33 -> 33, of which waited for: 15 -> 14; matrix products, arithmetic and copies ran while one was open for 1% -> 1% of each run, Pallas kernels for 9% -> 9%
where the time goes in v1:
time: 126 us
  waiting for transfers between devices  57.8 us (46%)
  starting transfers between devices  44.4 us (35%)
  Pallas kernels  19.3 us (15%)
  local copies, waits for them, and re-layouts  2.52 us (2%)
  other arithmetic  1.26 us (1%)
    ppermute x8, waiting for transfers between devices, along(): lax.ppermute(values, 'sp', [(i, (i + step) % sp_size) for i in range(sp_s...  37.2 us
    ppermute x19, starting transfers between devices, swap(): return lax.ppermute(values, axis, [(0, 1), (1, 0)])  17.6 us
    ppermute x19, waiting for transfers between devices, swap(): return lax.ppermute(values, axis, [(0, 1), (1, 0)])  15 us
    ppermute x8, starting transfers between devices, along(): lax.ppermute(values, 'sp', [(i, (i + step) % sp_size) for i in range(sp_s...  13.2 us
    pallas_call x5, Pallas kernels, kernel_call(): pl.pallas_call(body, out_shape=jax.tree.map(lambda leaf: result_space(lea...  11.7 us
    all_to_all x2, starting transfers between devices, exchange(): return lax.all_to_all(values, axis, 0, 0, tiled=True)  9.96 us
    pallas_call x1, Pallas kernels, project(): pl.pallas_call(body, out_shape=(pltpu.VMEM((seq_count, span, fine), jnp.b...  5.33 us
    ppermute x2, waiting for transfers between devices, across(): lax.ppermute(pick(values, 1 - side), 'sp', [(i, i ^ 1) for i in range(sp_...  3.47 us
  transfers between devices with their start and end apart: 33, of which 14 were waited for; matrix products, arithmetic and copies ran while one was open for 1% of the time, Pallas kernels for 9%

profile of v1, /device:TPU:0, one launch (start us, length us, event | category | flops | bytes accessed | tf_op | source)
XLA Modules:
  0.0 125.7 jit_solution(2007000161470297605)
XLA Ops:
  0.0 2.3 %outgoing_weights.1 = (bf16[4,128,512]{2,1,0:T(8,128)(2,1)}, bf16[128,512]{1,0:T(8,128)(2,1)}) custom-call(bf16[256,512]{1,0:T(8,128)(2,1)} %refs_0_.1, bf16[256,512]{1,0:T(8,128)(2,1)} %refs_1_.1, bf16[256,512]{1,0:T(8,128)(2,1)} %refs_2_.1, bf16[256,512]{1,0:T(8,128)(2,1)} %refs_3_.1, bf16[256,256]{1,0:T(8,128)(2,1)} %refs_4_.1), custom_call_target="tpu_custom_call" | custom-call | tf_op jit(solution)/shard_map/outgoing_weights/pallas_call | solution.py:422
  2.3 6.5 %all-to-all-start = ((bf16[4,128,512]{2,1,0:T(8,128)(2,1)}), bf16[4,128,512]{2,1,0:T(8,128)(2,1)S(1)}, u32[]{:S(2)}, u32[]{:S(2)}) async-start(bf16[4,128,512]{2,1,0:T(8,128)(2,1)} %get-tuple-element.31), calls=%async_computation | async-start | bytes 1048576 | tf_op jit(solution)/shard_map/all_to_all | solution.py:888
  9.2 3.0 %collective-permute-start.1 = (bf16[128,1024]{1,0:T(8,128)(2,1)S(1)}, bf16[128,1024]{1,0:T(8,128)(2,1)S(1)}, u32[]{:S(2)}, u32[]{:S(2)}) collective-permute-start(bf16[128,1024]{1,0:T(8,128)(2,1)S(1)} %get-tuple-element.33.refs_0_), channel_id=1, source_target_pairs={{0,8},{4,12},{8,0},{12,4},{1,9},{5,13},{9,1},{13,5},{2,10},{6,14},... | collective-permute-start | bytes 786440 | tf_op jit(solution)/shard_map/ppermute | solution.py:894
  12.2 1.5 %collective-permute-start = (bf16[128,1024]{1,0:T(8,128)(2,1)S(1)}, bf16[128,1024]{1,0:T(8,128)(2,1)S(1)}, u32[]{:S(2)}, u32[]{:S(2)}) collective-permute-start(bf16[128,1024]{1,0:T(8,128)(2,1)S(1)} %get-tuple-element.33.refs_0_), channel_id=1, source_target_pairs={{0,4},{4,0},{8,12},{12,8},{1,5},{5,1},{9,13},{13,9},{2,6},{6,2},{1... | collective-permute-start | bytes 786440 | tf_op jit(solution)/shard_map/ppermute | solution.py:908
  13.6 1.5 %collective-permute-start.9 = (bf16[128,512]{1,0:T(8,128)(2,1)S(1)}, bf16[128,512]{1,0:T(8,128)(2,1)S(1)}, u32[]{:S(2)}, u32[]{:S(2)}) collective-permute-start(bf16[128,512]{1,0:T(8,128)(2,1)S(1)} %copy-done.31), channel_id=1, source_target_pairs={{0,16},{16,0},{1,17},{17,1},{2,18},{18,2},{3,19},{19,3},{4,20},{20... | collective-permute-start | bytes 393224 | tf_op jit(solution)/shard_map/ppermute | solution.py:891
  15.2 1.5 %collective-permute-start.6 = (bf16[128,512]{1,0:T(8,128)(2,1)S(1)}, bf16[128,512]{1,0:T(8,128)(2,1)S(1)}, u32[]{:S(2)}, u32[]{:S(2)}) collective-permute-start(bf16[128,512]{1,0:T(8,128)(2,1)S(1)} %copy-done.31), channel_id=1, source_target_pairs={{0,2},{2,0},{1,3},{3,1},{4,6},{6,4},{5,7},{7,5},{8,10},{10,8},{9,1... | collective-permute-start | bytes 393224 | tf_op jit(solution)/shard_map/ppermute | solution.py:891
  16.6 2.0 %collective-permute-done.9.refs_12_ = bf16[128,512]{1,0:T(8,128)(2,1)S(1)} collective-permute-done((bf16[128,512]{1,0:T(8,128)(2,1)S(1)}, bf16[128,512]{1,0:T(8,128)(2,1)S(1)}, u32[]{:S(2)}, u32[]{:S(2)}) %collective-permute-start.9) | collective-permute-done | bytes 131104 | tf_op jit(solution)/shard_map/ppermute | solution.py:891
  18.6 1.5 %collective-permute-start.12 = (bf16[128,512]{1,0:T(8,128)(2,1)S(1)}, bf16[128,512]{1,0:T(8,128)(2,1)S(1)}, u32[]{:S(2)}, u32[]{:S(2)}) collective-permute-start(bf16[128,512]{1,0:T(8,128)(2,1)S(1)} %collective-permute-done.9.refs_12_), channel_id=1, source_target_pairs={{0,2},{2,0},{1,3},{3,1},{4,6},{6,4},{5,7},{7,5},{8,10},{10,8},{9,1... | collective-permute-start | bytes 393224 | tf_op jit(solution)/shard_map/ppermute | solution.py:891
  20.1 14.4 %collective-permute-done.1.refs_2_ = bf16[128,1024]{1,0:T(8,128)(2,1)S(1)} collective-permute-done((bf16[128,1024]{1,0:T(8,128)(2,1)S(1)}, bf16[128,1024]{1,0:T(8,128)(2,1)S(1)}, u32[]{:S(2)}, u32[]{:S(2)}) %collective-permute-start.1) | collective-permute-done | bytes 262176 | tf_op jit(solution)/shard_map/ppermute | solution.py:894
  34.6 0.5 collective-permute-start.3
  35.2 0.8 fusion.8
  36.0 1.6 %collective-permute-start.10 = (bf16[192,512]{1,0:T(8,128)(2,1)}, bf16[192,512]{1,0:T(8,128)(2,1)S(1)}, u32[]{:S(2)}, u32[]{:S(2)}) collective-permute-start(bf16[192,512]{1,0:T(8,128)(2,1)} %get-tuple-element.62), channel_id=1, source_target_pairs={{0,16},{16,0},{1,17},{17,1},{2,18},{18,2},{3,19},{19,3},{4,20},{20... | collective-permute-start | bytes 589832 | tf_op jit(solution)/shard_map/ppermute | solution.py:891
  37.6 0.6 copy-done.26
  38.3 1.5 %collective-permute-start.8 = (bf16[192,512]{1,0:T(8,128)(2,1)}, bf16[192,512]{1,0:T(8,128)(2,1)S(1)}, u32[]{:S(2)}, u32[]{:S(2)}) collective-permute-start(bf16[192,512]{1,0:T(8,128)(2,1)} %get-tuple-element.61), channel_id=1, source_target_pairs={{0,2},{2,0},{1,3},{3,1},{4,6},{6,4},{5,7},{7,5},{8,10},{10,8},{9,1... | collective-permute-start | bytes 589832 | tf_op jit(solution)/shard_map/ppermute | solution.py:891
  39.8 2.1 %collective-permute-done.2.refs_3_ = bf16[128,1024]{1,0:T(8,128)(2,1)S(1)} collective-permute-done((bf16[128,1024]{1,0:T(8,128)(2,1)S(1)}, bf16[128,1024]{1,0:T(8,128)(2,1)S(1)}, u32[]{:S(2)}, u32[]{:S(2)}) %collective-permute-start.2) | collective-permute-done | bytes 262176 | tf_op jit(solution)/shard_map/ppermute | solution.py:908
  41.9 2.0 %shard_map.200 = (bf16[48,2048]{1,0:T(8,128)(2,1)S(1)}, bf16[512,256]{1,0:T(8,128)(2,1)S(1)}, bf16[256,256]{1,0:T(8,128)(2,1)S(1)}) custom-call(bf16[32,2048]{1,0:T(8,128)(2,1)} %bitcast.37, bf16[8,2048]{1,0:T(8,128)(2,1)} %bitcast.38, bf16[8,2048]{1,0:T(8,128)(2,1)} %bitcast.39, bf16[512,768]{1,0:T(8,128)(2,1)} %query_ref.1, bf16[256,1024]{1,0:T(8,128)(2,1)} %latent_ref.1), custom_call_target="tpu_custom_call" | custom-call | tf_op jit(solution)/shard_map/pallas_call | solution.py:371
  44.0 1.6 %collective-permute-start.11 = (bf16[192,512]{1,0:T(8,128)(2,1)}, bf16[192,512]{1,0:T(8,128)(2,1)S(1)}, u32[]{:S(2)}, u32[]{:S(2)}) collective-permute-start(bf16[192,512]{1,0:T(8,128)(2,1)} %get-tuple-element.61), channel_id=1, source_target_pairs={{0,16},{16,0},{1,17},{17,1},{2,18},{18,2},{3,19},{19,3},{4,20},{20... | collective-permute-start | bytes 589832 | tf_op jit(solution)/shard_map/ppermute | solution.py:891
  45.5 1.5 %collective-permute-start.7 = (bf16[192,512]{1,0:T(8,128)(2,1)}, bf16[192,512]{1,0:T(8,128)(2,1)S(1)}, u32[]{:S(2)}, u32[]{:S(2)}) collective-permute-start(bf16[192,512]{1,0:T(8,128)(2,1)} %get-tuple-element.62), channel_id=1, source_target_pairs={{0,2},{2,0},{1,3},{3,1},{4,6},{6,4},{5,7},{7,5},{8,10},{10,8},{9,1... | collective-permute-start | bytes 589832 | tf_op jit(solution)/shard_map/ppermute | solution.py:891
  47.0 0.5 collective-permute-start.13
  47.6 0.6 collective-permute-start.14
  48.3 3.7 %collective-permute-done.11.refs_14_ = bf16[192,512]{1,0:T(8,128)(2,1)S(1)} collective-permute-done((bf16[192,512]{1,0:T(8,128)(2,1)}, bf16[192,512]{1,0:T(8,128)(2,1)S(1)}, u32[]{:S(2)}, u32[]{:S(2)}) %collective-permute-start.11) | collective-permute-done | bytes 196640 | tf_op jit(solution)/shard_map/ppermute | solution.py:891
  52.0 1.5 %collective-permute-done.7.refs_10_ = bf16[192,512]{1,0:T(8,128)(2,1)S(1)} collective-permute-done((bf16[192,512]{1,0:T(8,128)(2,1)}, bf16[192,512]{1,0:T(8,128)(2,1)S(1)}, u32[]{:S(2)}, u32[]{:S(2)}) %collective-permute-start.7) | collective-permute-done | bytes 196640 | tf_op jit(solution)/shard_map/ppermute | solution.py:891
  53.5 3.4 %collective-permute-done.13.refs_16_ = bf16[192,512]{1,0:T(8,128)(2,1)S(1)} collective-permute-done((bf16[192,512]{1,0:T(8,128)(2,1)S(1)}, bf16[192,512]{1,0:T(8,128)(2,1)S(1)}, u32[]{:S(2)}, u32[]{:S(2)}) %collective-permute-start.13) | collective-permute-done | bytes 196640 | tf_op jit(solution)/shard_map/ppermute | solution.py:891
  57.0 0.6 copy-done.22
  57.8 5.3 %project.1 = (bf16[2,256,384]{2,1,0:T(8,128)(2,1)S(1)}, bf16[4,384,128]{2,1,0:T(8,128)(2,1)}, f32[2,256,48]{2,1,0:T(8,128)S(1)}) custom-call(bf16[128,1024]{1,0:T(8,128)(2,1)} %copy-done.1, bf16[128,1024]{1,0:T(8,128)(2,1)} %copy-done.11, bf16[128,1024]{1,0:T(8,128)(2,1)} %copy-done.10, bf16[128,1024]{1,0:T(8,128)(2,1)} %copy-done.12, ...), custom_call_target="tpu_custom_call" | custom-call | tf_op jit(solution)/shard_map/project/pallas_call | solution.py:591
  63.1 3.5 %all-to-all-start.1 = ((bf16[4,384,128]{2,1,0:T(8,128)(2,1)}), bf16[4,384,128]{2,1,0:T(8,128)(2,1)S(1)}, u32[]{:S(2)}, u32[]{:S(2)}) async-start(bf16[4,384,128]{2,1,0:T(8,128)(2,1)} %get-tuple-element.45), calls=%async_computation.1 | async-start | bytes 786432 | tf_op jit(solution)/shard_map/all_to_all | solution.py:888
  66.7 2.9 %collective-permute-start.23 = (bf16[512,256]{1,0:T(8,128)(2,1)S(1)}, bf16[512,256]{1,0:T(8,128)(2,1)S(1)}, u32[]{:S(2)}, u32[]{:S(2)}) collective-permute-start(bf16[512,256]{1,0:T(8,128)(2,1)S(1)} %constant_dynamic-slice_fusion.2), channel_id=1, source_target_pairs={{0,8},{4,12},{8,0},{12,4},{1,9},{5,13},{9,1},{13,5},{2,10},{6,14},... | collective-permute-start | bytes 786440 | tf_op jit(solution)/shard_map/ppermute | solution.py:894
  69.6 1.5 %collective-permute-start.22 = (bf16[1024,256]{1,0:T(8,128)(2,1)S(1)}, bf16[1024,256]{1,0:T(8,128)(2,1)S(1)}, u32[]{:S(2)}, u32[]{:S(2)}) collective-permute-start(bf16[1024,256]{1,0:T(8,128)(2,1)S(1)} %pad_maximum_fusion.refs_8_), channel_id=1, source_target_pairs={{0,2},{2,0},{1,3},{3,1},{4,6},{6,4},{5,7},{7,5},{8,10},{10,8},{9,1... | collective-permute-start | bytes 1572872 | tf_op jit(solution)/shard_map/ppermute | solution.py:891
  71.1 18.2 %collective-permute-done.23.refs_10_ = bf16[512,256]{1,0:T(8,128)(2,1)S(1)} collective-permute-done((bf16[512,256]{1,0:T(8,128)(2,1)S(1)}, bf16[512,256]{1,0:T(8,128)(2,1)S(1)}, u32[]{:S(2)}, u32[]{:S(2)}) %collective-permute-start.23) | collective-permute-done | bytes 262176 | tf_op jit(solution)/shard_map/ppermute | solution.py:894
  89.2 0.5 collective-permute-start.24
  89.8 4.4 %shard_map.201 = (bf16[256,128]{1,0:T(8,128)(2,1)}, bf16[256,128]{1,0:T(8,128)(2,1)}, bf16[256,128]{1,0:T(8,128)(2,1)}, bf16[256,128]{1,0:T(8,128)(2,1)}) custom-call(bf16[2,256,384]{2,1,0:T(8,128)(2,1)S(1)} %get-tuple-element.38.fine_ref, f32[2,256,48]{2,1,0:T(8,128)S(1)} %get-tuple-element.39.ext_ref, f32[1,256]{1,0:T(1,128)S(1)} %bitcast.32), custom_call_target="tpu_custom_call" | custom-call | tf_op jit(solution)/shard_map/pallas_call | solution.py:371
  94.2 1.6 %collective-permute-start.25 = (bf16[512,256]{1,0:T(8,128)(2,1)S(1)}, bf16[512,256]{1,0:T(8,128)(2,1)S(1)}, u32[]{:S(2)}, u32[]{:S(2)}) collective-permute-start(bf16[512,256]{1,0:T(8,128)(2,1)S(1)} %collective-permute-done.23.refs_10_), channel_id=1, source_target_pairs={{0,2},{2,0},{1,3},{3,1},{4,6},{6,4},{5,7},{7,5},{8,10},{10,8},{9,1... | collective-permute-start | bytes 786440 | tf_op jit(solution)/shard_map/ppermute | solution.py:891
  95.7 0.8 collective-permute-done.24.refs_11_
  96.6 1.5 %collective-permute-start.26 = (bf16[512,256]{1,0:T(8,128)(2,1)S(1)}, bf16[512,256]{1,0:T(8,128)(2,1)S(1)}, u32[]{:S(2)}, u32[]{:S(2)}) collective-permute-start(bf16[512,256]{1,0:T(8,128)(2,1)S(1)} %collective-permute-done.24.refs_11_), channel_id=1, source_target_pairs={{0,2},{2,0},{1,3},{3,1},{4,6},{6,4},{5,7},{7,5},{8,10},{10,8},{9,1... | collective-permute-start | bytes 786440 | tf_op jit(solution)/shard_map/ppermute | solution.py:891
  98.1 1.4 %collective-permute-start.15 = (bf16[256,128]{1,0:T(8,128)(2,1)}, bf16[256,128]{1,0:T(8,128)(2,1)S(1)}, u32[]{:S(2)}, u32[]{:S(2)}) collective-permute-start(bf16[256,128]{1,0:T(8,128)(2,1)} %get-tuple-element.42), channel_id=1, source_target_pairs={{0,12},{4,0},{8,4},{12,8},{1,13},{5,1},{9,5},{13,9},{2,14},{6,2},{... | collective-permute-start | bytes 196616 | tf_op jit(solution)/shard_map/ppermute | solution.py:894
  99.5 4.2 %shard_map.202 = (bf16[256,128]{1,0:T(8,128)(2,1)S(1)}, bf16[256,128]{1,0:T(8,128)(2,1)S(1)}, bf16[256,128]{1,0:T(8,128)(2,1)S(1)}, bf16[256,128]{1,0:T(8,128)(2,1)S(1)}) custom-call(bf16[4,384,128]{2,1,0:T(8,128)(2,1)} %copy-done.9, bf16[4,384,128]{2,1,0:T(8,128)(2,1)S(1)} %collective-permute-done.18.their_ref, ...), custom_call_target="tpu_custom_call" | custom-call | tf_op jit(solution)/shard_map/pallas_call | solution.py:371
  103.7 0.7 collective-permute-start.17
  104.4 3.2 %collective-permute-start.19 = (bf16[256,128]{1,0:T(8,128)(2,1)S(1)}, bf16[256,128]{1,0:T(8,128)(2,1)S(1)}, u32[]{:S(2)}, u32[]{:S(2)}) collective-permute-start(bf16[256,128]{1,0:T(8,128)(2,1)S(1)} %get-tuple-element.51), channel_id=1, source_target_pairs={{0,12},{4,0},{8,4},{12,8},{1,13},{5,1},{9,5},{13,9},{2,14},{6,2},{... | collective-permute-start | bytes 196616 | tf_op jit(solution)/shard_map/ppermute | solution.py:894
  107.6 0.9 collective-permute-done.26.refs_13_
  108.7 1.8 %collective-permute-start.21 = (bf16[256,128]{1,0:T(8,128)(2,1)S(1)}, bf16[256,128]{1,0:T(8,128)(2,1)S(1)}, u32[]{:S(2)}, u32[]{:S(2)}) collective-permute-start(bf16[256,128]{1,0:T(8,128)(2,1)S(1)} %get-tuple-element.53), channel_id=1, source_target_pairs={{0,4},{4,8},{8,12},{12,0},{1,5},{5,9},{9,13},{13,1},{2,6},{6,10},{... | collective-permute-start | bytes 196616 | tf_op jit(solution)/shard_map/ppermute | solution.py:894
  110.5 4.7 %collective-permute-done.20.refs_6_ = bf16[256,128]{1,0:T(8,128)(2,1)S(1)} collective-permute-done((bf16[256,128]{1,0:T(8,128)(2,1)S(1)}, bf16[256,128]{1,0:T(8,128)(2,1)S(1)}, u32[]{:S(2)}, u32[]{:S(2)}) %collective-permute-start.20) | collective-permute-done | bytes 65568 | tf_op jit(solution)/shard_map/ppermute | solution.py:894
  115.2 0.9 shard_map.203
  116.1 1.5 %collective-permute-done.27 = bf16[2,128,512]{2,1,0:T(8,128)(2,1)S(1)} collective-permute-done((bf16[2,128,512]{2,1,0:T(8,128)(2,1)S(1)}, bf16[2,128,512]{2,1,0:T(8,128)(2,1)S(1)}, u32[]{:S(2)}, u32[]{:S(2)}) %collective-permute-start.27) | collective-permute-done | bytes 262176 | tf_op jit(solution)/shard_map/ppermute | solution.py:891
  118.0 1.0 collective-permute-done.29
  119.2 2.1 %collective-permute-start.28 = (bf16[128,512]{1,0:T(8,128)(2,1)S(1)}, bf16[128,512]{1,0:T(8,128)(2,1)S(1)}, u32[]{:S(2)}, u32[]{:S(2)}) collective-permute-start(bf16[128,512]{1,0:T(8,128)(2,1)S(1)} %dynamic-slice_bitcast_fusion), channel_id=1, source_target_pairs={{0,4},{4,0},{8,12},{12,8},{1,5},{5,1},{9,13},{13,9},{2,6},{6,2},{1... | collective-permute-start | bytes 393224 | tf_op jit(solution)/shard_map/ppermute | solution.py:984
  121.3 1.5 %collective-permute-done.30 = f32[128]{0:T(128)S(1)} collective-permute-done((f32[128]{0:T(128)S(1)}, f32[128]{0:T(128)S(1)}, u32[]{:S(2)}, u32[]{:S(2)}) %collective-permute-start.30) | collective-permute-done | bytes 544 | tf_op jit(solution)/shard_map/ppermute | solution.py:984
  122.8 2.0 %collective-permute-done.28 = bf16[128,512]{1,0:T(8,128)(2,1)S(1)} collective-permute-done((bf16[128,512]{1,0:T(8,128)(2,1)S(1)}, bf16[128,512]{1,0:T(8,128)(2,1)S(1)}, u32[]{:S(2)}, u32[]{:S(2)}) %collective-permute-start.28) | collective-permute-done | bytes 131104 | tf_op jit(solution)/shard_map/ppermute | solution.py:984
  124.9 0.8 fusion.1
  (107 shorter events, 1.9 us)
Async XLA Ops:
  2.3 6.5 %copy-start = (bf16[2,64,2048]{2,1,0:T(8,128)(2,1)S(1)}, bf16[2,64,2048]{2,1,0:T(8,128)(2,1)}, u32[]{:S(2)}) copy-start(bf16[2,64,2048]{2,1,0:T(8,128)(2,1)} %param.21) | copy-start | bytes 1572868
  2.3 6.5 %copy-start.6 = (f32[2048]{0:T(1024)S(1)}, f32[2048]{0:T(1024)}, u32[]{:S(2)}) copy-start(f32[2048]{0:T(1024)} %param.22) | copy-start | bytes 24580
  2.3 32.7 %all-to-all-start = ((bf16[4,128,512]{2,1,0:T(8,128)(2,1)}), bf16[4,128,512]{2,1,0:T(8,128)(2,1)S(1)}, u32[]{:S(2)}, u32[]{:S(2)}) async-start(bf16[4,128,512]{2,1,0:T(8,128)(2,1)} %get-tuple-element.31), calls=%async_computation | async-start | bytes 1048576 | tf_op jit(solution)/shard_map/all_to_all | solution.py:888
  9.2 26.0 %copy-start.1 = (bf16[128,1024]{1,0:T(8,128)(2,1)}, bf16[128,1024]{1,0:T(8,128)(2,1)S(1)}, u32[]{:S(2)}) copy-start(bf16[128,1024]{1,0:T(8,128)(2,1)S(1)} %get-tuple-element.33.refs_0_) | copy-start | bytes 786436
  9.2 26.0 %copy-start.2 = (bf16[128,1024]{1,0:T(8,128)(2,1)}, bf16[128,1024]{1,0:T(8,128)(2,1)S(1)}, u32[]{:S(2)}) copy-start(bf16[128,1024]{1,0:T(8,128)(2,1)S(1)} %get-tuple-element.35.refs_4_) | copy-start | bytes 786436
  9.2 25.3 %collective-permute-start.1 = (bf16[128,1024]{1,0:T(8,128)(2,1)S(1)}, bf16[128,1024]{1,0:T(8,128)(2,1)S(1)}, u32[]{:S(2)}, u32[]{:S(2)}) collective-permute-start(bf16[128,1024]{1,0:T(8,128)(2,1)S(1)} %get-tuple-element.33.refs_0_), channel_id=1, source_target_pairs={{0,8},{4,12},{8,0},{12,4},{1,9},{5,13},{9,1},{13,5},{2,10},{6,14},... | collective-permute-start | bytes 786440 | tf_op jit(solution)/shard_map/ppermute | solution.py:894
  12.2 22.4 %collective-permute-start = (bf16[128,1024]{1,0:T(8,128)(2,1)S(1)}, bf16[128,1024]{1,0:T(8,128)(2,1)S(1)}, u32[]{:S(2)}, u32[]{:S(2)}) collective-permute-start(bf16[128,1024]{1,0:T(8,128)(2,1)S(1)} %get-tuple-element.33.refs_0_), channel_id=1, source_target_pairs={{0,4},{4,0},{8,12},{12,8},{1,5},{5,1},{9,13},{13,9},{2,6},{6,2},{1... | collective-permute-start | bytes 786440 | tf_op jit(solution)/shard_map/ppermute | solution.py:908
  13.6 5.0 %collective-permute-start.9 = (bf16[128,512]{1,0:T(8,128)(2,1)S(1)}, bf16[128,512]{1,0:T(8,128)(2,1)S(1)}, u32[]{:S(2)}, u32[]{:S(2)}) collective-permute-start(bf16[128,512]{1,0:T(8,128)(2,1)S(1)} %copy-done.31), channel_id=1, source_target_pairs={{0,16},{16,0},{1,17},{17,1},{2,18},{18,2},{3,19},{19,3},{4,20},{20... | collective-permute-start | bytes 393224 | tf_op jit(solution)/shard_map/ppermute | solution.py:891
  15.2 20.9 %collective-permute-start.6 = (bf16[128,512]{1,0:T(8,128)(2,1)S(1)}, bf16[128,512]{1,0:T(8,128)(2,1)S(1)}, u32[]{:S(2)}, u32[]{:S(2)}) collective-permute-start(bf16[128,512]{1,0:T(8,128)(2,1)S(1)} %copy-done.31), channel_id=1, source_target_pairs={{0,2},{2,0},{1,3},{3,1},{4,6},{6,4},{5,7},{7,5},{8,10},{10,8},{9,1... | collective-permute-start | bytes 393224 | tf_op jit(solution)/shard_map/ppermute | solution.py:891
  18.6 16.6 %copy-start.24 = (bf16[128,512]{1,0:T(8,128)(2,1)}, bf16[128,512]{1,0:T(8,128)(2,1)S(1)}, u32[]{:S(2)}) copy-start(bf16[128,512]{1,0:T(8,128)(2,1)S(1)} %collective-permute-done.9.refs_12_) | copy-start | bytes 393220
  18.6 19.0 %collective-permute-start.12 = (bf16[128,512]{1,0:T(8,128)(2,1)S(1)}, bf16[128,512]{1,0:T(8,128)(2,1)S(1)}, u32[]{:S(2)}, u32[]{:S(2)}) collective-permute-start(bf16[128,512]{1,0:T(8,128)(2,1)S(1)} %collective-permute-done.9.refs_12_), channel_id=1, source_target_pairs={{0,2},{2,0},{1,3},{3,1},{4,6},{6,4},{5,7},{7,5},{8,10},{10,8},{9,1... | collective-permute-start | bytes 393224 | tf_op jit(solution)/shard_map/ppermute | solution.py:891
  34.5 7.3 %collective-permute-start.2 = (bf16[128,1024]{1,0:T(8,128)(2,1)S(1)}, bf16[128,1024]{1,0:T(8,128)(2,1)S(1)}, u32[]{:S(2)}, u32[]{:S(2)}) collective-permute-start(bf16[128,1024]{1,0:T(8,128)(2,1)S(1)} %collective-permute-done.1.refs_2_), channel_id=1, source_target_pairs={{0,4},{4,0},{8,12},{12,8},{1,5},{5,1},{9,13},{13,9},{2,6},{6,2},{1... | collective-permute-start | bytes 786440 | tf_op jit(solution)/shard_map/ppermute | solution.py:908
  34.5 9.4 %collective-permute-start.4 = (bf16[128,1024]{1,0:T(8,128)(2,1)S(1)}, bf16[128,1024]{1,0:T(8,128)(2,1)S(1)}, u32[]{:S(2)}, u32[]{:S(2)}) collective-permute-start(bf16[128,1024]{1,0:T(8,128)(2,1)S(1)} %collective-permute-done.1.refs_2_), channel_id=1, source_target_pairs={{0,1},{1,0},{2,3},{3,2},{4,5},{5,4},{6,7},{7,6},{8,9},{9,8},{10,11... | collective-permute-start | bytes 786440 | tf_op jit(solution)/shard_map/ppermute | solution.py:891
  34.6 11.0 %collective-permute-start.3 = (bf16[128,1024]{1,0:T(8,128)(2,1)S(1)}, bf16[128,1024]{1,0:T(8,128)(2,1)S(1)}, u32[]{:S(2)}, u32[]{:S(2)}) collective-permute-start(bf16[128,1024]{1,0:T(8,128)(2,1)S(1)} %collective-permute-done.refs_1_), channel_id=1, source_target_pairs={{0,1},{1,0},{2,3},{3,2},{4,5},{5,4},{6,7},{7,6},{8,9},{9,8},{10,11... | collective-permute-start | bytes 786440 | tf_op jit(solution)/shard_map/ppermute | solution.py:891
  36.0 5.9 %copy-start.25 = (bf16[128,512]{1,0:T(8,128)(2,1)}, bf16[128,512]{1,0:T(8,128)(2,1)S(1)}, u32[]{:S(2)}) copy-start(bf16[128,512]{1,0:T(8,128)(2,1)S(1)} %collective-permute-done.6.refs_9_) | copy-start | bytes 393220
  36.0 11.0 %collective-permute-start.10 = (bf16[192,512]{1,0:T(8,128)(2,1)}, bf16[192,512]{1,0:T(8,128)(2,1)S(1)}, u32[]{:S(2)}, u32[]{:S(2)}) collective-permute-start(bf16[192,512]{1,0:T(8,128)(2,1)} %get-tuple-element.62), channel_id=1, source_target_pairs={{0,16},{16,0},{1,17},{17,1},{2,18},{18,2},{3,19},{19,3},{4,20},{20... | collective-permute-start | bytes 589832 | tf_op jit(solution)/shard_map/ppermute | solution.py:891
  38.3 9.3 %collective-permute-start.8 = (bf16[192,512]{1,0:T(8,128)(2,1)}, bf16[192,512]{1,0:T(8,128)(2,1)S(1)}, u32[]{:S(2)}, u32[]{:S(2)}) collective-permute-start(bf16[192,512]{1,0:T(8,128)(2,1)} %get-tuple-element.61), channel_id=1, source_target_pairs={{0,2},{2,0},{1,3},{3,1},{4,6},{6,4},{5,7},{7,5},{8,10},{10,8},{9,1... | collective-permute-start | bytes 589832 | tf_op jit(solution)/shard_map/ppermute | solution.py:891
  41.9 6.4 %collective-permute-start.5 = (bf16[128,1024]{1,0:T(8,128)(2,1)S(1)}, bf16[128,1024]{1,0:T(8,128)(2,1)S(1)}, u32[]{:S(2)}, u32[]{:S(2)}) collective-permute-start(bf16[128,1024]{1,0:T(8,128)(2,1)S(1)} %collective-permute-done.2.refs_3_), channel_id=1, source_target_pairs={{0,1},{1,0},{2,3},{3,2},{4,5},{5,4},{6,7},{7,6},{8,9},{9,8},{10,11... | collective-permute-start | bytes 786440 | tf_op jit(solution)/shard_map/ppermute | solution.py:891
  41.9 6.2 %copy-start.16 = (bf16[512,256]{1,0:T(8,128)(2,1)S(1)}, bf16[512,256]{1,0:T(8,128)(2,1)}, u32[]{:S(2)}) copy-start(bf16[512,256]{1,0:T(8,128)(2,1)} %param.37) | copy-start | bytes 786436
  41.9 6.2 %copy-start.17 = (bf16[512,256]{1,0:T(8,128)(2,1)S(1)}, bf16[512,256]{1,0:T(8,128)(2,1)}, u32[]{:S(2)}) copy-start(bf16[512,256]{1,0:T(8,128)(2,1)} %param.38) | copy-start | bytes 786436
  44.0 8.0 %collective-permute-start.11 = (bf16[192,512]{1,0:T(8,128)(2,1)}, bf16[192,512]{1,0:T(8,128)(2,1)S(1)}, u32[]{:S(2)}, u32[]{:S(2)}) collective-permute-start(bf16[192,512]{1,0:T(8,128)(2,1)} %get-tuple-element.61), channel_id=1, source_target_pairs={{0,16},{16,0},{1,17},{17,1},{2,18},{18,2},{3,19},{19,3},{4,20},{20... | collective-permute-start | bytes 589832 | tf_op jit(solution)/shard_map/ppermute | solution.py:891
  45.5 8.0 %collective-permute-start.7 = (bf16[192,512]{1,0:T(8,128)(2,1)}, bf16[192,512]{1,0:T(8,128)(2,1)S(1)}, u32[]{:S(2)}, u32[]{:S(2)}) collective-permute-start(bf16[192,512]{1,0:T(8,128)(2,1)} %get-tuple-element.62), channel_id=1, source_target_pairs={{0,2},{2,0},{1,3},{3,1},{4,6},{6,4},{5,7},{7,5},{8,10},{10,8},{9,1... | collective-permute-start | bytes 589832 | tf_op jit(solution)/shard_map/ppermute | solution.py:891
  47.0 9.9 %collective-permute-start.13 = (bf16[192,512]{1,0:T(8,128)(2,1)S(1)}, bf16[192,512]{1,0:T(8,128)(2,1)S(1)}, u32[]{:S(2)}, u32[]{:S(2)}) collective-permute-start(bf16[192,512]{1,0:T(8,128)(2,1)S(1)} %collective-permute-done.10.refs_13_), channel_id=1, source_target_pairs={{0,2},{2,0},{1,3},{3,1},{4,6},{6,4},{5,7},{7,5},{8,10},{10,8},{9,1... | collective-permute-start | bytes 589832 | tf_op jit(solution)/shard_map/ppermute | solution.py:891
  47.6 9.4 %collective-permute-start.14 = (bf16[192,512]{1,0:T(8,128)(2,1)S(1)}, bf16[192,512]{1,0:T(8,128)(2,1)S(1)}, u32[]{:S(2)}, u32[]{:S(2)}) collective-permute-start(bf16[192,512]{1,0:T(8,128)(2,1)S(1)} %collective-permute-done.8.refs_11_), channel_id=1, source_target_pairs={{0,16},{16,0},{1,17},{17,1},{2,18},{18,2},{3,19},{19,3},{4,20},{20... | collective-permute-start | bytes 589832 | tf_op jit(solution)/shard_map/ppermute | solution.py:891
  48.3 8.7 %copy-start.15 = (bf16[128,1024]{1,0:T(8,128)(2,1)}, bf16[128,1024]{1,0:T(8,128)(2,1)S(1)}, u32[]{:S(2)}) copy-start(bf16[128,1024]{1,0:T(8,128)(2,1)S(1)} %collective-permute-done.5.refs_7_) | copy-start | bytes 786436
  52.0 5.0 %copy-start.20 = (bf16[192,512]{1,0:T(8,128)(2,1)}, bf16[192,512]{1,0:T(8,128)(2,1)S(1)}, u32[]{:S(2)}) copy-start(bf16[192,512]{1,0:T(8,128)(2,1)S(1)} %collective-permute-done.11.refs_14_) | copy-start | bytes 589828
  63.1 31.0 %all-to-all-start.1 = ((bf16[4,384,128]{2,1,0:T(8,128)(2,1)}), bf16[4,384,128]{2,1,0:T(8,128)(2,1)S(1)}, u32[]{:S(2)}, u32[]{:S(2)}) async-start(bf16[4,384,128]{2,1,0:T(8,128)(2,1)} %get-tuple-element.45), calls=%async_computation.1 | async-start | bytes 786432 | tf_op jit(solution)/shard_map/all_to_all | solution.py:888
  66.7 22.6 %collective-permute-start.23 = (bf16[512,256]{1,0:T(8,128)(2,1)S(1)}, bf16[512,256]{1,0:T(8,128)(2,1)S(1)}, u32[]{:S(2)}, u32[]{:S(2)}) collective-permute-start(bf16[512,256]{1,0:T(8,128)(2,1)S(1)} %constant_dynamic-slice_fusion.2), channel_id=1, source_target_pairs={{0,8},{4,12},{8,0},{12,4},{1,9},{5,13},{9,1},{13,5},{2,10},{6,14},... | collective-permute-start | bytes 786440 | tf_op jit(solution)/shard_map/ppermute | solution.py:894
  69.6 34.8 %collective-permute-start.22 = (bf16[1024,256]{1,0:T(8,128)(2,1)S(1)}, bf16[1024,256]{1,0:T(8,128)(2,1)S(1)}, u32[]{:S(2)}, u32[]{:S(2)}) collective-permute-start(bf16[1024,256]{1,0:T(8,128)(2,1)S(1)} %pad_maximum_fusion.refs_8_), channel_id=1, source_target_pairs={{0,2},{2,0},{1,3},{3,1},{4,6},{6,4},{5,7},{7,5},{8,10},{10,8},{9,1... | collective-permute-start | bytes 1572872 | tf_op jit(solution)/shard_map/ppermute | solution.py:891
  89.2 7.3 %collective-permute-start.24 = (bf16[512,256]{1,0:T(8,128)(2,1)S(1)}, bf16[512,256]{1,0:T(8,128)(2,1)S(1)}, u32[]{:S(2)}, u32[]{:S(2)}) collective-permute-start(bf16[512,256]{1,0:T(8,128)(2,1)S(1)} %collective-permute-done.23.refs_10_), channel_id=1, source_target_pairs={{0,16},{16,0},{1,17},{17,1},{2,18},{18,2},{3,19},{19,3},{4,20},{20... | collective-permute-start | bytes 786440 | tf_op jit(solution)/shard_map/ppermute | solution.py:891
  89.8 9.7 %copy-start.3 = (f32[256,64]{1,0:T(8,128)S(1)}, f32[256,64]{1,0:T(8,128)}, u32[]{:S(2)}) copy-start(f32[256,64]{1,0:T(8,128)} %constant.53.clone.cos_ref) | copy-start | bytes 196612
  89.8 9.7 %copy-start.4 = (f32[256,64]{1,0:T(8,128)S(1)}, f32[256,64]{1,0:T(8,128)}, u32[]{:S(2)}) copy-start(f32[256,64]{1,0:T(8,128)} %constant.54.clone.sin_ref) | copy-start | bytes 196612
  94.1 5.4 %copy-start.9 = (bf16[4,384,128]{2,1,0:T(8,128)(2,1)}, bf16[4,384,128]{2,1,0:T(8,128)(2,1)S(1)}, u32[]{:S(2)}) copy-start(bf16[4,384,128]{2,1,0:T(8,128)(2,1)S(1)} %all-to-all-done.1.mine_ref) | copy-start | bytes 1179652
  94.1 5.4 %collective-permute-start.18 = (bf16[4,384,128]{2,1,0:T(8,128)(2,1)S(1)}, bf16[4,384,128]{2,1,0:T(8,128)(2,1)S(1)}, u32[]{:S(2)}, u32[]{:S(2)}) collective-permute-start(bf16[4,384,128]{2,1,0:T(8,128)(2,1)S(1)} %all-to-all-done.1.mine_ref), channel_id=1, source_target_pairs={{0,1},{1,0},{2,3},{3,2},{4,5},{5,4},{6,7},{7,6},{8,9},{9,8},{10,11... | collective-permute-start | bytes 1179656 | tf_op jit(solution)/shard_map/ppermute | solution.py:891
  94.2 9.5 %collective-permute-start.25 = (bf16[512,256]{1,0:T(8,128)(2,1)S(1)}, bf16[512,256]{1,0:T(8,128)(2,1)S(1)}, u32[]{:S(2)}, u32[]{:S(2)}) collective-permute-start(bf16[512,256]{1,0:T(8,128)(2,1)S(1)} %collective-permute-done.23.refs_10_), channel_id=1, source_target_pairs={{0,2},{2,0},{1,3},{3,1},{4,6},{6,4},{5,7},{7,5},{8,10},{10,8},{9,1... | collective-permute-start | bytes 786440 | tf_op jit(solution)/shard_map/ppermute | solution.py:891
  96.6 11.9 %collective-permute-start.26 = (bf16[512,256]{1,0:T(8,128)(2,1)S(1)}, bf16[512,256]{1,0:T(8,128)(2,1)S(1)}, u32[]{:S(2)}, u32[]{:S(2)}) collective-permute-start(bf16[512,256]{1,0:T(8,128)(2,1)S(1)} %collective-permute-done.24.refs_11_), channel_id=1, source_target_pairs={{0,2},{2,0},{1,3},{3,1},{4,6},{6,4},{5,7},{7,5},{8,10},{10,8},{9,1... | collective-permute-start | bytes 786440 | tf_op jit(solution)/shard_map/ppermute | solution.py:891
  98.1 10.6 %collective-permute-start.15 = (bf16[256,128]{1,0:T(8,128)(2,1)}, bf16[256,128]{1,0:T(8,128)(2,1)S(1)}, u32[]{:S(2)}, u32[]{:S(2)}) collective-permute-start(bf16[256,128]{1,0:T(8,128)(2,1)} %get-tuple-element.42), channel_id=1, source_target_pairs={{0,12},{4,0},{8,4},{12,8},{1,13},{5,1},{9,5},{13,9},{2,14},{6,2},{... | collective-permute-start | bytes 196616 | tf_op jit(solution)/shard_map/ppermute | solution.py:894
  99.5 11.0 %collective-permute-start.16 = (bf16[256,128]{1,0:T(8,128)(2,1)}, bf16[256,128]{1,0:T(8,128)(2,1)S(1)}, u32[]{:S(2)}, u32[]{:S(2)}) collective-permute-start(bf16[256,128]{1,0:T(8,128)(2,1)} %get-tuple-element.43), channel_id=1, source_target_pairs={{0,8},{4,12},{8,0},{12,4},{1,9},{5,13},{9,1},{13,5},{2,10},{6,14},... | collective-permute-start | bytes 196616 | tf_op jit(solution)/shard_map/ppermute | solution.py:894
  99.5 15.7 %copy-start.5 = (bf16[256,128]{1,0:T(8,128)(2,1)S(1)}, bf16[256,128]{1,0:T(8,128)(2,1)}, u32[]{:S(2)}) copy-start(bf16[256,128]{1,0:T(8,128)(2,1)} %get-tuple-element.41.refs_0_) | copy-start | bytes 196612
  103.7 6.8 %collective-permute-start.17 = (bf16[256,128]{1,0:T(8,128)(2,1)S(1)}, bf16[256,128]{1,0:T(8,128)(2,1)S(1)}, u32[]{:S(2)}, u32[]{:S(2)}) collective-permute-start(bf16[256,128]{1,0:T(8,128)(2,1)S(1)} %copy-done.32), channel_id=1, source_target_pairs={{0,4},{4,8},{8,12},{12,0},{1,5},{5,9},{9,13},{13,1},{2,6},{6,10},{... | collective-permute-start | bytes 196616 | tf_op jit(solution)/shard_map/ppermute | solution.py:894
  104.4 10.8 %copy-start.7 = (f32[1024]{0:T(1024)S(1)}, f32[1024]{0:T(1024)}, u32[]{:S(2)}) copy-start(f32[1024]{0:T(1024)} %param.39) | copy-start | bytes 12292
  104.4 6.1 %collective-permute-start.19 = (bf16[256,128]{1,0:T(8,128)(2,1)S(1)}, bf16[256,128]{1,0:T(8,128)(2,1)S(1)}, u32[]{:S(2)}, u32[]{:S(2)}) collective-permute-start(bf16[256,128]{1,0:T(8,128)(2,1)S(1)} %get-tuple-element.51), channel_id=1, source_target_pairs={{0,12},{4,0},{8,4},{12,8},{1,13},{5,1},{9,5},{13,9},{2,14},{6,2},{... | collective-permute-start | bytes 196616 | tf_op jit(solution)/shard_map/ppermute | solution.py:894
  108.5 6.7 %collective-permute-start.20 = (bf16[256,128]{1,0:T(8,128)(2,1)S(1)}, bf16[256,128]{1,0:T(8,128)(2,1)S(1)}, u32[]{:S(2)}, u32[]{:S(2)}) collective-permute-start(bf16[256,128]{1,0:T(8,128)(2,1)S(1)} %get-tuple-element.52), channel_id=1, source_target_pairs={{0,8},{4,12},{8,0},{12,4},{1,9},{5,13},{9,1},{13,5},{2,10},{6,14},... | collective-permute-start | bytes 196616 | tf_op jit(solution)/shard_map/ppermute | solution.py:894
  108.7 6.5 %collective-permute-start.21 = (bf16[256,128]{1,0:T(8,128)(2,1)S(1)}, bf16[256,128]{1,0:T(8,128)(2,1)S(1)}, u32[]{:S(2)}, u32[]{:S(2)}) collective-permute-start(bf16[256,128]{1,0:T(8,128)(2,1)S(1)} %get-tuple-element.53), channel_id=1, source_target_pairs={{0,4},{4,8},{8,12},{12,0},{1,5},{5,9},{9,13},{13,1},{2,6},{6,10},{... | collective-permute-start | bytes 196616 | tf_op jit(solution)/shard_map/ppermute | solution.py:894
  116.1 1.6 %collective-permute-start.27 = (bf16[2,128,512]{2,1,0:T(8,128)(2,1)S(1)}, bf16[2,128,512]{2,1,0:T(8,128)(2,1)S(1)}, u32[]{:S(2)}, u32[]{:S(2)}) collective-permute-start(bf16[2,128,512]{2,1,0:T(8,128)(2,1)S(1)} %get-tuple-element.55), channel_id=1, source_target_pairs={{0,1},{1,0},{2,3},{3,2},{4,5},{5,4},{6,7},{7,6},{8,9},{9,8},{10,11... | collective-permute-start | bytes 786440 | tf_op jit(solution)/shard_map/ppermute | solution.py:891
  117.8 1.2 collective-permute-start.29
  119.1 3.6 %collective-permute-start.30 = (f32[128]{0:T(128)S(1)}, f32[128]{0:T(128)S(1)}, u32[]{:S(2)}, u32[]{:S(2)}) collective-permute-start(f32[128]{0:T(128)S(1)} %fusion.7), channel_id=1, source_target_pairs={{0,4},{4,0},{8,12},{12,8},{1,5},{5,1},{9,13},{13,9},{2,6},{6,2},{1... | collective-permute-start | bytes 1544 | tf_op jit(solution)/shard_map/ppermute | solution.py:984
  119.2 5.6 %collective-permute-start.28 = (bf16[128,512]{1,0:T(8,128)(2,1)S(1)}, bf16[128,512]{1,0:T(8,128)(2,1)S(1)}, u32[]{:S(2)}, u32[]{:S(2)}) collective-permute-start(bf16[128,512]{1,0:T(8,128)(2,1)S(1)} %dynamic-slice_bitcast_fusion), channel_id=1, source_target_pairs={{0,4},{4,0},{8,12},{12,8},{1,5},{5,1},{9,13},{13,9},{2,6},{6,2},{1... | collective-permute-start | bytes 393224 | tf_op jit(solution)/shard_map/ppermute | solution.py:984
  (18 other events, 42.6 us)

commit v2 on v1

--- a/solution.py
+++ b/solution.py
@@ -745,7 +745,7 @@
         for s in range(sp_size):
             own, other = mine_ref[s], their_ref[s]
             pairs += [jnp.where(first, own, other), jnp.where(first, other, own)]
-        joins = []
+        joins, held = [], []
         for n in range(seq_count):
             q_parts = [unpack(p, n, 0, q_cols) for p in pairs]
             kv_parts = [unpack(p, n, rows * q_cols // 128, kv_cols) for p in pairs]
@@ -763,7 +763,6 @@
             raw = ext_ref[n, :, :ROPE].astype(jnp.bfloat16).astype(jnp.float32)
             back = jnp.concatenate([raw[:, ROPE // 2 :], raw[:, : ROPE // 2]], axis=1)
             key_turn = (raw * cosine[:, :ROPE] + back * sine[:, :ROPE]).astype(jnp.bfloat16)
-            results = []
             for h in range(heads):
                 key_plain = kv_all[:, h * (NOPE + VDIM) : h * (NOPE + VDIM) + NOPE]
                 values = kv_all[:, h * (NOPE + VDIM) + NOPE : (h + 1) * (NOPE + VDIM)]
@@ -771,12 +770,16 @@
                     dot_t(plain[:, h * NOPE : (h + 1) * NOPE], key_plain)
                     + dot_t(turned[:, h * ROPE : (h + 1) * ROPE], key_turn)
                 ) * scale
-                logits = jnp.where(allowed, logits, -jnp.inf)
-                peak = jnp.max(logits, axis=-1, keepdims=True)
-                weights = jnp.exp(logits - peak)
-                total = jnp.sum(weights, axis=-1, keepdims=True)
-                results.append(dot32(weights.astype(jnp.bfloat16), values) / total)
-            joined = jnp.concatenate(results, axis=1).astype(jnp.bfloat16)
+                held.append((jnp.where(allowed, logits, -jnp.inf), values))
+        peaks = [jnp.max(logits, axis=-1, keepdims=True) for logits, _ in held]
+        weights = [jnp.exp(logits - peak) for (logits, _), peak in zip(held, peaks)]
+        totals = [jnp.sum(w, axis=-1, keepdims=True) for w in weights]
+        mixed = [dot32(w.astype(jnp.bfloat16), v) for w, (_, v) in zip(weights, held)]
+        results = [m / t for m, t in zip(mixed, totals)]
+        for n in range(seq_count):
+            joined = jnp.concatenate(results[n * heads : (n + 1) * heads], axis=1).astype(
+                jnp.bfloat16
+            )
             joins.append((joined[: span // 2], joined[span // 2 :]))
         send_by_pair(out_refs, joins, sp_size)
 

time: 126 us -> 126 us (level)
  transfers between devices with their start and end apart: 33 -> 33, of which waited for: 14 -> 15; matrix products, arithmetic and copies ran while one was open for 1% -> 1% of each run, Pallas kernels for 9% -> 8%
where the time goes in v2:
time: 126 us
  waiting for transfers between devices  58.2 us (46%)
  starting transfers between devices  44.4 us (35%)
  Pallas kernels  18.8 us (15%)
  local copies, waits for them, and re-layouts  2.52 us (2%)
  other arithmetic  1.26 us (1%)
    ppermute x8, waiting for transfers between devices, along(): lax.ppermute(values, 'sp', [(i, (i + step) % sp_size) for i in range(sp_s...  37.1 us
    ppermute x19, starting transfers between devices, swap(): return lax.ppermute(values, axis, [(0, 1), (1, 0)])  17.6 us
    ppermute x19, waiting for transfers between devices, swap(): return lax.ppermute(values, axis, [(0, 1), (1, 0)])  15.6 us
    ppermute x8, starting transfers between devices, along(): lax.ppermute(values, 'sp', [(i, (i + step) % sp_size) for i in range(sp_s...  13.2 us
    pallas_call x5, Pallas kernels, kernel_call(): pl.pallas_call(body, out_shape=jax.tree.map(lambda leaf: result_space(lea...  11.2 us
    all_to_all x2, starting transfers between devices, exchange(): return lax.all_to_all(values, axis, 0, 0, tiled=True)  9.96 us
    pallas_call x1, Pallas kernels, project(): pl.pallas_call(body, out_shape=(pltpu.VMEM((seq_count, span, fine), jnp.b...  5.33 us
    ppermute x2, waiting for transfers between devices, across(): lax.ppermute(pick(values, 1 - side), 'sp', [(i, i ^ 1) for i in range(sp_...  3.47 us
  transfers between devices with their start and end apart: 33, of which 15 were waited for; matrix products, arithmetic and copies ran while one was open for 1% of the time, Pallas kernels for 8%

profile of v2, /device:TPU:0, one launch (start us, length us, event | category | flops | bytes accessed | tf_op | source)
XLA Modules:
  0.0 125.5 jit_solution(8572371609438057541)
XLA Ops:
  0.0 2.3 %outgoing_weights.1 = (bf16[4,128,512]{2,1,0:T(8,128)(2,1)}, bf16[128,512]{1,0:T(8,128)(2,1)}) custom-call(bf16[256,512]{1,0:T(8,128)(2,1)} %refs_0_.1, bf16[256,512]{1,0:T(8,128)(2,1)} %refs_1_.1, bf16[256,512]{1,0:T(8,128)(2,1)} %refs_2_.1, bf16[256,512]{1,0:T(8,128)(2,1)} %refs_3_.1, bf16[256,256]{1,0:T(8,128)(2,1)} %refs_4_.1), custom_call_target="tpu_custom_call" | custom-call | tf_op jit(solution)/shard_map/outgoing_weights/pallas_call | solution.py:422
  2.3 6.5 %all-to-all-start = ((bf16[4,128,512]{2,1,0:T(8,128)(2,1)}), bf16[4,128,512]{2,1,0:T(8,128)(2,1)S(1)}, u32[]{:S(2)}, u32[]{:S(2)}) async-start(bf16[4,128,512]{2,1,0:T(8,128)(2,1)} %get-tuple-element.31), calls=%async_computation | async-start | bytes 1048576 | tf_op jit(solution)/shard_map/all_to_all | solution.py:891
  9.2 3.0 %collective-permute-start.1 = (bf16[128,1024]{1,0:T(8,128)(2,1)S(1)}, bf16[128,1024]{1,0:T(8,128)(2,1)S(1)}, u32[]{:S(2)}, u32[]{:S(2)}) collective-permute-start(bf16[128,1024]{1,0:T(8,128)(2,1)S(1)} %get-tuple-element.33.refs_0_), channel_id=1, source_target_pairs={{0,8},{4,12},{8,0},{12,4},{1,9},{5,13},{9,1},{13,5},{2,10},{6,14},... | collective-permute-start | bytes 786440 | tf_op jit(solution)/shard_map/ppermute | solution.py:897
  12.2 1.5 %collective-permute-start = (bf16[128,1024]{1,0:T(8,128)(2,1)S(1)}, bf16[128,1024]{1,0:T(8,128)(2,1)S(1)}, u32[]{:S(2)}, u32[]{:S(2)}) collective-permute-start(bf16[128,1024]{1,0:T(8,128)(2,1)S(1)} %get-tuple-element.33.refs_0_), channel_id=1, source_target_pairs={{0,4},{4,0},{8,12},{12,8},{1,5},{5,1},{9,13},{13,9},{2,6},{6,2},{1... | collective-permute-start | bytes 786440 | tf_op jit(solution)/shard_map/ppermute | solution.py:911
  13.6 1.5 %collective-permute-start.9 = (bf16[128,512]{1,0:T(8,128)(2,1)S(1)}, bf16[128,512]{1,0:T(8,128)(2,1)S(1)}, u32[]{:S(2)}, u32[]{:S(2)}) collective-permute-start(bf16[128,512]{1,0:T(8,128)(2,1)S(1)} %copy-done.31), channel_id=1, source_target_pairs={{0,16},{16,0},{1,17},{17,1},{2,18},{18,2},{3,19},{19,3},{4,20},{20... | collective-permute-start | bytes 393224 | tf_op jit(solution)/shard_map/ppermute | solution.py:894
  15.2 1.5 %collective-permute-start.6 = (bf16[128,512]{1,0:T(8,128)(2,1)S(1)}, bf16[128,512]{1,0:T(8,128)(2,1)S(1)}, u32[]{:S(2)}, u32[]{:S(2)}) collective-permute-start(bf16[128,512]{1,0:T(8,128)(2,1)S(1)} %copy-done.31), channel_id=1, source_target_pairs={{0,2},{2,0},{1,3},{3,1},{4,6},{6,4},{5,7},{7,5},{8,10},{10,8},{9,1... | collective-permute-start | bytes 393224 | tf_op jit(solution)/shard_map/ppermute | solution.py:894
  16.6 2.0 %collective-permute-done.9.refs_12_ = bf16[128,512]{1,0:T(8,128)(2,1)S(1)} collective-permute-done((bf16[128,512]{1,0:T(8,128)(2,1)S(1)}, bf16[128,512]{1,0:T(8,128)(2,1)S(1)}, u32[]{:S(2)}, u32[]{:S(2)}) %collective-permute-start.9) | collective-permute-done | bytes 131104 | tf_op jit(solution)/shard_map/ppermute | solution.py:894
  18.6 1.5 %collective-permute-start.12 = (bf16[128,512]{1,0:T(8,128)(2,1)S(1)}, bf16[128,512]{1,0:T(8,128)(2,1)S(1)}, u32[]{:S(2)}, u32[]{:S(2)}) collective-permute-start(bf16[128,512]{1,0:T(8,128)(2,1)S(1)} %collective-permute-done.9.refs_12_), channel_id=1, source_target_pairs={{0,2},{2,0},{1,3},{3,1},{4,6},{6,4},{5,7},{7,5},{8,10},{10,8},{9,1... | collective-permute-start | bytes 393224 | tf_op jit(solution)/shard_map/ppermute | solution.py:894
  20.1 14.4 %collective-permute-done.1.refs_2_ = bf16[128,1024]{1,0:T(8,128)(2,1)S(1)} collective-permute-done((bf16[128,1024]{1,0:T(8,128)(2,1)S(1)}, bf16[128,1024]{1,0:T(8,128)(2,1)S(1)}, u32[]{:S(2)}, u32[]{:S(2)}) %collective-permute-start.1) | collective-permute-done | bytes 262176 | tf_op jit(solution)/shard_map/ppermute | solution.py:897
  34.6 0.5 collective-permute-start.3
  35.2 0.8 fusion.8
  36.0 1.6 %collective-permute-start.10 = (bf16[192,512]{1,0:T(8,128)(2,1)}, bf16[192,512]{1,0:T(8,128)(2,1)S(1)}, u32[]{:S(2)}, u32[]{:S(2)}) collective-permute-start(bf16[192,512]{1,0:T(8,128)(2,1)} %get-tuple-element.62), channel_id=1, source_target_pairs={{0,16},{16,0},{1,17},{17,1},{2,18},{18,2},{3,19},{19,3},{4,20},{20... | collective-permute-start | bytes 589832 | tf_op jit(solution)/shard_map/ppermute | solution.py:894
  37.6 0.6 copy-done.26
  38.3 1.5 %collective-permute-start.8 = (bf16[192,512]{1,0:T(8,128)(2,1)}, bf16[192,512]{1,0:T(8,128)(2,1)S(1)}, u32[]{:S(2)}, u32[]{:S(2)}) collective-permute-start(bf16[192,512]{1,0:T(8,128)(2,1)} %get-tuple-element.61), channel_id=1, source_target_pairs={{0,2},{2,0},{1,3},{3,1},{4,6},{6,4},{5,7},{7,5},{8,10},{10,8},{9,1... | collective-permute-start | bytes 589832 | tf_op jit(solution)/shard_map/ppermute | solution.py:894
  39.8 2.1 %collective-permute-done.2.refs_3_ = bf16[128,1024]{1,0:T(8,128)(2,1)S(1)} collective-permute-done((bf16[128,1024]{1,0:T(8,128)(2,1)S(1)}, bf16[128,1024]{1,0:T(8,128)(2,1)S(1)}, u32[]{:S(2)}, u32[]{:S(2)}) %collective-permute-start.2) | collective-permute-done | bytes 262176 | tf_op jit(solution)/shard_map/ppermute | solution.py:911
  41.9 2.0 %shard_map.200 = (bf16[48,2048]{1,0:T(8,128)(2,1)S(1)}, bf16[512,256]{1,0:T(8,128)(2,1)S(1)}, bf16[256,256]{1,0:T(8,128)(2,1)S(1)}) custom-call(bf16[32,2048]{1,0:T(8,128)(2,1)} %bitcast.37, bf16[8,2048]{1,0:T(8,128)(2,1)} %bitcast.38, bf16[8,2048]{1,0:T(8,128)(2,1)} %bitcast.39, bf16[512,768]{1,0:T(8,128)(2,1)} %query_ref.1, bf16[256,1024]{1,0:T(8,128)(2,1)} %latent_ref.1), custom_call_target="tpu_custom_call" | custom-call | tf_op jit(solution)/shard_map/pallas_call | solution.py:371
  44.0 1.6 %collective-permute-start.11 = (bf16[192,512]{1,0:T(8,128)(2,1)}, bf16[192,512]{1,0:T(8,128)(2,1)S(1)}, u32[]{:S(2)}, u32[]{:S(2)}) collective-permute-start(bf16[192,512]{1,0:T(8,128)(2,1)} %get-tuple-element.61), channel_id=1, source_target_pairs={{0,16},{16,0},{1,17},{17,1},{2,18},{18,2},{3,19},{19,3},{4,20},{20... | collective-permute-start | bytes 589832 | tf_op jit(solution)/shard_map/ppermute | solution.py:894
  45.5 1.5 %collective-permute-start.7 = (bf16[192,512]{1,0:T(8,128)(2,1)}, bf16[192,512]{1,0:T(8,128)(2,1)S(1)}, u32[]{:S(2)}, u32[]{:S(2)}) collective-permute-start(bf16[192,512]{1,0:T(8,128)(2,1)} %get-tuple-element.62), channel_id=1, source_target_pairs={{0,2},{2,0},{1,3},{3,1},{4,6},{6,4},{5,7},{7,5},{8,10},{10,8},{9,1... | collective-permute-start | bytes 589832 | tf_op jit(solution)/shard_map/ppermute | solution.py:894
  47.0 0.5 collective-permute-start.13
  47.6 0.6 collective-permute-start.14
  48.3 3.7 %collective-permute-done.11.refs_14_ = bf16[192,512]{1,0:T(8,128)(2,1)S(1)} collective-permute-done((bf16[192,512]{1,0:T(8,128)(2,1)}, bf16[192,512]{1,0:T(8,128)(2,1)S(1)}, u32[]{:S(2)}, u32[]{:S(2)}) %collective-permute-start.11) | collective-permute-done | bytes 196640 | tf_op jit(solution)/shard_map/ppermute | solution.py:894
  52.0 1.5 %collective-permute-done.7.refs_10_ = bf16[192,512]{1,0:T(8,128)(2,1)S(1)} collective-permute-done((bf16[192,512]{1,0:T(8,128)(2,1)}, bf16[192,512]{1,0:T(8,128)(2,1)S(1)}, u32[]{:S(2)}, u32[]{:S(2)}) %collective-permute-start.7) | collective-permute-done | bytes 196640 | tf_op jit(solution)/shard_map/ppermute | solution.py:894
  53.5 3.4 %collective-permute-done.13.refs_16_ = bf16[192,512]{1,0:T(8,128)(2,1)S(1)} collective-permute-done((bf16[192,512]{1,0:T(8,128)(2,1)S(1)}, bf16[192,512]{1,0:T(8,128)(2,1)S(1)}, u32[]{:S(2)}, u32[]{:S(2)}) %collective-permute-start.13) | collective-permute-done | bytes 196640 | tf_op jit(solution)/shard_map/ppermute | solution.py:894
  57.0 0.6 copy-done.22
  57.8 5.3 %project.1 = (bf16[2,256,384]{2,1,0:T(8,128)(2,1)S(1)}, bf16[4,384,128]{2,1,0:T(8,128)(2,1)}, f32[2,256,48]{2,1,0:T(8,128)S(1)}) custom-call(bf16[128,1024]{1,0:T(8,128)(2,1)} %copy-done.1, bf16[128,1024]{1,0:T(8,128)(2,1)} %copy-done.11, bf16[128,1024]{1,0:T(8,128)(2,1)} %copy-done.10, bf16[128,1024]{1,0:T(8,128)(2,1)} %copy-done.12, ...), custom_call_target="tpu_custom_call" | custom-call | tf_op jit(solution)/shard_map/project/pallas_call | solution.py:591
  63.1 3.5 %all-to-all-start.1 = ((bf16[4,384,128]{2,1,0:T(8,128)(2,1)}), bf16[4,384,128]{2,1,0:T(8,128)(2,1)S(1)}, u32[]{:S(2)}, u32[]{:S(2)}) async-start(bf16[4,384,128]{2,1,0:T(8,128)(2,1)} %get-tuple-element.45), calls=%async_computation.1 | async-start | bytes 786432 | tf_op jit(solution)/shard_map/all_to_all | solution.py:891
  66.7 2.9 %collective-permute-start.23 = (bf16[512,256]{1,0:T(8,128)(2,1)S(1)}, bf16[512,256]{1,0:T(8,128)(2,1)S(1)}, u32[]{:S(2)}, u32[]{:S(2)}) collective-permute-start(bf16[512,256]{1,0:T(8,128)(2,1)S(1)} %constant_dynamic-slice_fusion.2), channel_id=1, source_target_pairs={{0,8},{4,12},{8,0},{12,4},{1,9},{5,13},{9,1},{13,5},{2,10},{6,14},... | collective-permute-start | bytes 786440 | tf_op jit(solution)/shard_map/ppermute | solution.py:897
  69.6 1.5 %collective-permute-start.22 = (bf16[1024,256]{1,0:T(8,128)(2,1)S(1)}, bf16[1024,256]{1,0:T(8,128)(2,1)S(1)}, u32[]{:S(2)}, u32[]{:S(2)}) collective-permute-start(bf16[1024,256]{1,0:T(8,128)(2,1)S(1)} %pad_maximum_fusion.refs_8_), channel_id=1, source_target_pairs={{0,2},{2,0},{1,3},{3,1},{4,6},{6,4},{5,7},{7,5},{8,10},{10,8},{9,1... | collective-permute-start | bytes 1572872 | tf_op jit(solution)/shard_map/ppermute | solution.py:894
  71.1 18.2 %collective-permute-done.23.refs_10_ = bf16[512,256]{1,0:T(8,128)(2,1)S(1)} collective-permute-done((bf16[512,256]{1,0:T(8,128)(2,1)S(1)}, bf16[512,256]{1,0:T(8,128)(2,1)S(1)}, u32[]{:S(2)}, u32[]{:S(2)}) %collective-permute-start.23) | collective-permute-done | bytes 262176 | tf_op jit(solution)/shard_map/ppermute | solution.py:897
  89.2 0.5 collective-permute-start.24
  89.8 4.4 %shard_map.201 = (bf16[256,128]{1,0:T(8,128)(2,1)}, bf16[256,128]{1,0:T(8,128)(2,1)}, bf16[256,128]{1,0:T(8,128)(2,1)}, bf16[256,128]{1,0:T(8,128)(2,1)}) custom-call(bf16[2,256,384]{2,1,0:T(8,128)(2,1)S(1)} %get-tuple-element.38.fine_ref, f32[2,256,48]{2,1,0:T(8,128)S(1)} %get-tuple-element.39.ext_ref, f32[1,256]{1,0:T(1,128)S(1)} %bitcast.32), custom_call_target="tpu_custom_call" | custom-call | tf_op jit(solution)/shard_map/pallas_call | solution.py:371
  94.2 1.6 %collective-permute-start.25 = (bf16[512,256]{1,0:T(8,128)(2,1)S(1)}, bf16[512,256]{1,0:T(8,128)(2,1)S(1)}, u32[]{:S(2)}, u32[]{:S(2)}) collective-permute-start(bf16[512,256]{1,0:T(8,128)(2,1)S(1)} %collective-permute-done.23.refs_10_), channel_id=1, source_target_pairs={{0,2},{2,0},{1,3},{3,1},{4,6},{6,4},{5,7},{7,5},{8,10},{10,8},{9,1... | collective-permute-start | bytes 786440 | tf_op jit(solution)/shard_map/ppermute | solution.py:894
  95.7 0.8 collective-permute-done.24.refs_11_
  96.6 1.5 %collective-permute-start.26 = (bf16[512,256]{1,0:T(8,128)(2,1)S(1)}, bf16[512,256]{1,0:T(8,128)(2,1)S(1)}, u32[]{:S(2)}, u32[]{:S(2)}) collective-permute-start(bf16[512,256]{1,0:T(8,128)(2,1)S(1)} %collective-permute-done.24.refs_11_), channel_id=1, source_target_pairs={{0,2},{2,0},{1,3},{3,1},{4,6},{6,4},{5,7},{7,5},{8,10},{10,8},{9,1... | collective-permute-start | bytes 786440 | tf_op jit(solution)/shard_map/ppermute | solution.py:894
  98.1 1.4 %collective-permute-start.15 = (bf16[256,128]{1,0:T(8,128)(2,1)}, bf16[256,128]{1,0:T(8,128)(2,1)S(1)}, u32[]{:S(2)}, u32[]{:S(2)}) collective-permute-start(bf16[256,128]{1,0:T(8,128)(2,1)} %get-tuple-element.42), channel_id=1, source_target_pairs={{0,12},{4,0},{8,4},{12,8},{1,13},{5,1},{9,5},{13,9},{2,14},{6,2},{... | collective-permute-start | bytes 196616 | tf_op jit(solution)/shard_map/ppermute | solution.py:897
  99.5 3.6 %shard_map.202 = (bf16[256,128]{1,0:T(8,128)(2,1)S(1)}, bf16[256,128]{1,0:T(8,128)(2,1)S(1)}, bf16[256,128]{1,0:T(8,128)(2,1)S(1)}, bf16[256,128]{1,0:T(8,128)(2,1)S(1)}) custom-call(bf16[4,384,128]{2,1,0:T(8,128)(2,1)} %copy-done.9, bf16[4,384,128]{2,1,0:T(8,128)(2,1)S(1)} %collective-permute-done.18.their_ref, ...), custom_call_target="tpu_custom_call" | custom-call | tf_op jit(solution)/shard_map/pallas_call | solution.py:371
  103.4 0.5 collective-permute-start.17
  103.9 3.4 %collective-permute-start.19 = (bf16[256,128]{1,0:T(8,128)(2,1)S(1)}, bf16[256,128]{1,0:T(8,128)(2,1)S(1)}, u32[]{:S(2)}, u32[]{:S(2)}) collective-permute-start(bf16[256,128]{1,0:T(8,128)(2,1)S(1)} %get-tuple-element.51), channel_id=1, source_target_pairs={{0,12},{4,0},{8,4},{12,8},{1,13},{5,1},{9,5},{13,9},{2,14},{6,2},{... | collective-permute-start | bytes 196616 | tf_op jit(solution)/shard_map/ppermute | solution.py:897
  107.2 1.2 collective-permute-done.26.refs_13_
  108.5 2.0 %collective-permute-start.21 = (bf16[256,128]{1,0:T(8,128)(2,1)S(1)}, bf16[256,128]{1,0:T(8,128)(2,1)S(1)}, u32[]{:S(2)}, u32[]{:S(2)}) collective-permute-start(bf16[256,128]{1,0:T(8,128)(2,1)S(1)} %get-tuple-element.53), channel_id=1, source_target_pairs={{0,4},{4,8},{8,12},{12,0},{1,5},{5,9},{9,13},{13,1},{2,6},{6,10},{... | collective-permute-start | bytes 196616 | tf_op jit(solution)/shard_map/ppermute | solution.py:897
  110.5 4.5 %collective-permute-done.20.refs_6_ = bf16[256,128]{1,0:T(8,128)(2,1)S(1)} collective-permute-done((bf16[256,128]{1,0:T(8,128)(2,1)S(1)}, bf16[256,128]{1,0:T(8,128)(2,1)S(1)}, u32[]{:S(2)}, u32[]{:S(2)}) %collective-permute-start.20) | collective-permute-done | bytes 65568 | tf_op jit(solution)/shard_map/ppermute | solution.py:897
  115.0 0.9 shard_map.203
  116.0 1.5 %collective-permute-done.27 = bf16[2,128,512]{2,1,0:T(8,128)(2,1)S(1)} collective-permute-done((bf16[2,128,512]{2,1,0:T(8,128)(2,1)S(1)}, bf16[2,128,512]{2,1,0:T(8,128)(2,1)S(1)}, u32[]{:S(2)}, u32[]{:S(2)}) %collective-permute-start.27) | collective-permute-done | bytes 262176 | tf_op jit(solution)/shard_map/ppermute | solution.py:894
  117.9 1.0 collective-permute-done.29
  119.0 2.1 %collective-permute-start.28 = (bf16[128,512]{1,0:T(8,128)(2,1)S(1)}, bf16[128,512]{1,0:T(8,128)(2,1)S(1)}, u32[]{:S(2)}, u32[]{:S(2)}) collective-permute-start(bf16[128,512]{1,0:T(8,128)(2,1)S(1)} %dynamic-slice_bitcast_fusion), channel_id=1, source_target_pairs={{0,4},{4,0},{8,12},{12,8},{1,5},{5,1},{9,13},{13,9},{2,6},{6,2},{1... | collective-permute-start | bytes 393224 | tf_op jit(solution)/shard_map/ppermute | solution.py:987
  121.1 1.5 %collective-permute-done.30 = f32[128]{0:T(128)S(1)} collective-permute-done((f32[128]{0:T(128)S(1)}, f32[128]{0:T(128)S(1)}, u32[]{:S(2)}, u32[]{:S(2)}) %collective-permute-start.30) | collective-permute-done | bytes 544 | tf_op jit(solution)/shard_map/ppermute | solution.py:987
  122.6 2.0 %collective-permute-done.28 = bf16[128,512]{1,0:T(8,128)(2,1)S(1)} collective-permute-done((bf16[128,512]{1,0:T(8,128)(2,1)S(1)}, bf16[128,512]{1,0:T(8,128)(2,1)S(1)}, u32[]{:S(2)}, u32[]{:S(2)}) %collective-permute-start.28) | collective-permute-done | bytes 131104 | tf_op jit(solution)/shard_map/ppermute | solution.py:987
  124.7 0.8 fusion.1
  (107 shorter events, 1.9 us)
Async XLA Ops:
  2.3 6.5 %copy-start = (bf16[2,64,2048]{2,1,0:T(8,128)(2,1)S(1)}, bf16[2,64,2048]{2,1,0:T(8,128)(2,1)}, u32[]{:S(2)}) copy-start(bf16[2,64,2048]{2,1,0:T(8,128)(2,1)} %param.21) | copy-start | bytes 1572868
  2.3 6.5 %copy-start.6 = (f32[2048]{0:T(1024)S(1)}, f32[2048]{0:T(1024)}, u32[]{:S(2)}) copy-start(f32[2048]{0:T(1024)} %param.22) | copy-start | bytes 24580
  2.3 32.7 %all-to-all-start = ((bf16[4,128,512]{2,1,0:T(8,128)(2,1)}), bf16[4,128,512]{2,1,0:T(8,128)(2,1)S(1)}, u32[]{:S(2)}, u32[]{:S(2)}) async-start(bf16[4,128,512]{2,1,0:T(8,128)(2,1)} %get-tuple-element.31), calls=%async_computation | async-start | bytes 1048576 | tf_op jit(solution)/shard_map/all_to_all | solution.py:891
  9.2 26.0 %copy-start.1 = (bf16[128,1024]{1,0:T(8,128)(2,1)}, bf16[128,1024]{1,0:T(8,128)(2,1)S(1)}, u32[]{:S(2)}) copy-start(bf16[128,1024]{1,0:T(8,128)(2,1)S(1)} %get-tuple-element.33.refs_0_) | copy-start | bytes 786436
  9.2 26.0 %copy-start.2 = (bf16[128,1024]{1,0:T(8,128)(2,1)}, bf16[128,1024]{1,0:T(8,128)(2,1)S(1)}, u32[]{:S(2)}) copy-start(bf16[128,1024]{1,0:T(8,128)(2,1)S(1)} %get-tuple-element.35.refs_4_) | copy-start | bytes 786436
  9.2 25.3 %collective-permute-start.1 = (bf16[128,1024]{1,0:T(8,128)(2,1)S(1)}, bf16[128,1024]{1,0:T(8,128)(2,1)S(1)}, u32[]{:S(2)}, u32[]{:S(2)}) collective-permute-start(bf16[128,1024]{1,0:T(8,128)(2,1)S(1)} %get-tuple-element.33.refs_0_), channel_id=1, source_target_pairs={{0,8},{4,12},{8,0},{12,4},{1,9},{5,13},{9,1},{13,5},{2,10},{6,14},... | collective-permute-start | bytes 786440 | tf_op jit(solution)/shard_map/ppermute | solution.py:897
  12.2 22.4 %collective-permute-start = (bf16[128,1024]{1,0:T(8,128)(2,1)S(1)}, bf16[128,1024]{1,0:T(8,128)(2,1)S(1)}, u32[]{:S(2)}, u32[]{:S(2)}) collective-permute-start(bf16[128,1024]{1,0:T(8,128)(2,1)S(1)} %get-tuple-element.33.refs_0_), channel_id=1, source_target_pairs={{0,4},{4,0},{8,12},{12,8},{1,5},{5,1},{9,13},{13,9},{2,6},{6,2},{1... | collective-permute-start | bytes 786440 | tf_op jit(solution)/shard_map/ppermute | solution.py:911
  13.6 5.0 %collective-permute-start.9 = (bf16[128,512]{1,0:T(8,128)(2,1)S(1)}, bf16[128,512]{1,0:T(8,128)(2,1)S(1)}, u32[]{:S(2)}, u32[]{:S(2)}) collective-permute-start(bf16[128,512]{1,0:T(8,128)(2,1)S(1)} %copy-done.31), channel_id=1, source_target_pairs={{0,16},{16,0},{1,17},{17,1},{2,18},{18,2},{3,19},{19,3},{4,20},{20... | collective-permute-start | bytes 393224 | tf_op jit(solution)/shard_map/ppermute | solution.py:894
  15.2 20.9 %collective-permute-start.6 = (bf16[128,512]{1,0:T(8,128)(2,1)S(1)}, bf16[128,512]{1,0:T(8,128)(2,1)S(1)}, u32[]{:S(2)}, u32[]{:S(2)}) collective-permute-start(bf16[128,512]{1,0:T(8,128)(2,1)S(1)} %copy-done.31), channel_id=1, source_target_pairs={{0,2},{2,0},{1,3},{3,1},{4,6},{6,4},{5,7},{7,5},{8,10},{10,8},{9,1... | collective-permute-start | bytes 393224 | tf_op jit(solution)/shard_map/ppermute | solution.py:894
  18.6 16.6 %copy-start.24 = (bf16[128,512]{1,0:T(8,128)(2,1)}, bf16[128,512]{1,0:T(8,128)(2,1)S(1)}, u32[]{:S(2)}) copy-start(bf16[128,512]{1,0:T(8,128)(2,1)S(1)} %collective-permute-done.9.refs_12_) | copy-start | bytes 393220
  18.6 19.0 %collective-permute-start.12 = (bf16[128,512]{1,0:T(8,128)(2,1)S(1)}, bf16[128,512]{1,0:T(8,128)(2,1)S(1)}, u32[]{:S(2)}, u32[]{:S(2)}) collective-permute-start(bf16[128,512]{1,0:T(8,128)(2,1)S(1)} %collective-permute-done.9.refs_12_), channel_id=1, source_target_pairs={{0,2},{2,0},{1,3},{3,1},{4,6},{6,4},{5,7},{7,5},{8,10},{10,8},{9,1... | collective-permute-start | bytes 393224 | tf_op jit(solution)/shard_map/ppermute | solution.py:894
  34.5 7.3 %collective-permute-start.2 = (bf16[128,1024]{1,0:T(8,128)(2,1)S(1)}, bf16[128,1024]{1,0:T(8,128)(2,1)S(1)}, u32[]{:S(2)}, u32[]{:S(2)}) collective-permute-start(bf16[128,1024]{1,0:T(8,128)(2,1)S(1)} %collective-permute-done.1.refs_2_), channel_id=1, source_target_pairs={{0,4},{4,0},{8,12},{12,8},{1,5},{5,1},{9,13},{13,9},{2,6},{6,2},{1... | collective-permute-start | bytes 786440 | tf_op jit(solution)/shard_map/ppermute | solution.py:911
  34.5 9.4 %collective-permute-start.4 = (bf16[128,1024]{1,0:T(8,128)(2,1)S(1)}, bf16[128,1024]{1,0:T(8,128)(2,1)S(1)}, u32[]{:S(2)}, u32[]{:S(2)}) collective-permute-start(bf16[128,1024]{1,0:T(8,128)(2,1)S(1)} %collective-permute-done.1.refs_2_), channel_id=1, source_target_pairs={{0,1},{1,0},{2,3},{3,2},{4,5},{5,4},{6,7},{7,6},{8,9},{9,8},{10,11... | collective-permute-start | bytes 786440 | tf_op jit(solution)/shard_map/ppermute | solution.py:894
  34.6 11.0 %collective-permute-start.3 = (bf16[128,1024]{1,0:T(8,128)(2,1)S(1)}, bf16[128,1024]{1,0:T(8,128)(2,1)S(1)}, u32[]{:S(2)}, u32[]{:S(2)}) collective-permute-start(bf16[128,1024]{1,0:T(8,128)(2,1)S(1)} %collective-permute-done.refs_1_), channel_id=1, source_target_pairs={{0,1},{1,0},{2,3},{3,2},{4,5},{5,4},{6,7},{7,6},{8,9},{9,8},{10,11... | collective-permute-start | bytes 786440 | tf_op jit(solution)/shard_map/ppermute | solution.py:894
  36.0 5.9 %copy-start.25 = (bf16[128,512]{1,0:T(8,128)(2,1)}, bf16[128,512]{1,0:T(8,128)(2,1)S(1)}, u32[]{:S(2)}) copy-start(bf16[128,512]{1,0:T(8,128)(2,1)S(1)} %collective-permute-done.6.refs_9_) | copy-start | bytes 393220
  36.0 11.0 %collective-permute-start.10 = (bf16[192,512]{1,0:T(8,128)(2,1)}, bf16[192,512]{1,0:T(8,128)(2,1)S(1)}, u32[]{:S(2)}, u32[]{:S(2)}) collective-permute-start(bf16[192,512]{1,0:T(8,128)(2,1)} %get-tuple-element.62), channel_id=1, source_target_pairs={{0,16},{16,0},{1,17},{17,1},{2,18},{18,2},{3,19},{19,3},{4,20},{20... | collective-permute-start | bytes 589832 | tf_op jit(solution)/shard_map/ppermute | solution.py:894
  38.3 9.3 %collective-permute-start.8 = (bf16[192,512]{1,0:T(8,128)(2,1)}, bf16[192,512]{1,0:T(8,128)(2,1)S(1)}, u32[]{:S(2)}, u32[]{:S(2)}) collective-permute-start(bf16[192,512]{1,0:T(8,128)(2,1)} %get-tuple-element.61), channel_id=1, source_target_pairs={{0,2},{2,0},{1,3},{3,1},{4,6},{6,4},{5,7},{7,5},{8,10},{10,8},{9,1... | collective-permute-start | bytes 589832 | tf_op jit(solution)/shard_map/ppermute | solution.py:894
  41.9 6.4 %collective-permute-start.5 = (bf16[128,1024]{1,0:T(8,128)(2,1)S(1)}, bf16[128,1024]{1,0:T(8,128)(2,1)S(1)}, u32[]{:S(2)}, u32[]{:S(2)}) collective-permute-start(bf16[128,1024]{1,0:T(8,128)(2,1)S(1)} %collective-permute-done.2.refs_3_), channel_id=1, source_target_pairs={{0,1},{1,0},{2,3},{3,2},{4,5},{5,4},{6,7},{7,6},{8,9},{9,8},{10,11... | collective-permute-start | bytes 786440 | tf_op jit(solution)/shard_map/ppermute | solution.py:894
  41.9 6.2 %copy-start.16 = (bf16[512,256]{1,0:T(8,128)(2,1)S(1)}, bf16[512,256]{1,0:T(8,128)(2,1)}, u32[]{:S(2)}) copy-start(bf16[512,256]{1,0:T(8,128)(2,1)} %param.37) | copy-start | bytes 786436
  41.9 6.2 %copy-start.17 = (bf16[512,256]{1,0:T(8,128)(2,1)S(1)}, bf16[512,256]{1,0:T(8,128)(2,1)}, u32[]{:S(2)}) copy-start(bf16[512,256]{1,0:T(8,128)(2,1)} %param.38) | copy-start | bytes 786436
  44.0 8.0 %collective-permute-start.11 = (bf16[192,512]{1,0:T(8,128)(2,1)}, bf16[192,512]{1,0:T(8,128)(2,1)S(1)}, u32[]{:S(2)}, u32[]{:S(2)}) collective-permute-start(bf16[192,512]{1,0:T(8,128)(2,1)} %get-tuple-element.61), channel_id=1, source_target_pairs={{0,16},{16,0},{1,17},{17,1},{2,18},{18,2},{3,19},{19,3},{4,20},{20... | collective-permute-start | bytes 589832 | tf_op jit(solution)/shard_map/ppermute | solution.py:894
  45.5 8.0 %collective-permute-start.7 = (bf16[192,512]{1,0:T(8,128)(2,1)}, bf16[192,512]{1,0:T(8,128)(2,1)S(1)}, u32[]{:S(2)}, u32[]{:S(2)}) collective-permute-start(bf16[192,512]{1,0:T(8,128)(2,1)} %get-tuple-element.62), channel_id=1, source_target_pairs={{0,2},{2,0},{1,3},{3,1},{4,6},{6,4},{5,7},{7,5},{8,10},{10,8},{9,1... | collective-permute-start | bytes 589832 | tf_op jit(solution)/shard_map/ppermute | solution.py:894
  47.0 9.9 %collective-permute-start.13 = (bf16[192,512]{1,0:T(8,128)(2,1)S(1)}, bf16[192,512]{1,0:T(8,128)(2,1)S(1)}, u32[]{:S(2)}, u32[]{:S(2)}) collective-permute-start(bf16[192,512]{1,0:T(8,128)(2,1)S(1)} %collective-permute-done.10.refs_13_), channel_id=1, source_target_pairs={{0,2},{2,0},{1,3},{3,1},{4,6},{6,4},{5,7},{7,5},{8,10},{10,8},{9,1... | collective-permute-start | bytes 589832 | tf_op jit(solution)/shard_map/ppermute | solution.py:894
  47.6 9.4 %collective-permute-start.14 = (bf16[192,512]{1,0:T(8,128)(2,1)S(1)}, bf16[192,512]{1,0:T(8,128)(2,1)S(1)}, u32[]{:S(2)}, u32[]{:S(2)}) collective-permute-start(bf16[192,512]{1,0:T(8,128)(2,1)S(1)} %collective-permute-done.8.refs_11_), channel_id=1, source_target_pairs={{0,16},{16,0},{1,17},{17,1},{2,18},{18,2},{3,19},{19,3},{4,20},{20... | collective-permute-start | bytes 589832 | tf_op jit(solution)/shard_map/ppermute | solution.py:894
  48.3 8.7 %copy-start.15 = (bf16[128,1024]{1,0:T(8,128)(2,1)}, bf16[128,1024]{1,0:T(8,128)(2,1)S(1)}, u32[]{:S(2)}) copy-start(bf16[128,1024]{1,0:T(8,128)(2,1)S(1)} %collective-permute-done.5.refs_7_) | copy-start | bytes 786436
  52.0 5.0 %copy-start.20 = (bf16[192,512]{1,0:T(8,128)(2,1)}, bf16[192,512]{1,0:T(8,128)(2,1)S(1)}, u32[]{:S(2)}) copy-start(bf16[192,512]{1,0:T(8,128)(2,1)S(1)} %collective-permute-done.11.refs_14_) | copy-start | bytes 589828
  63.1 31.0 %all-to-all-start.1 = ((bf16[4,384,128]{2,1,0:T(8,128)(2,1)}), bf16[4,384,128]{2,1,0:T(8,128)(2,1)S(1)}, u32[]{:S(2)}, u32[]{:S(2)}) async-start(bf16[4,384,128]{2,1,0:T(8,128)(2,1)} %get-tuple-element.45), calls=%async_computation.1 | async-start | bytes 786432 | tf_op jit(solution)/shard_map/all_to_all | solution.py:891
  66.7 22.6 %collective-permute-start.23 = (bf16[512,256]{1,0:T(8,128)(2,1)S(1)}, bf16[512,256]{1,0:T(8,128)(2,1)S(1)}, u32[]{:S(2)}, u32[]{:S(2)}) collective-permute-start(bf16[512,256]{1,0:T(8,128)(2,1)S(1)} %constant_dynamic-slice_fusion.2), channel_id=1, source_target_pairs={{0,8},{4,12},{8,0},{12,4},{1,9},{5,13},{9,1},{13,5},{2,10},{6,14},... | collective-permute-start | bytes 786440 | tf_op jit(solution)/shard_map/ppermute | solution.py:897
  69.6 34.3 %collective-permute-start.22 = (bf16[1024,256]{1,0:T(8,128)(2,1)S(1)}, bf16[1024,256]{1,0:T(8,128)(2,1)S(1)}, u32[]{:S(2)}, u32[]{:S(2)}) collective-permute-start(bf16[1024,256]{1,0:T(8,128)(2,1)S(1)} %pad_maximum_fusion.refs_8_), channel_id=1, source_target_pairs={{0,2},{2,0},{1,3},{3,1},{4,6},{6,4},{5,7},{7,5},{8,10},{10,8},{9,1... | collective-permute-start | bytes 1572872 | tf_op jit(solution)/shard_map/ppermute | solution.py:894
  89.2 7.3 %collective-permute-start.24 = (bf16[512,256]{1,0:T(8,128)(2,1)S(1)}, bf16[512,256]{1,0:T(8,128)(2,1)S(1)}, u32[]{:S(2)}, u32[]{:S(2)}) collective-permute-start(bf16[512,256]{1,0:T(8,128)(2,1)S(1)} %collective-permute-done.23.refs_10_), channel_id=1, source_target_pairs={{0,16},{16,0},{1,17},{17,1},{2,18},{18,2},{3,19},{19,3},{4,20},{20... | collective-permute-start | bytes 786440 | tf_op jit(solution)/shard_map/ppermute | solution.py:894
  89.8 9.7 %copy-start.3 = (f32[256,64]{1,0:T(8,128)S(1)}, f32[256,64]{1,0:T(8,128)}, u32[]{:S(2)}) copy-start(f32[256,64]{1,0:T(8,128)} %constant.53.clone.cos_ref) | copy-start | bytes 196612
  89.8 9.7 %copy-start.4 = (f32[256,64]{1,0:T(8,128)S(1)}, f32[256,64]{1,0:T(8,128)}, u32[]{:S(2)}) copy-start(f32[256,64]{1,0:T(8,128)} %constant.54.clone.sin_ref) | copy-start | bytes 196612
  94.1 5.4 %copy-start.9 = (bf16[4,384,128]{2,1,0:T(8,128)(2,1)}, bf16[4,384,128]{2,1,0:T(8,128)(2,1)S(1)}, u32[]{:S(2)}) copy-start(bf16[4,384,128]{2,1,0:T(8,128)(2,1)S(1)} %all-to-all-done.1.mine_ref) | copy-start | bytes 1179652
  94.1 5.4 %collective-permute-start.18 = (bf16[4,384,128]{2,1,0:T(8,128)(2,1)S(1)}, bf16[4,384,128]{2,1,0:T(8,128)(2,1)S(1)}, u32[]{:S(2)}, u32[]{:S(2)}) collective-permute-start(bf16[4,384,128]{2,1,0:T(8,128)(2,1)S(1)} %all-to-all-done.1.mine_ref), channel_id=1, source_target_pairs={{0,1},{1,0},{2,3},{3,2},{4,5},{5,4},{6,7},{7,6},{8,9},{9,8},{10,11... | collective-permute-start | bytes 1179656 | tf_op jit(solution)/shard_map/ppermute | solution.py:894
  94.2 9.2 %collective-permute-start.25 = (bf16[512,256]{1,0:T(8,128)(2,1)S(1)}, bf16[512,256]{1,0:T(8,128)(2,1)S(1)}, u32[]{:S(2)}, u32[]{:S(2)}) collective-permute-start(bf16[512,256]{1,0:T(8,128)(2,1)S(1)} %collective-permute-done.23.refs_10_), channel_id=1, source_target_pairs={{0,2},{2,0},{1,3},{3,1},{4,6},{6,4},{5,7},{7,5},{8,10},{10,8},{9,1... | collective-permute-start | bytes 786440 | tf_op jit(solution)/shard_map/ppermute | solution.py:894
  96.6 11.9 %collective-permute-start.26 = (bf16[512,256]{1,0:T(8,128)(2,1)S(1)}, bf16[512,256]{1,0:T(8,128)(2,1)S(1)}, u32[]{:S(2)}, u32[]{:S(2)}) collective-permute-start(bf16[512,256]{1,0:T(8,128)(2,1)S(1)} %collective-permute-done.24.refs_11_), channel_id=1, source_target_pairs={{0,2},{2,0},{1,3},{3,1},{4,6},{6,4},{5,7},{7,5},{8,10},{10,8},{9,1... | collective-permute-start | bytes 786440 | tf_op jit(solution)/shard_map/ppermute | solution.py:894
  98.1 10.4 %collective-permute-start.15 = (bf16[256,128]{1,0:T(8,128)(2,1)}, bf16[256,128]{1,0:T(8,128)(2,1)S(1)}, u32[]{:S(2)}, u32[]{:S(2)}) collective-permute-start(bf16[256,128]{1,0:T(8,128)(2,1)} %get-tuple-element.42), channel_id=1, source_target_pairs={{0,12},{4,0},{8,4},{12,8},{1,13},{5,1},{9,5},{13,9},{2,14},{6,2},{... | collective-permute-start | bytes 196616 | tf_op jit(solution)/shard_map/ppermute | solution.py:897
  99.5 11.0 %collective-permute-start.16 = (bf16[256,128]{1,0:T(8,128)(2,1)}, bf16[256,128]{1,0:T(8,128)(2,1)S(1)}, u32[]{:S(2)}, u32[]{:S(2)}) collective-permute-start(bf16[256,128]{1,0:T(8,128)(2,1)} %get-tuple-element.43), channel_id=1, source_target_pairs={{0,8},{4,12},{8,0},{12,4},{1,9},{5,13},{9,1},{13,5},{2,10},{6,14},... | collective-permute-start | bytes 196616 | tf_op jit(solution)/shard_map/ppermute | solution.py:897
  99.5 15.5 %copy-start.5 = (bf16[256,128]{1,0:T(8,128)(2,1)S(1)}, bf16[256,128]{1,0:T(8,128)(2,1)}, u32[]{:S(2)}) copy-start(bf16[256,128]{1,0:T(8,128)(2,1)} %get-tuple-element.41.refs_0_) | copy-start | bytes 196612
  103.4 7.1 %collective-permute-start.17 = (bf16[256,128]{1,0:T(8,128)(2,1)S(1)}, bf16[256,128]{1,0:T(8,128)(2,1)S(1)}, u32[]{:S(2)}, u32[]{:S(2)}) collective-permute-start(bf16[256,128]{1,0:T(8,128)(2,1)S(1)} %copy-done.32), channel_id=1, source_target_pairs={{0,4},{4,8},{8,12},{12,0},{1,5},{5,9},{9,13},{13,1},{2,6},{6,10},{... | collective-permute-start | bytes 196616 | tf_op jit(solution)/shard_map/ppermute | solution.py:897
  103.9 11.1 %copy-start.7 = (f32[1024]{0:T(1024)S(1)}, f32[1024]{0:T(1024)}, u32[]{:S(2)}) copy-start(f32[1024]{0:T(1024)} %param.39) | copy-start | bytes 12292
  103.9 6.6 %collective-permute-start.19 = (bf16[256,128]{1,0:T(8,128)(2,1)S(1)}, bf16[256,128]{1,0:T(8,128)(2,1)S(1)}, u32[]{:S(2)}, u32[]{:S(2)}) collective-permute-start(bf16[256,128]{1,0:T(8,128)(2,1)S(1)} %get-tuple-element.51), channel_id=1, source_target_pairs={{0,12},{4,0},{8,4},{12,8},{1,13},{5,1},{9,5},{13,9},{2,14},{6,2},{... | collective-permute-start | bytes 196616 | tf_op jit(solution)/shard_map/ppermute | solution.py:897
  108.5 6.5 %collective-permute-start.20 = (bf16[256,128]{1,0:T(8,128)(2,1)S(1)}, bf16[256,128]{1,0:T(8,128)(2,1)S(1)}, u32[]{:S(2)}, u32[]{:S(2)}) collective-permute-start(bf16[256,128]{1,0:T(8,128)(2,1)S(1)} %get-tuple-element.52), channel_id=1, source_target_pairs={{0,8},{4,12},{8,0},{12,4},{1,9},{5,13},{9,1},{13,5},{2,10},{6,14},... | collective-permute-start | bytes 196616 | tf_op jit(solution)/shard_map/ppermute | solution.py:897
  108.5 6.5 %collective-permute-start.21 = (bf16[256,128]{1,0:T(8,128)(2,1)S(1)}, bf16[256,128]{1,0:T(8,128)(2,1)S(1)}, u32[]{:S(2)}, u32[]{:S(2)}) collective-permute-start(bf16[256,128]{1,0:T(8,128)(2,1)S(1)} %get-tuple-element.53), channel_id=1, source_target_pairs={{0,4},{4,8},{8,12},{12,0},{1,5},{5,9},{9,13},{13,1},{2,6},{6,10},{... | collective-permute-start | bytes 196616 | tf_op jit(solution)/shard_map/ppermute | solution.py:897
  115.9 1.6 %collective-permute-start.27 = (bf16[2,128,512]{2,1,0:T(8,128)(2,1)S(1)}, bf16[2,128,512]{2,1,0:T(8,128)(2,1)S(1)}, u32[]{:S(2)}, u32[]{:S(2)}) collective-permute-start(bf16[2,128,512]{2,1,0:T(8,128)(2,1)S(1)} %get-tuple-element.55), channel_id=1, source_target_pairs={{0,1},{1,0},{2,3},{3,2},{4,5},{5,4},{6,7},{7,6},{8,9},{9,8},{10,11... | collective-permute-start | bytes 786440 | tf_op jit(solution)/shard_map/ppermute | solution.py:894
  117.7 1.2 collective-permute-start.29
  118.9 3.6 %collective-permute-start.30 = (f32[128]{0:T(128)S(1)}, f32[128]{0:T(128)S(1)}, u32[]{:S(2)}, u32[]{:S(2)}) collective-permute-start(f32[128]{0:T(128)S(1)} %fusion.7), channel_id=1, source_target_pairs={{0,4},{4,0},{8,12},{12,8},{1,5},{5,1},{9,13},{13,9},{2,6},{6,2},{1... | collective-permute-start | bytes 1544 | tf_op jit(solution)/shard_map/ppermute | solution.py:987
  119.0 5.6 %collective-permute-start.28 = (bf16[128,512]{1,0:T(8,128)(2,1)S(1)}, bf16[128,512]{1,0:T(8,128)(2,1)S(1)}, u32[]{:S(2)}, u32[]{:S(2)}) collective-permute-start(bf16[128,512]{1,0:T(8,128)(2,1)S(1)} %dynamic-slice_bitcast_fusion), channel_id=1, source_target_pairs={{0,4},{4,0},{8,12},{12,8},{1,5},{5,1},{9,13},{13,9},{2,6},{6,2},{1... | collective-permute-start | bytes 393224 | tf_op jit(solution)/shard_map/ppermute | solution.py:987
  (18 other events, 42.4 us)

commit v3 on v2

--- a/solution.py
+++ b/solution.py
@@ -557,17 +557,22 @@
                 copy.wait()
             lhs = token_ref[o * chunk : (o + 1) * chunk, :]
             value = dot32(lhs, weight_ref[...]).astype(jnp.bfloat16)
-            outer = dot_t(lhs, extra_ref[...])
             source = lax.bitwise_xor(place, o)
             for n in range(seq_count):
                 of = slice(n * token_count, (n + 1) * token_count)
                 at = pl.ds(pl.multiple_of(source * token_count, token_count), token_count)
                 fine_ref[n, at, :] = value[of, :fine]
-                ext_ref[n, at, :] = outer[of]
                 at = pl.ds(
                     pl.multiple_of(n * span + source * token_count, token_count), token_count
                 )
                 lat_ref[at, :] = value[of, fine : fine + 128]
+        outer = dot_t(token_ref[...], extra_ref[...])
+        for o in range(sp_size):
+            source = lax.bitwise_xor(place, o)
+            for n in range(seq_count):
+                of = slice(o * chunk + n * token_count, o * chunk + (n + 1) * token_count)
+                at = pl.ds(pl.multiple_of(source * token_count, token_count), token_count)
+                ext_ref[n, at, :] = outer[of]
         for start, first, width, count in (
             (0, 0, q_cols, q_stack),
             (rows // q_stack, q_cols, kv_cols, kv_stack),

time: 126 us -> 125 us (level)
  no operation moved by 1% of the time
where the time goes in v3:
time: 125 us
  waiting for transfers between devices  58.2 us (47%)
  starting transfers between devices  44.4 us (36%)
  Pallas kernels  18 us (14%)
  local copies, waits for them, and re-layouts  2.52 us (2%)
  other arithmetic  1.26 us (1%)
    ppermute x8, waiting for transfers between devices, along(): lax.ppermute(values, 'sp', [(i, (i + step) % sp_size) for i in range(sp_s...  37.1 us
    ppermute x19, starting transfers between devices, swap(): return lax.ppermute(values, axis, [(0, 1), (1, 0)])  17.6 us
    ppermute x19, waiting for transfers between devices, swap(): return lax.ppermute(values, axis, [(0, 1), (1, 0)])  15.6 us
    ppermute x8, starting transfers between devices, along(): lax.ppermute(values, 'sp', [(i, (i + step) % sp_size) for i in range(sp_s...  13.2 us
    pallas_call x5, Pallas kernels, kernel_call(): pl.pallas_call(body, out_shape=jax.tree.map(lambda leaf: result_space(lea...  11.2 us
    all_to_all x2, starting transfers between devices, exchange(): return lax.all_to_all(values, axis, 0, 0, tiled=True)  9.96 us
    pallas_call x1, Pallas kernels, project(): pl.pallas_call(body, out_shape=(pltpu.VMEM((seq_count, span, fine), jnp.b...  4.55 us
    ppermute x2, waiting for transfers between devices, across(): lax.ppermute(pick(values, 1 - side), 'sp', [(i, i ^ 1) for i in range(sp_...  3.47 us
  transfers between devices with their start and end apart: 33, of which 15 were waited for; matrix products, arithmetic and copies ran while one was open for 1% of the time, Pallas kernels for 8%

profile of v3, /device:TPU:0, one launch (start us, length us, event | category | flops | bytes accessed | tf_op | source)
XLA Modules:
  0.0 124.8 jit_solution(18300744836271909564)
XLA Ops:
  0.0 2.3 %outgoing_weights.1 = (bf16[4,128,512]{2,1,0:T(8,128)(2,1)}, bf16[128,512]{1,0:T(8,128)(2,1)}) custom-call(bf16[256,512]{1,0:T(8,128)(2,1)} %refs_0_.1, bf16[256,512]{1,0:T(8,128)(2,1)} %refs_1_.1, bf16[256,512]{1,0:T(8,128)(2,1)} %refs_2_.1, bf16[256,512]{1,0:T(8,128)(2,1)} %refs_3_.1, bf16[256,256]{1,0:T(8,128)(2,1)} %refs_4_.1), custom_call_target="tpu_custom_call" | custom-call | tf_op jit(solution)/shard_map/outgoing_weights/pallas_call | solution.py:422
  2.3 6.5 %all-to-all-start = ((bf16[4,128,512]{2,1,0:T(8,128)(2,1)}), bf16[4,128,512]{2,1,0:T(8,128)(2,1)S(1)}, u32[]{:S(2)}, u32[]{:S(2)}) async-start(bf16[4,128,512]{2,1,0:T(8,128)(2,1)} %get-tuple-element.31), calls=%async_computation | async-start | bytes 1048576 | tf_op jit(solution)/shard_map/all_to_all | solution.py:896
  9.2 3.0 %collective-permute-start.1 = (bf16[128,1024]{1,0:T(8,128)(2,1)S(1)}, bf16[128,1024]{1,0:T(8,128)(2,1)S(1)}, u32[]{:S(2)}, u32[]{:S(2)}) collective-permute-start(bf16[128,1024]{1,0:T(8,128)(2,1)S(1)} %get-tuple-element.33.refs_0_), channel_id=1, source_target_pairs={{0,8},{4,12},{8,0},{12,4},{1,9},{5,13},{9,1},{13,5},{2,10},{6,14},... | collective-permute-start | bytes 786440 | tf_op jit(solution)/shard_map/ppermute | solution.py:902
  12.2 1.5 %collective-permute-start = (bf16[128,1024]{1,0:T(8,128)(2,1)S(1)}, bf16[128,1024]{1,0:T(8,128)(2,1)S(1)}, u32[]{:S(2)}, u32[]{:S(2)}) collective-permute-start(bf16[128,1024]{1,0:T(8,128)(2,1)S(1)} %get-tuple-element.33.refs_0_), channel_id=1, source_target_pairs={{0,4},{4,0},{8,12},{12,8},{1,5},{5,1},{9,13},{13,9},{2,6},{6,2},{1... | collective-permute-start | bytes 786440 | tf_op jit(solution)/shard_map/ppermute | solution.py:916
  13.6 1.5 %collective-permute-start.9 = (bf16[128,512]{1,0:T(8,128)(2,1)S(1)}, bf16[128,512]{1,0:T(8,128)(2,1)S(1)}, u32[]{:S(2)}, u32[]{:S(2)}) collective-permute-start(bf16[128,512]{1,0:T(8,128)(2,1)S(1)} %copy-done.31), channel_id=1, source_target_pairs={{0,16},{16,0},{1,17},{17,1},{2,18},{18,2},{3,19},{19,3},{4,20},{20... | collective-permute-start | bytes 393224 | tf_op jit(solution)/shard_map/ppermute | solution.py:899
  15.2 1.5 %collective-permute-start.6 = (bf16[128,512]{1,0:T(8,128)(2,1)S(1)}, bf16[128,512]{1,0:T(8,128)(2,1)S(1)}, u32[]{:S(2)}, u32[]{:S(2)}) collective-permute-start(bf16[128,512]{1,0:T(8,128)(2,1)S(1)} %copy-done.31), channel_id=1, source_target_pairs={{0,2},{2,0},{1,3},{3,1},{4,6},{6,4},{5,7},{7,5},{8,10},{10,8},{9,1... | collective-permute-start | bytes 393224 | tf_op jit(solution)/shard_map/ppermute | solution.py:899
  16.6 2.0 %collective-permute-done.9.refs_12_ = bf16[128,512]{1,0:T(8,128)(2,1)S(1)} collective-permute-done((bf16[128,512]{1,0:T(8,128)(2,1)S(1)}, bf16[128,512]{1,0:T(8,128)(2,1)S(1)}, u32[]{:S(2)}, u32[]{:S(2)}) %collective-permute-start.9) | collective-permute-done | bytes 131104 | tf_op jit(solution)/shard_map/ppermute | solution.py:899
  18.6 1.5 %collective-permute-start.12 = (bf16[128,512]{1,0:T(8,128)(2,1)S(1)}, bf16[128,512]{1,0:T(8,128)(2,1)S(1)}, u32[]{:S(2)}, u32[]{:S(2)}) collective-permute-start(bf16[128,512]{1,0:T(8,128)(2,1)S(1)} %collective-permute-done.9.refs_12_), channel_id=1, source_target_pairs={{0,2},{2,0},{1,3},{3,1},{4,6},{6,4},{5,7},{7,5},{8,10},{10,8},{9,1... | collective-permute-start | bytes 393224 | tf_op jit(solution)/shard_map/ppermute | solution.py:899
  20.1 14.4 %collective-permute-done.1.refs_2_ = bf16[128,1024]{1,0:T(8,128)(2,1)S(1)} collective-permute-done((bf16[128,1024]{1,0:T(8,128)(2,1)S(1)}, bf16[128,1024]{1,0:T(8,128)(2,1)S(1)}, u32[]{:S(2)}, u32[]{:S(2)}) %collective-permute-start.1) | collective-permute-done | bytes 262176 | tf_op jit(solution)/shard_map/ppermute | solution.py:902
  34.6 0.5 collective-permute-start.3
  35.2 0.8 fusion.8
  36.0 1.6 %collective-permute-start.10 = (bf16[192,512]{1,0:T(8,128)(2,1)}, bf16[192,512]{1,0:T(8,128)(2,1)S(1)}, u32[]{:S(2)}, u32[]{:S(2)}) collective-permute-start(bf16[192,512]{1,0:T(8,128)(2,1)} %get-tuple-element.62), channel_id=1, source_target_pairs={{0,16},{16,0},{1,17},{17,1},{2,18},{18,2},{3,19},{19,3},{4,20},{20... | collective-permute-start | bytes 589832 | tf_op jit(solution)/shard_map/ppermute | solution.py:899
  37.6 0.6 copy-done.26
  38.3 1.5 %collective-permute-start.8 = (bf16[192,512]{1,0:T(8,128)(2,1)}, bf16[192,512]{1,0:T(8,128)(2,1)S(1)}, u32[]{:S(2)}, u32[]{:S(2)}) collective-permute-start(bf16[192,512]{1,0:T(8,128)(2,1)} %get-tuple-element.61), channel_id=1, source_target_pairs={{0,2},{2,0},{1,3},{3,1},{4,6},{6,4},{5,7},{7,5},{8,10},{10,8},{9,1... | collective-permute-start | bytes 589832 | tf_op jit(solution)/shard_map/ppermute | solution.py:899
  39.8 2.1 %collective-permute-done.2.refs_3_ = bf16[128,1024]{1,0:T(8,128)(2,1)S(1)} collective-permute-done((bf16[128,1024]{1,0:T(8,128)(2,1)S(1)}, bf16[128,1024]{1,0:T(8,128)(2,1)S(1)}, u32[]{:S(2)}, u32[]{:S(2)}) %collective-permute-start.2) | collective-permute-done | bytes 262176 | tf_op jit(solution)/shard_map/ppermute | solution.py:916
  41.9 2.0 %shard_map.200 = (bf16[48,2048]{1,0:T(8,128)(2,1)S(1)}, bf16[512,256]{1,0:T(8,128)(2,1)S(1)}, bf16[256,256]{1,0:T(8,128)(2,1)S(1)}) custom-call(bf16[32,2048]{1,0:T(8,128)(2,1)} %bitcast.37, bf16[8,2048]{1,0:T(8,128)(2,1)} %bitcast.38, bf16[8,2048]{1,0:T(8,128)(2,1)} %bitcast.39, bf16[512,768]{1,0:T(8,128)(2,1)} %query_ref.1, bf16[256,1024]{1,0:T(8,128)(2,1)} %latent_ref.1), custom_call_target="tpu_custom_call" | custom-call | tf_op jit(solution)/shard_map/pallas_call | solution.py:371
  44.0 1.6 %collective-permute-start.11 = (bf16[192,512]{1,0:T(8,128)(2,1)}, bf16[192,512]{1,0:T(8,128)(2,1)S(1)}, u32[]{:S(2)}, u32[]{:S(2)}) collective-permute-start(bf16[192,512]{1,0:T(8,128)(2,1)} %get-tuple-element.61), channel_id=1, source_target_pairs={{0,16},{16,0},{1,17},{17,1},{2,18},{18,2},{3,19},{19,3},{4,20},{20... | collective-permute-start | bytes 589832 | tf_op jit(solution)/shard_map/ppermute | solution.py:899
  45.5 1.5 %collective-permute-start.7 = (bf16[192,512]{1,0:T(8,128)(2,1)}, bf16[192,512]{1,0:T(8,128)(2,1)S(1)}, u32[]{:S(2)}, u32[]{:S(2)}) collective-permute-start(bf16[192,512]{1,0:T(8,128)(2,1)} %get-tuple-element.62), channel_id=1, source_target_pairs={{0,2},{2,0},{1,3},{3,1},{4,6},{6,4},{5,7},{7,5},{8,10},{10,8},{9,1... | collective-permute-start | bytes 589832 | tf_op jit(solution)/shard_map/ppermute | solution.py:899
  47.0 0.5 collective-permute-start.13
  47.6 0.6 collective-permute-start.14
  48.3 3.7 %collective-permute-done.11.refs_14_ = bf16[192,512]{1,0:T(8,128)(2,1)S(1)} collective-permute-done((bf16[192,512]{1,0:T(8,128)(2,1)}, bf16[192,512]{1,0:T(8,128)(2,1)S(1)}, u32[]{:S(2)}, u32[]{:S(2)}) %collective-permute-start.11) | collective-permute-done | bytes 196640 | tf_op jit(solution)/shard_map/ppermute | solution.py:899
  52.0 1.5 %collective-permute-done.7.refs_10_ = bf16[192,512]{1,0:T(8,128)(2,1)S(1)} collective-permute-done((bf16[192,512]{1,0:T(8,128)(2,1)}, bf16[192,512]{1,0:T(8,128)(2,1)S(1)}, u32[]{:S(2)}, u32[]{:S(2)}) %collective-permute-start.7) | collective-permute-done | bytes 196640 | tf_op jit(solution)/shard_map/ppermute | solution.py:899
  53.5 3.4 %collective-permute-done.13.refs_16_ = bf16[192,512]{1,0:T(8,128)(2,1)S(1)} collective-permute-done((bf16[192,512]{1,0:T(8,128)(2,1)S(1)}, bf16[192,512]{1,0:T(8,128)(2,1)S(1)}, u32[]{:S(2)}, u32[]{:S(2)}) %collective-permute-start.13) | collective-permute-done | bytes 196640 | tf_op jit(solution)/shard_map/ppermute | solution.py:899
  57.0 0.6 copy-done.22
  57.8 4.6 %project.1 = (bf16[2,256,384]{2,1,0:T(8,128)(2,1)S(1)}, bf16[4,384,128]{2,1,0:T(8,128)(2,1)}, f32[2,256,48]{2,1,0:T(8,128)S(1)}) custom-call(bf16[128,1024]{1,0:T(8,128)(2,1)} %copy-done.1, bf16[128,1024]{1,0:T(8,128)(2,1)} %copy-done.11, bf16[128,1024]{1,0:T(8,128)(2,1)} %copy-done.10, bf16[128,1024]{1,0:T(8,128)(2,1)} %copy-done.12, ...), custom_call_target="tpu_custom_call" | custom-call | tf_op jit(solution)/shard_map/project/pallas_call | solution.py:596
  62.3 3.5 %all-to-all-start.1 = ((bf16[4,384,128]{2,1,0:T(8,128)(2,1)}), bf16[4,384,128]{2,1,0:T(8,128)(2,1)S(1)}, u32[]{:S(2)}, u32[]{:S(2)}) async-start(bf16[4,384,128]{2,1,0:T(8,128)(2,1)} %get-tuple-element.45), calls=%async_computation.1 | async-start | bytes 786432 | tf_op jit(solution)/shard_map/all_to_all | solution.py:896
  65.9 2.9 %collective-permute-start.23 = (bf16[512,256]{1,0:T(8,128)(2,1)S(1)}, bf16[512,256]{1,0:T(8,128)(2,1)S(1)}, u32[]{:S(2)}, u32[]{:S(2)}) collective-permute-start(bf16[512,256]{1,0:T(8,128)(2,1)S(1)} %constant_dynamic-slice_fusion.2), channel_id=1, source_target_pairs={{0,8},{4,12},{8,0},{12,4},{1,9},{5,13},{9,1},{13,5},{2,10},{6,14},... | collective-permute-start | bytes 786440 | tf_op jit(solution)/shard_map/ppermute | solution.py:902
  68.8 1.5 %collective-permute-start.22 = (bf16[1024,256]{1,0:T(8,128)(2,1)S(1)}, bf16[1024,256]{1,0:T(8,128)(2,1)S(1)}, u32[]{:S(2)}, u32[]{:S(2)}) collective-permute-start(bf16[1024,256]{1,0:T(8,128)(2,1)S(1)} %pad_maximum_fusion.refs_8_), channel_id=1, source_target_pairs={{0,2},{2,0},{1,3},{3,1},{4,6},{6,4},{5,7},{7,5},{8,10},{10,8},{9,1... | collective-permute-start | bytes 1572872 | tf_op jit(solution)/shard_map/ppermute | solution.py:899
  70.3 18.1 %collective-permute-done.23.refs_10_ = bf16[512,256]{1,0:T(8,128)(2,1)S(1)} collective-permute-done((bf16[512,256]{1,0:T(8,128)(2,1)S(1)}, bf16[512,256]{1,0:T(8,128)(2,1)S(1)}, u32[]{:S(2)}, u32[]{:S(2)}) %collective-permute-start.23) | collective-permute-done | bytes 262176 | tf_op jit(solution)/shard_map/ppermute | solution.py:902
  88.5 0.5 collective-permute-start.24
  89.0 4.4 %shard_map.201 = (bf16[256,128]{1,0:T(8,128)(2,1)}, bf16[256,128]{1,0:T(8,128)(2,1)}, bf16[256,128]{1,0:T(8,128)(2,1)}, bf16[256,128]{1,0:T(8,128)(2,1)}) custom-call(bf16[2,256,384]{2,1,0:T(8,128)(2,1)S(1)} %get-tuple-element.38.fine_ref, f32[2,256,48]{2,1,0:T(8,128)S(1)} %get-tuple-element.39.ext_ref, f32[1,256]{1,0:T(1,128)S(1)} %bitcast.32), custom_call_target="tpu_custom_call" | custom-call | tf_op jit(solution)/shard_map/pallas_call | solution.py:371
  93.4 1.6 %collective-permute-start.25 = (bf16[512,256]{1,0:T(8,128)(2,1)S(1)}, bf16[512,256]{1,0:T(8,128)(2,1)S(1)}, u32[]{:S(2)}, u32[]{:S(2)}) collective-permute-start(bf16[512,256]{1,0:T(8,128)(2,1)S(1)} %collective-permute-done.23.refs_10_), channel_id=1, source_target_pairs={{0,2},{2,0},{1,3},{3,1},{4,6},{6,4},{5,7},{7,5},{8,10},{10,8},{9,1... | collective-permute-start | bytes 786440 | tf_op jit(solution)/shard_map/ppermute | solution.py:899
  94.9 0.9 collective-permute-done.24.refs_11_
  95.8 1.5 %collective-permute-start.26 = (bf16[512,256]{1,0:T(8,128)(2,1)S(1)}, bf16[512,256]{1,0:T(8,128)(2,1)S(1)}, u32[]{:S(2)}, u32[]{:S(2)}) collective-permute-start(bf16[512,256]{1,0:T(8,128)(2,1)S(1)} %collective-permute-done.24.refs_11_), channel_id=1, source_target_pairs={{0,2},{2,0},{1,3},{3,1},{4,6},{6,4},{5,7},{7,5},{8,10},{10,8},{9,1... | collective-permute-start | bytes 786440 | tf_op jit(solution)/shard_map/ppermute | solution.py:899
  97.3 1.4 %collective-permute-start.15 = (bf16[256,128]{1,0:T(8,128)(2,1)}, bf16[256,128]{1,0:T(8,128)(2,1)S(1)}, u32[]{:S(2)}, u32[]{:S(2)}) collective-permute-start(bf16[256,128]{1,0:T(8,128)(2,1)} %get-tuple-element.42), channel_id=1, source_target_pairs={{0,12},{4,0},{8,4},{12,8},{1,13},{5,1},{9,5},{13,9},{2,14},{6,2},{... | collective-permute-start | bytes 196616 | tf_op jit(solution)/shard_map/ppermute | solution.py:902
  98.7 3.6 %shard_map.202 = (bf16[256,128]{1,0:T(8,128)(2,1)S(1)}, bf16[256,128]{1,0:T(8,128)(2,1)S(1)}, bf16[256,128]{1,0:T(8,128)(2,1)S(1)}, bf16[256,128]{1,0:T(8,128)(2,1)S(1)}) custom-call(bf16[4,384,128]{2,1,0:T(8,128)(2,1)} %copy-done.9, bf16[4,384,128]{2,1,0:T(8,128)(2,1)S(1)} %collective-permute-done.18.their_ref, ...), custom_call_target="tpu_custom_call" | custom-call | tf_op jit(solution)/shard_map/pallas_call | solution.py:371
  102.6 0.5 collective-permute-start.17
  103.1 3.4 %collective-permute-start.19 = (bf16[256,128]{1,0:T(8,128)(2,1)S(1)}, bf16[256,128]{1,0:T(8,128)(2,1)S(1)}, u32[]{:S(2)}, u32[]{:S(2)}) collective-permute-start(bf16[256,128]{1,0:T(8,128)(2,1)S(1)} %get-tuple-element.51), channel_id=1, source_target_pairs={{0,12},{4,0},{8,4},{12,8},{1,13},{5,1},{9,5},{13,9},{2,14},{6,2},{... | collective-permute-start | bytes 196616 | tf_op jit(solution)/shard_map/ppermute | solution.py:902
  106.5 1.2 collective-permute-done.26.refs_13_
  107.7 2.0 %collective-permute-start.21 = (bf16[256,128]{1,0:T(8,128)(2,1)S(1)}, bf16[256,128]{1,0:T(8,128)(2,1)S(1)}, u32[]{:S(2)}, u32[]{:S(2)}) collective-permute-start(bf16[256,128]{1,0:T(8,128)(2,1)S(1)} %get-tuple-element.53), channel_id=1, source_target_pairs={{0,4},{4,8},{8,12},{12,0},{1,5},{5,9},{9,13},{13,1},{2,6},{6,10},{... | collective-permute-start | bytes 196616 | tf_op jit(solution)/shard_map/ppermute | solution.py:902
  109.8 4.5 %collective-permute-done.20.refs_6_ = bf16[256,128]{1,0:T(8,128)(2,1)S(1)} collective-permute-done((bf16[256,128]{1,0:T(8,128)(2,1)S(1)}, bf16[256,128]{1,0:T(8,128)(2,1)S(1)}, u32[]{:S(2)}, u32[]{:S(2)}) %collective-permute-start.20) | collective-permute-done | bytes 65568 | tf_op jit(solution)/shard_map/ppermute | solution.py:902
  114.2 0.9 shard_map.203
  115.2 1.5 %collective-permute-done.27 = bf16[2,128,512]{2,1,0:T(8,128)(2,1)S(1)} collective-permute-done((bf16[2,128,512]{2,1,0:T(8,128)(2,1)S(1)}, bf16[2,128,512]{2,1,0:T(8,128)(2,1)S(1)}, u32[]{:S(2)}, u32[]{:S(2)}) %collective-permute-start.27) | collective-permute-done | bytes 262176 | tf_op jit(solution)/shard_map/ppermute | solution.py:899
  117.1 1.0 collective-permute-done.29
  118.2 2.1 %collective-permute-start.28 = (bf16[128,512]{1,0:T(8,128)(2,1)S(1)}, bf16[128,512]{1,0:T(8,128)(2,1)S(1)}, u32[]{:S(2)}, u32[]{:S(2)}) collective-permute-start(bf16[128,512]{1,0:T(8,128)(2,1)S(1)} %dynamic-slice_bitcast_fusion), channel_id=1, source_target_pairs={{0,4},{4,0},{8,12},{12,8},{1,5},{5,1},{9,13},{13,9},{2,6},{6,2},{1... | collective-permute-start | bytes 393224 | tf_op jit(solution)/shard_map/ppermute | solution.py:992
  120.3 1.5 %collective-permute-done.30 = f32[128]{0:T(128)S(1)} collective-permute-done((f32[128]{0:T(128)S(1)}, f32[128]{0:T(128)S(1)}, u32[]{:S(2)}, u32[]{:S(2)}) %collective-permute-start.30) | collective-permute-done | bytes 544 | tf_op jit(solution)/shard_map/ppermute | solution.py:992
  121.9 2.0 %collective-permute-done.28 = bf16[128,512]{1,0:T(8,128)(2,1)S(1)} collective-permute-done((bf16[128,512]{1,0:T(8,128)(2,1)S(1)}, bf16[128,512]{1,0:T(8,128)(2,1)S(1)}, u32[]{:S(2)}, u32[]{:S(2)}) %collective-permute-start.28) | collective-permute-done | bytes 131104 | tf_op jit(solution)/shard_map/ppermute | solution.py:992
  123.9 0.8 fusion.1
  (107 shorter events, 1.9 us)
Async XLA Ops:
  2.3 6.5 %copy-start = (bf16[2,64,2048]{2,1,0:T(8,128)(2,1)S(1)}, bf16[2,64,2048]{2,1,0:T(8,128)(2,1)}, u32[]{:S(2)}) copy-start(bf16[2,64,2048]{2,1,0:T(8,128)(2,1)} %param.21) | copy-start | bytes 1572868
  2.3 6.5 %copy-start.6 = (f32[2048]{0:T(1024)S(1)}, f32[2048]{0:T(1024)}, u32[]{:S(2)}) copy-start(f32[2048]{0:T(1024)} %param.22) | copy-start | bytes 24580
  2.3 32.7 %all-to-all-start = ((bf16[4,128,512]{2,1,0:T(8,128)(2,1)}), bf16[4,128,512]{2,1,0:T(8,128)(2,1)S(1)}, u32[]{:S(2)}, u32[]{:S(2)}) async-start(bf16[4,128,512]{2,1,0:T(8,128)(2,1)} %get-tuple-element.31), calls=%async_computation | async-start | bytes 1048576 | tf_op jit(solution)/shard_map/all_to_all | solution.py:896
  9.2 26.0 %copy-start.1 = (bf16[128,1024]{1,0:T(8,128)(2,1)}, bf16[128,1024]{1,0:T(8,128)(2,1)S(1)}, u32[]{:S(2)}) copy-start(bf16[128,1024]{1,0:T(8,128)(2,1)S(1)} %get-tuple-element.33.refs_0_) | copy-start | bytes 786436
  9.2 26.0 %copy-start.2 = (bf16[128,1024]{1,0:T(8,128)(2,1)}, bf16[128,1024]{1,0:T(8,128)(2,1)S(1)}, u32[]{:S(2)}) copy-start(bf16[128,1024]{1,0:T(8,128)(2,1)S(1)} %get-tuple-element.35.refs_4_) | copy-start | bytes 786436
  9.2 25.3 %collective-permute-start.1 = (bf16[128,1024]{1,0:T(8,128)(2,1)S(1)}, bf16[128,1024]{1,0:T(8,128)(2,1)S(1)}, u32[]{:S(2)}, u32[]{:S(2)}) collective-permute-start(bf16[128,1024]{1,0:T(8,128)(2,1)S(1)} %get-tuple-element.33.refs_0_), channel_id=1, source_target_pairs={{0,8},{4,12},{8,0},{12,4},{1,9},{5,13},{9,1},{13,5},{2,10},{6,14},... | collective-permute-start | bytes 786440 | tf_op jit(solution)/shard_map/ppermute | solution.py:902
  12.2 22.4 %collective-permute-start = (bf16[128,1024]{1,0:T(8,128)(2,1)S(1)}, bf16[128,1024]{1,0:T(8,128)(2,1)S(1)}, u32[]{:S(2)}, u32[]{:S(2)}) collective-permute-start(bf16[128,1024]{1,0:T(8,128)(2,1)S(1)} %get-tuple-element.33.refs_0_), channel_id=1, source_target_pairs={{0,4},{4,0},{8,12},{12,8},{1,5},{5,1},{9,13},{13,9},{2,6},{6,2},{1... | collective-permute-start | bytes 786440 | tf_op jit(solution)/shard_map/ppermute | solution.py:916
  13.6 5.0 %collective-permute-start.9 = (bf16[128,512]{1,0:T(8,128)(2,1)S(1)}, bf16[128,512]{1,0:T(8,128)(2,1)S(1)}, u32[]{:S(2)}, u32[]{:S(2)}) collective-permute-start(bf16[128,512]{1,0:T(8,128)(2,1)S(1)} %copy-done.31), channel_id=1, source_target_pairs={{0,16},{16,0},{1,17},{17,1},{2,18},{18,2},{3,19},{19,3},{4,20},{20... | collective-permute-start | bytes 393224 | tf_op jit(solution)/shard_map/ppermute | solution.py:899
  15.2 20.9 %collective-permute-start.6 = (bf16[128,512]{1,0:T(8,128)(2,1)S(1)}, bf16[128,512]{1,0:T(8,128)(2,1)S(1)}, u32[]{:S(2)}, u32[]{:S(2)}) collective-permute-start(bf16[128,512]{1,0:T(8,128)(2,1)S(1)} %copy-done.31), channel_id=1, source_target_pairs={{0,2},{2,0},{1,3},{3,1},{4,6},{6,4},{5,7},{7,5},{8,10},{10,8},{9,1... | collective-permute-start | bytes 393224 | tf_op jit(solution)/shard_map/ppermute | solution.py:899
  18.6 16.6 %copy-start.24 = (bf16[128,512]{1,0:T(8,128)(2,1)}, bf16[128,512]{1,0:T(8,128)(2,1)S(1)}, u32[]{:S(2)}) copy-start(bf16[128,512]{1,0:T(8,128)(2,1)S(1)} %collective-permute-done.9.refs_12_) | copy-start | bytes 393220
  18.6 19.0 %collective-permute-start.12 = (bf16[128,512]{1,0:T(8,128)(2,1)S(1)}, bf16[128,512]{1,0:T(8,128)(2,1)S(1)}, u32[]{:S(2)}, u32[]{:S(2)}) collective-permute-start(bf16[128,512]{1,0:T(8,128)(2,1)S(1)} %collective-permute-done.9.refs_12_), channel_id=1, source_target_pairs={{0,2},{2,0},{1,3},{3,1},{4,6},{6,4},{5,7},{7,5},{8,10},{10,8},{9,1... | collective-permute-start | bytes 393224 | tf_op jit(solution)/shard_map/ppermute | solution.py:899
  34.5 7.3 %collective-permute-start.2 = (bf16[128,1024]{1,0:T(8,128)(2,1)S(1)}, bf16[128,1024]{1,0:T(8,128)(2,1)S(1)}, u32[]{:S(2)}, u32[]{:S(2)}) collective-permute-start(bf16[128,1024]{1,0:T(8,128)(2,1)S(1)} %collective-permute-done.1.refs_2_), channel_id=1, source_target_pairs={{0,4},{4,0},{8,12},{12,8},{1,5},{5,1},{9,13},{13,9},{2,6},{6,2},{1... | collective-permute-start | bytes 786440 | tf_op jit(solution)/shard_map/ppermute | solution.py:916
  34.5 9.4 %collective-permute-start.4 = (bf16[128,1024]{1,0:T(8,128)(2,1)S(1)}, bf16[128,1024]{1,0:T(8,128)(2,1)S(1)}, u32[]{:S(2)}, u32[]{:S(2)}) collective-permute-start(bf16[128,1024]{1,0:T(8,128)(2,1)S(1)} %collective-permute-done.1.refs_2_), channel_id=1, source_target_pairs={{0,1},{1,0},{2,3},{3,2},{4,5},{5,4},{6,7},{7,6},{8,9},{9,8},{10,11... | collective-permute-start | bytes 786440 | tf_op jit(solution)/shard_map/ppermute | solution.py:899
  34.6 11.0 %collective-permute-start.3 = (bf16[128,1024]{1,0:T(8,128)(2,1)S(1)}, bf16[128,1024]{1,0:T(8,128)(2,1)S(1)}, u32[]{:S(2)}, u32[]{:S(2)}) collective-permute-start(bf16[128,1024]{1,0:T(8,128)(2,1)S(1)} %collective-permute-done.refs_1_), channel_id=1, source_target_pairs={{0,1},{1,0},{2,3},{3,2},{4,5},{5,4},{6,7},{7,6},{8,9},{9,8},{10,11... | collective-permute-start | bytes 786440 | tf_op jit(solution)/shard_map/ppermute | solution.py:899
  36.0 5.9 %copy-start.25 = (bf16[128,512]{1,0:T(8,128)(2,1)}, bf16[128,512]{1,0:T(8,128)(2,1)S(1)}, u32[]{:S(2)}) copy-start(bf16[128,512]{1,0:T(8,128)(2,1)S(1)} %collective-permute-done.6.refs_9_) | copy-start | bytes 393220
  36.0 11.0 %collective-permute-start.10 = (bf16[192,512]{1,0:T(8,128)(2,1)}, bf16[192,512]{1,0:T(8,128)(2,1)S(1)}, u32[]{:S(2)}, u32[]{:S(2)}) collective-permute-start(bf16[192,512]{1,0:T(8,128)(2,1)} %get-tuple-element.62), channel_id=1, source_target_pairs={{0,16},{16,0},{1,17},{17,1},{2,18},{18,2},{3,19},{19,3},{4,20},{20... | collective-permute-start | bytes 589832 | tf_op jit(solution)/shard_map/ppermute | solution.py:899
  38.3 9.3 %collective-permute-start.8 = (bf16[192,512]{1,0:T(8,128)(2,1)}, bf16[192,512]{1,0:T(8,128)(2,1)S(1)}, u32[]{:S(2)}, u32[]{:S(2)}) collective-permute-start(bf16[192,512]{1,0:T(8,128)(2,1)} %get-tuple-element.61), channel_id=1, source_target_pairs={{0,2},{2,0},{1,3},{3,1},{4,6},{6,4},{5,7},{7,5},{8,10},{10,8},{9,1... | collective-permute-start | bytes 589832 | tf_op jit(solution)/shard_map/ppermute | solution.py:899
  41.9 6.4 %collective-permute-start.5 = (bf16[128,1024]{1,0:T(8,128)(2,1)S(1)}, bf16[128,1024]{1,0:T(8,128)(2,1)S(1)}, u32[]{:S(2)}, u32[]{:S(2)}) collective-permute-start(bf16[128,1024]{1,0:T(8,128)(2,1)S(1)} %collective-permute-done.2.refs_3_), channel_id=1, source_target_pairs={{0,1},{1,0},{2,3},{3,2},{4,5},{5,4},{6,7},{7,6},{8,9},{9,8},{10,11... | collective-permute-start | bytes 786440 | tf_op jit(solution)/shard_map/ppermute | solution.py:899
  41.9 6.2 %copy-start.16 = (bf16[512,256]{1,0:T(8,128)(2,1)S(1)}, bf16[512,256]{1,0:T(8,128)(2,1)}, u32[]{:S(2)}) copy-start(bf16[512,256]{1,0:T(8,128)(2,1)} %param.37) | copy-start | bytes 786436
  41.9 6.2 %copy-start.17 = (bf16[512,256]{1,0:T(8,128)(2,1)S(1)}, bf16[512,256]{1,0:T(8,128)(2,1)}, u32[]{:S(2)}) copy-start(bf16[512,256]{1,0:T(8,128)(2,1)} %param.38) | copy-start | bytes 786436
  44.0 8.0 %collective-permute-start.11 = (bf16[192,512]{1,0:T(8,128)(2,1)}, bf16[192,512]{1,0:T(8,128)(2,1)S(1)}, u32[]{:S(2)}, u32[]{:S(2)}) collective-permute-start(bf16[192,512]{1,0:T(8,128)(2,1)} %get-tuple-element.61), channel_id=1, source_target_pairs={{0,16},{16,0},{1,17},{17,1},{2,18},{18,2},{3,19},{19,3},{4,20},{20... | collective-permute-start | bytes 589832 | tf_op jit(solution)/shard_map/ppermute | solution.py:899
  45.5 8.0 %collective-permute-start.7 = (bf16[192,512]{1,0:T(8,128)(2,1)}, bf16[192,512]{1,0:T(8,128)(2,1)S(1)}, u32[]{:S(2)}, u32[]{:S(2)}) collective-permute-start(bf16[192,512]{1,0:T(8,128)(2,1)} %get-tuple-element.62), channel_id=1, source_target_pairs={{0,2},{2,0},{1,3},{3,1},{4,6},{6,4},{5,7},{7,5},{8,10},{10,8},{9,1... | collective-permute-start | bytes 589832 | tf_op jit(solution)/shard_map/ppermute | solution.py:899
  47.0 9.9 %collective-permute-start.13 = (bf16[192,512]{1,0:T(8,128)(2,1)S(1)}, bf16[192,512]{1,0:T(8,128)(2,1)S(1)}, u32[]{:S(2)}, u32[]{:S(2)}) collective-permute-start(bf16[192,512]{1,0:T(8,128)(2,1)S(1)} %collective-permute-done.10.refs_13_), channel_id=1, source_target_pairs={{0,2},{2,0},{1,3},{3,1},{4,6},{6,4},{5,7},{7,5},{8,10},{10,8},{9,1... | collective-permute-start | bytes 589832 | tf_op jit(solution)/shard_map/ppermute | solution.py:899
  47.6 9.4 %collective-permute-start.14 = (bf16[192,512]{1,0:T(8,128)(2,1)S(1)}, bf16[192,512]{1,0:T(8,128)(2,1)S(1)}, u32[]{:S(2)}, u32[]{:S(2)}) collective-permute-start(bf16[192,512]{1,0:T(8,128)(2,1)S(1)} %collective-permute-done.8.refs_11_), channel_id=1, source_target_pairs={{0,16},{16,0},{1,17},{17,1},{2,18},{18,2},{3,19},{19,3},{4,20},{20... | collective-permute-start | bytes 589832 | tf_op jit(solution)/shard_map/ppermute | solution.py:899
  48.3 8.7 %copy-start.15 = (bf16[128,1024]{1,0:T(8,128)(2,1)}, bf16[128,1024]{1,0:T(8,128)(2,1)S(1)}, u32[]{:S(2)}) copy-start(bf16[128,1024]{1,0:T(8,128)(2,1)S(1)} %collective-permute-done.5.refs_7_) | copy-start | bytes 786436
  52.0 5.0 %copy-start.20 = (bf16[192,512]{1,0:T(8,128)(2,1)}, bf16[192,512]{1,0:T(8,128)(2,1)S(1)}, u32[]{:S(2)}) copy-start(bf16[192,512]{1,0:T(8,128)(2,1)S(1)} %collective-permute-done.11.refs_14_) | copy-start | bytes 589828
  62.3 31.0 %all-to-all-start.1 = ((bf16[4,384,128]{2,1,0:T(8,128)(2,1)}), bf16[4,384,128]{2,1,0:T(8,128)(2,1)S(1)}, u32[]{:S(2)}, u32[]{:S(2)}) async-start(bf16[4,384,128]{2,1,0:T(8,128)(2,1)} %get-tuple-element.45), calls=%async_computation.1 | async-start | bytes 786432 | tf_op jit(solution)/shard_map/all_to_all | solution.py:896
  65.9 22.6 %collective-permute-start.23 = (bf16[512,256]{1,0:T(8,128)(2,1)S(1)}, bf16[512,256]{1,0:T(8,128)(2,1)S(1)}, u32[]{:S(2)}, u32[]{:S(2)}) collective-permute-start(bf16[512,256]{1,0:T(8,128)(2,1)S(1)} %constant_dynamic-slice_fusion.2), channel_id=1, source_target_pairs={{0,8},{4,12},{8,0},{12,4},{1,9},{5,13},{9,1},{13,5},{2,10},{6,14},... | collective-permute-start | bytes 786440 | tf_op jit(solution)/shard_map/ppermute | solution.py:902
  68.8 34.3 %collective-permute-start.22 = (bf16[1024,256]{1,0:T(8,128)(2,1)S(1)}, bf16[1024,256]{1,0:T(8,128)(2,1)S(1)}, u32[]{:S(2)}, u32[]{:S(2)}) collective-permute-start(bf16[1024,256]{1,0:T(8,128)(2,1)S(1)} %pad_maximum_fusion.refs_8_), channel_id=1, source_target_pairs={{0,2},{2,0},{1,3},{3,1},{4,6},{6,4},{5,7},{7,5},{8,10},{10,8},{9,1... | collective-permute-start | bytes 1572872 | tf_op jit(solution)/shard_map/ppermute | solution.py:899
  88.5 7.3 %collective-permute-start.24 = (bf16[512,256]{1,0:T(8,128)(2,1)S(1)}, bf16[512,256]{1,0:T(8,128)(2,1)S(1)}, u32[]{:S(2)}, u32[]{:S(2)}) collective-permute-start(bf16[512,256]{1,0:T(8,128)(2,1)S(1)} %collective-permute-done.23.refs_10_), channel_id=1, source_target_pairs={{0,16},{16,0},{1,17},{17,1},{2,18},{18,2},{3,19},{19,3},{4,20},{20... | collective-permute-start | bytes 786440 | tf_op jit(solution)/shard_map/ppermute | solution.py:899
  89.0 9.7 %copy-start.3 = (f32[256,64]{1,0:T(8,128)S(1)}, f32[256,64]{1,0:T(8,128)}, u32[]{:S(2)}) copy-start(f32[256,64]{1,0:T(8,128)} %constant.53.clone.cos_ref) | copy-start | bytes 196612
  89.0 9.7 %copy-start.4 = (f32[256,64]{1,0:T(8,128)S(1)}, f32[256,64]{1,0:T(8,128)}, u32[]{:S(2)}) copy-start(f32[256,64]{1,0:T(8,128)} %constant.54.clone.sin_ref) | copy-start | bytes 196612
  93.3 5.3 %copy-start.9 = (bf16[4,384,128]{2,1,0:T(8,128)(2,1)}, bf16[4,384,128]{2,1,0:T(8,128)(2,1)S(1)}, u32[]{:S(2)}) copy-start(bf16[4,384,128]{2,1,0:T(8,128)(2,1)S(1)} %all-to-all-done.1.mine_ref) | copy-start | bytes 1179652
  93.3 5.3 %collective-permute-start.18 = (bf16[4,384,128]{2,1,0:T(8,128)(2,1)S(1)}, bf16[4,384,128]{2,1,0:T(8,128)(2,1)S(1)}, u32[]{:S(2)}, u32[]{:S(2)}) collective-permute-start(bf16[4,384,128]{2,1,0:T(8,128)(2,1)S(1)} %all-to-all-done.1.mine_ref), channel_id=1, source_target_pairs={{0,1},{1,0},{2,3},{3,2},{4,5},{5,4},{6,7},{7,6},{8,9},{9,8},{10,11... | collective-permute-start | bytes 1179656 | tf_op jit(solution)/shard_map/ppermute | solution.py:899
  93.4 9.2 %collective-permute-start.25 = (bf16[512,256]{1,0:T(8,128)(2,1)S(1)}, bf16[512,256]{1,0:T(8,128)(2,1)S(1)}, u32[]{:S(2)}, u32[]{:S(2)}) collective-permute-start(bf16[512,256]{1,0:T(8,128)(2,1)S(1)} %collective-permute-done.23.refs_10_), channel_id=1, source_target_pairs={{0,2},{2,0},{1,3},{3,1},{4,6},{6,4},{5,7},{7,5},{8,10},{10,8},{9,1... | collective-permute-start | bytes 786440 | tf_op jit(solution)/shard_map/ppermute | solution.py:899
  95.8 11.9 %collective-permute-start.26 = (bf16[512,256]{1,0:T(8,128)(2,1)S(1)}, bf16[512,256]{1,0:T(8,128)(2,1)S(1)}, u32[]{:S(2)}, u32[]{:S(2)}) collective-permute-start(bf16[512,256]{1,0:T(8,128)(2,1)S(1)} %collective-permute-done.24.refs_11_), channel_id=1, source_target_pairs={{0,2},{2,0},{1,3},{3,1},{4,6},{6,4},{5,7},{7,5},{8,10},{10,8},{9,1... | collective-permute-start | bytes 786440 | tf_op jit(solution)/shard_map/ppermute | solution.py:899
  97.3 10.4 %collective-permute-start.15 = (bf16[256,128]{1,0:T(8,128)(2,1)}, bf16[256,128]{1,0:T(8,128)(2,1)S(1)}, u32[]{:S(2)}, u32[]{:S(2)}) collective-permute-start(bf16[256,128]{1,0:T(8,128)(2,1)} %get-tuple-element.42), channel_id=1, source_target_pairs={{0,12},{4,0},{8,4},{12,8},{1,13},{5,1},{9,5},{13,9},{2,14},{6,2},{... | collective-permute-start | bytes 196616 | tf_op jit(solution)/shard_map/ppermute | solution.py:902
  98.7 11.1 %collective-permute-start.16 = (bf16[256,128]{1,0:T(8,128)(2,1)}, bf16[256,128]{1,0:T(8,128)(2,1)S(1)}, u32[]{:S(2)}, u32[]{:S(2)}) collective-permute-start(bf16[256,128]{1,0:T(8,128)(2,1)} %get-tuple-element.43), channel_id=1, source_target_pairs={{0,8},{4,12},{8,0},{12,4},{1,9},{5,13},{9,1},{13,5},{2,10},{6,14},... | collective-permute-start | bytes 196616 | tf_op jit(solution)/shard_map/ppermute | solution.py:902
  98.7 15.5 %copy-start.5 = (bf16[256,128]{1,0:T(8,128)(2,1)S(1)}, bf16[256,128]{1,0:T(8,128)(2,1)}, u32[]{:S(2)}) copy-start(bf16[256,128]{1,0:T(8,128)(2,1)} %get-tuple-element.41.refs_0_) | copy-start | bytes 196612
  102.6 7.1 %collective-permute-start.17 = (bf16[256,128]{1,0:T(8,128)(2,1)S(1)}, bf16[256,128]{1,0:T(8,128)(2,1)S(1)}, u32[]{:S(2)}, u32[]{:S(2)}) collective-permute-start(bf16[256,128]{1,0:T(8,128)(2,1)S(1)} %copy-done.32), channel_id=1, source_target_pairs={{0,4},{4,8},{8,12},{12,0},{1,5},{5,9},{9,13},{13,1},{2,6},{6,10},{... | collective-permute-start | bytes 196616 | tf_op jit(solution)/shard_map/ppermute | solution.py:902
  103.1 11.1 %copy-start.7 = (f32[1024]{0:T(1024)S(1)}, f32[1024]{0:T(1024)}, u32[]{:S(2)}) copy-start(f32[1024]{0:T(1024)} %param.39) | copy-start | bytes 12292
  103.1 6.7 %collective-permute-start.19 = (bf16[256,128]{1,0:T(8,128)(2,1)S(1)}, bf16[256,128]{1,0:T(8,128)(2,1)S(1)}, u32[]{:S(2)}, u32[]{:S(2)}) collective-permute-start(bf16[256,128]{1,0:T(8,128)(2,1)S(1)} %get-tuple-element.51), channel_id=1, source_target_pairs={{0,12},{4,0},{8,4},{12,8},{1,13},{5,1},{9,5},{13,9},{2,14},{6,2},{... | collective-permute-start | bytes 196616 | tf_op jit(solution)/shard_map/ppermute | solution.py:902
  107.7 6.5 %collective-permute-start.20 = (bf16[256,128]{1,0:T(8,128)(2,1)S(1)}, bf16[256,128]{1,0:T(8,128)(2,1)S(1)}, u32[]{:S(2)}, u32[]{:S(2)}) collective-permute-start(bf16[256,128]{1,0:T(8,128)(2,1)S(1)} %get-tuple-element.52), channel_id=1, source_target_pairs={{0,8},{4,12},{8,0},{12,4},{1,9},{5,13},{9,1},{13,5},{2,10},{6,14},... | collective-permute-start | bytes 196616 | tf_op jit(solution)/shard_map/ppermute | solution.py:902
  107.7 6.5 %collective-permute-start.21 = (bf16[256,128]{1,0:T(8,128)(2,1)S(1)}, bf16[256,128]{1,0:T(8,128)(2,1)S(1)}, u32[]{:S(2)}, u32[]{:S(2)}) collective-permute-start(bf16[256,128]{1,0:T(8,128)(2,1)S(1)} %get-tuple-element.53), channel_id=1, source_target_pairs={{0,4},{4,8},{8,12},{12,0},{1,5},{5,9},{9,13},{13,1},{2,6},{6,10},{... | collective-permute-start | bytes 196616 | tf_op jit(solution)/shard_map/ppermute | solution.py:902
  115.1 1.6 %collective-permute-start.27 = (bf16[2,128,512]{2,1,0:T(8,128)(2,1)S(1)}, bf16[2,128,512]{2,1,0:T(8,128)(2,1)S(1)}, u32[]{:S(2)}, u32[]{:S(2)}) collective-permute-start(bf16[2,128,512]{2,1,0:T(8,128)(2,1)S(1)} %get-tuple-element.55), channel_id=1, source_target_pairs={{0,1},{1,0},{2,3},{3,2},{4,5},{5,4},{6,7},{7,6},{8,9},{9,8},{10,11... | collective-permute-start | bytes 786440 | tf_op jit(solution)/shard_map/ppermute | solution.py:899
  116.9 1.2 collective-permute-start.29
  118.1 3.6 %collective-permute-start.30 = (f32[128]{0:T(128)S(1)}, f32[128]{0:T(128)S(1)}, u32[]{:S(2)}, u32[]{:S(2)}) collective-permute-start(f32[128]{0:T(128)S(1)} %fusion.7), channel_id=1, source_target_pairs={{0,4},{4,0},{8,12},{12,8},{1,5},{5,1},{9,13},{13,9},{2,6},{6,2},{1... | collective-permute-start | bytes 1544 | tf_op jit(solution)/shard_map/ppermute | solution.py:992
  118.2 5.6 %collective-permute-start.28 = (bf16[128,512]{1,0:T(8,128)(2,1)S(1)}, bf16[128,512]{1,0:T(8,128)(2,1)S(1)}, u32[]{:S(2)}, u32[]{:S(2)}) collective-permute-start(bf16[128,512]{1,0:T(8,128)(2,1)S(1)} %dynamic-slice_bitcast_fusion), channel_id=1, source_target_pairs={{0,4},{4,0},{8,12},{12,8},{1,5},{5,1},{9,13},{13,9},{2,6},{6,2},{1... | collective-permute-start | bytes 393224 | tf_op jit(solution)/shard_map/ppermute | solution.py:992
  (18 other events, 42.4 us)
